TPU v7x, 32 devices: a whole 2x2x4 slice. The times are simulated.
32 devices in a mesh: grp: 2 (over y), sp: 4 (over z), tp: 4 (over x, core).
Axes of the slice: x: 2, y: 2, z: 4, core: 2. Of those that a mesh axis runs over, the one named last changes fastest.
Arguments:
- queries_small: bfloat16 [2048, 1024], P(('grp', 'sp'), 'tp'), parts along dimension 0, may hold values from -6 to 6
- keys_small: bfloat16 [2048, 512], P(('grp', 'sp'), 'tp'), parts along dimension 0, may hold values from -6 to 6
- values_small: bfloat16 [2048, 512], P(('grp', 'sp'), 'tp'), parts along dimension 0, may hold values from -6 to 6
- queries_large: bfloat16 [2048, 1024], P(('grp', 'sp'), 'tp'), parts along dimension 0, may hold values from -6 to 6
- keys_large: bfloat16 [2048, 512], P(('grp', 'sp'), 'tp'), parts along dimension 0, may hold values from -6 to 6
- values_large: bfloat16 [2048, 512], P(('grp', 'sp'), 'tp'), parts along dimension 0, may hold values from -6 to 6
- query_gain_small: float32 [128], P('grp'), parts along dimension 0, may hold values from 1.2 to 12
- key_gain_small: float32 [128], P('grp'), parts along dimension 0, may hold values from 1.2 to 12
- query_gain_large: float32 [256], P('grp'), parts along dimension 0, may hold values from 1.2 to 12
- key_gain_large: float32 [256], P('grp'), parts along dimension 0, may hold values from 1.2 to 12
- residual_in: bfloat16 [2048, 2048], P(('grp', 'sp', 'tp')), parts along dimension 0, may hold values from -1.5 to 1.5
- out_weight_small: bfloat16 [1024, 2048], P('tp'), may hold values from -0.125 to 0.125
- out_weight_large: bfloat16 [1024, 2048], P('tp'), may hold values from -0.125 to 0.125
- norm_gain: float32 [2048], replicated, may hold values from 0.1 to 1.9
- routes: int32 [2048, 2], P(('grp', 'sp', 'tp')), parts along dimension 0, may hold values from 0 to 7, all different within a row; in each aligned block of 64 rows (0 to 63, 64 to 127, ...) at most 32 rows name the same one
- route_scores: float32 [2048, 2], P(('grp', 'sp', 'tp')), parts along dimension 0, may hold values from 0.05 to 1
- expert_gate: bfloat16 [8, 2048, 1024], P('sp', None, 'tp'), may hold values from -0.125 to 0.125
- expert_up: bfloat16 [8, 2048, 1024], P('sp', None, 'tp'), may hold values from -0.125 to 0.125
- expert_down: bfloat16 [8, 1024, 2048], P('sp', 'tp'), may hold values from -0.1875 to 0.1875
Outputs:
- result: bfloat16 [2048, 2048], P(('grp', 'sp', 'tp')), parts along dimension 0
There are 2 independent parts, one for each index of `grp`. A program takes and returns all parts, laid end to end along the dimension named above; an argument that names none is the same for every part. Nothing has to cross between parts.
Inputs may be any that keep to these rules, and one draw needn't show every extreme that they name: `routes`: each token names 2 different experts; within the rows of one device (aligned blocks of 64 tokens) no expert is named more than 32 times, a bound that some block reaches.
All inputs are finite; a program needn't handle non-finite values.
Results may differ from a plain program's by a relative error of at most 0.02.
The roundings to bfloat16 on the way count: a program that leaves them out, or rounds other values in their place, can miss the bound.
Values may be sent and summed in bfloat16 or wider, within the bound.
No kernel may reach another device: no remote copies, remote signals or barrier semaphores. Data moves between devices by JAX's collectives and lax.ppermute only.
A program may use at most 128 MiB of HBM per device.

v0:
```python
import jax
import jax.numpy as jnp
from jax import lax
from jax.sharding import PartitionSpec as P

HS_SMALL = 64
HS_LARGE = 128
GRID_W = 64


theta_base = 10000.0
norm_eps = 1e-06
block_target = 1280


def grid_tables(offset, length, head_size):
    places = offset + jnp.arange(length, dtype=jnp.int32)
    grid_rows = (places // GRID_W).astype(jnp.float32)
    grid_cols = (places % GRID_W).astype(jnp.float32)
    rates = jnp.power(
        theta_base, -2.0 * jnp.arange(head_size // 4, dtype=jnp.float32) / (head_size // 2)
    )
    row_angles = grid_rows[:, None, None] * rates
    col_angles = grid_cols[:, None, None] * rates
    return (jnp.cos(row_angles), jnp.sin(row_angles), jnp.cos(col_angles), jnp.sin(col_angles))


def half_turn(segment, cosine, sine_part):
    half_size = segment.shape[-1] // 2
    leading = segment[..., :half_size]
    trailing = segment[..., half_size:]
    return jnp.concatenate(
        [leading * cosine - trailing * sine_part, trailing * cosine + leading * sine_part], axis=-1
    )


def grid_turn(vectors, tables):
    row_cos, row_sin, col_cos, col_sin = tables
    half_size = vectors.shape[-1] // 2
    return jnp.concatenate(
        [
            half_turn(vectors[..., :half_size], row_cos, row_sin),
            half_turn(vectors[..., half_size:], col_cos, col_sin),
        ],
        axis=-1,
    )


def normed_turn(raw_rows, gain, tables):
    widened = raw_rows.astype(jnp.float32)
    scaled = (
        widened * lax.rsqrt(jnp.mean(widened * widened, axis=-1, keepdims=True) + norm_eps) * gain
    )
    return grid_turn(scaled, tables).astype(jnp.bfloat16)


def block_rows(row_count, shard_rows):
    shards = row_count // shard_rows
    chosen = 1
    for factor in range(1, max(1, block_target // shard_rows) + 1):
        if shards % factor == 0:
            chosen = factor
    return chosen * shard_rows


def attend_block(state, queries, key_rows, value_rows):
    largest, weight_sum, accumulated = state
    head_size = queries.shape[-1]
    kv_local = queries.shape[1]
    key_heads = key_rows.reshape(key_rows.shape[0], kv_local, head_size)
    value_heads = value_rows.reshape(value_rows.shape[0], kv_local, head_size)
    scores = jnp.einsum(
        "qgrd,kgd->qgrk", queries, key_heads, preferred_element_type=jnp.float32
    ) * head_size ** (-0.5)
    peak_score = jnp.maximum(largest, jnp.max(scores, axis=-1))
    shrink = jnp.exp(largest - peak_score)
    weights = jnp.exp(scores - peak_score[..., None])
    weight_sum = weight_sum * shrink + jnp.sum(weights, axis=-1)
    accumulated = accumulated * shrink[..., None] + jnp.einsum(
        "qgrk,kgd->qgrd",
        weights.astype(jnp.bfloat16),
        value_heads,
        preferred_element_type=jnp.float32,
    )
    return (peak_score, weight_sum, accumulated)


def attend_rows(state, queries, key_rows, value_rows):
    row_count = key_rows.shape[0]
    step_rows = block_rows(row_count, queries.shape[0])
    if step_rows == row_count:
        return attend_block(state, queries, key_rows, value_rows)

    def one_block(block_index, carried):
        offset = block_index * step_rows
        return attend_block(
            carried,
            queries,
            lax.dynamic_slice_in_dim(key_rows, offset, step_rows, 0),
            lax.dynamic_slice_in_dim(value_rows, offset, step_rows, 0),
        )

    return lax.fori_loop(0, row_count // step_rows, one_block, state)


def empty_state(queries):
    state_shape = queries.shape[:3]
    return (
        jnp.full(state_shape, -1e30, jnp.float32),
        jnp.zeros(state_shape, jnp.float32),
        jnp.zeros(queries.shape, jnp.float32),
    )


def finish(state):
    largest, weight_sum, accumulated = state
    merged = accumulated / weight_sum[..., None]
    return merged.reshape(merged.shape[0], -1).astype(jnp.bfloat16)


def on_device(
    queries_small,
    keys_small,
    values_small,
    queries_large,
    keys_large,
    values_large,
    query_gain_small,
    key_gain_small,
    query_gain_large,
    key_gain_large,
    residual_in,
    out_weight_small,
    out_weight_large,
    norm_gain,
    routes,
    route_scores,
    expert_gate,
    expert_up,
    expert_down,
):
    token_rows = queries_small.shape[0]
    offset = lax.axis_index("sp") * token_rows
    tables_small = grid_tables(offset, token_rows, HS_SMALL)
    tables_large = grid_tables(offset, token_rows, HS_LARGE)
    kv_small = keys_small.shape[1] // HS_SMALL
    kv_large = keys_large.shape[1] // HS_LARGE
    asked_small = normed_turn(
        queries_small.reshape(token_rows, -1, HS_SMALL), query_gain_small, tables_small
    ).reshape(token_rows, kv_small, -1, HS_SMALL)
    asked_large = normed_turn(
        queries_large.reshape(token_rows, -1, HS_LARGE), query_gain_large, tables_large
    ).reshape(token_rows, kv_large, -1, HS_LARGE)
    turned_small = normed_turn(
        keys_small.reshape(token_rows, kv_small, HS_SMALL), key_gain_small, tables_small
    ).reshape(token_rows, -1)
    turned_large = normed_turn(
        keys_large.reshape(token_rows, kv_large, HS_LARGE), key_gain_large, tables_large
    ).reshape(token_rows, -1)
    key_small = lax.all_gather(turned_small, "sp", axis=0, tiled=True)
    value_small = lax.all_gather(values_small, "sp", axis=0, tiled=True)
    key_large = lax.all_gather(turned_large, "sp", axis=0, tiled=True)
    value_large = lax.all_gather(values_large, "sp", axis=0, tiled=True)
    state_small = attend_rows(empty_state(asked_small), asked_small, key_small, value_small)
    state_large = attend_rows(empty_state(asked_large), asked_large, key_large, value_large)
    heard_small = finish(state_small)
    heard_large = finish(state_large)
    projected = lax.psum_scatter(
        (
            jnp.dot(heard_small, out_weight_small, preferred_element_type=jnp.float32)
            + jnp.dot(heard_large, out_weight_large, preferred_element_type=jnp.float32)
        ).astype(jnp.bfloat16),
        "tp",
        scatter_dimension=0,
        tiled=True,
    ).astype(jnp.float32)
    attended = (residual_in.astype(jnp.float32) + projected).astype(jnp.bfloat16)
    widened = attended.astype(jnp.float32)
    normed = (
        widened
        * lax.rsqrt(jnp.mean(widened * widened, axis=-1, keepdims=True) + norm_eps)
        * norm_gain
    ).astype(jnp.bfloat16)
    local_rows = routes.shape[0]
    top_count = routes.shape[1]
    sp_count = lax.axis_size("sp")
    local_experts = expert_gate.shape[0]
    expert_count = local_experts * sp_count
    capacity = max(2, (2 * top_count * local_rows + expert_count - 1) // expert_count)
    flat_routes = routes.reshape(-1)
    member = (flat_routes[:, None] == jnp.arange(expert_count, dtype=jnp.int32)[None, :]).astype(
        jnp.int32
    )
    ranks = jnp.sum((jnp.cumsum(member, axis=0) - member) * member, axis=1)
    slots = flat_routes * capacity + ranks
    picker = (
        slots[:, None] == jnp.arange(expert_count * capacity, dtype=jnp.int32)[None, :]
    ).astype(jnp.bfloat16)
    placer = jnp.sum(picker.reshape(local_rows, top_count, -1), axis=1)
    outgoing = jnp.einsum("ts,td->sd", placer, normed, preferred_element_type=jnp.float32).astype(
        jnp.bfloat16
    )
    outgoing = outgoing.reshape(sp_count, local_experts, capacity, -1)
    everyone = lax.all_gather(
        lax.all_to_all(outgoing, "sp", split_axis=0, concat_axis=0, tiled=True),
        "tp",
        axis=0,
        tiled=True,
    )
    gate_out = jnp.einsum(
        "secd,edf->secf", everyone, expert_gate, preferred_element_type=jnp.float32
    )
    up_out = jnp.einsum("secd,edf->secf", everyone, expert_up, preferred_element_type=jnp.float32)
    active = (jax.nn.silu(gate_out) * up_out).astype(jnp.bfloat16)
    summed = lax.psum_scatter(
        jnp.einsum(
            "secf,efd->secd", active, expert_down, preferred_element_type=jnp.float32
        ).astype(jnp.bfloat16),
        "tp",
        scatter_dimension=0,
        tiled=True,
    )
    returned = lax.all_to_all(summed, "sp", split_axis=0, concat_axis=0, tiled=True)
    back_rows = returned.reshape(expert_count * capacity, -1)
    chosen_rows = jnp.dot(picker, back_rows, preferred_element_type=jnp.float32).reshape(
        local_rows, top_count, -1
    )
    shares = route_scores / jnp.sum(route_scores, axis=1, keepdims=True)
    mixed = jnp.sum(chosen_rows * shares[:, :, None], axis=1)
    return (attended.astype(jnp.float32) + mixed).astype(jnp.bfloat16)


def solution(mesh):
    in_specs = (
        P(("grp", "sp"), "tp"),
        P(("grp", "sp"), "tp"),
        P(("grp", "sp"), "tp"),
        P(("grp", "sp"), "tp"),
        P(("grp", "sp"), "tp"),
        P(("grp", "sp"), "tp"),
        P("grp"),
        P("grp"),
        P("grp"),
        P("grp"),
        P(("grp", "sp", "tp"), None),
        P("tp", None),
        P("tp", None),
        P(),
        P(("grp", "sp", "tp"), None),
        P(("grp", "sp", "tp"), None),
        P("sp", None, "tp"),
        P("sp", None, "tp"),
        P("sp", "tp", None),
    )
    out_specs = P(("grp", "sp", "tp"), None)
    return jax.shard_map(
        on_device, mesh=mesh, in_specs=in_specs, out_specs=out_specs, check_vma=False
    )
```

profile of v0, /device:TPU:0, one launch (start us, length us, event | category | flops | bytes accessed | tf_op | source)
XLA Modules:
  0.0 313.0 jit_solution(7394251430156797041)
XLA Ops:
  6.6 1.1 copy.83
  7.7 0.7 fusion.63
  8.5 1.0 multiply_cosine_fusion.1
  9.5 0.3 fusion.104
  9.8 15.7 %all_gather.17 = bf16[1024,128]{0,1:T(8,128)(2,1)S(1)} all-gather(bf16[256,128]{0,1:T(8,128)(2,1)S(1)} %pad_maximum_fusion.1), channel_id=1, replica_groups=mesh['grp'=2,'sp'=4,'tp'=4] {'sp'}, dimensions={0}, use_global_device_ids=true | all-gather | bytes 327680 | tf_op jit(solution)/shard_map/all_gather | solution.py:162
  25.5 1.0 copy.84
  26.5 0.1 copy.85
  26.6 0.1 multiply_multiply_fusion
  26.8 0.3 subtract_convert_fusion.1
  27.1 0.0 copy-start.9
  27.1 0.0 copy-start.10
  27.1 0.6 bitcast_reduce_fusion.1
  27.7 0.0 copy-start.7
  27.7 0.0 copy-start.16
  27.8 1.3 copy-done.2
  29.0 0.4 fusion.12
  29.4 0.1 copy.87
  29.5 14.4 %all_gather.18 = bf16[1024,128]{0,1:T(8,128)(2,1)S(1)} all-gather(bf16[256,128]{0,1:T(8,128)(2,1)S(1)} %copy.87), channel_id=1, replica_groups=mesh['grp'=2,'sp'=4,'tp'=4] {'sp'}, dimensions={0}, use_global_device_ids=true | all-gather | bytes 327680 | tf_op jit(solution)/shard_map/all_gather | solution.py:163
  44.0 0.2 multiply_cosine_fusion.5
  44.2 0.1 copy.79
  44.3 0.1 fusion.65
  44.5 13.8 %all_gather.15 = bf16[1024,128]{0,1:T(8,128)(2,1)S(1)} all-gather(bf16[256,128]{0,1:T(8,128)(2,1)S(1)} %bitcast.168), channel_id=1, replica_groups=mesh['grp'=2,'sp'=4,'tp'=4] {'sp'}, dimensions={0}, use_global_device_ids=true | all-gather | bytes 327680 | tf_op jit(solution)/shard_map/all_gather | solution.py:160
  58.3 0.1 copy.80
  58.5 0.1 fusion.54
  58.6 0.8 bitcast_reduce_fusion
  59.4 0.7 fusion.1
  60.1 1.2 copy-done.1
  61.3 13.8 %all_gather.16 = bf16[1024,128]{1,0:T(8,128)(2,1)S(1)} all-gather(bf16[256,128]{1,0:T(8,128)(2,1)S(1)} %copy-done.8), channel_id=1, replica_groups=mesh['grp'=2,'sp'=4,'tp'=4] {'sp'}, dimensions={0}, use_global_device_ids=true | all-gather | bytes 327680 | tf_op jit(solution)/shard_map/all_gather | solution.py:161
  75.1 0.1 copy.81
  75.3 3.1 fusion.38
  78.4 0.5 fusion.117
  78.9 1.1 copy-done.3
  80.0 0.5 fusion.41
  80.5 1.5 fusion.3
  82.0 0.0 reduce-scatter.5.cloned.1.call-update
  82.0 0.0 all-gather.2.cloned.1.call-start
  82.1 0.1 copy.89
  82.2 0.1 eq.54
  82.3 0.1 fusion.86
  82.4 0.2 reduce_window_sum.11
  82.6 0.2 select_reduce_fusion
  82.8 0.1 reduce_sum.111
  82.9 0.1 copy.90
  83.0 0.1 fusion.84
  83.1 25.4 %reduce-scatter.5.cloned.1.call-done = bf16[64,2048]{1,0:T(8,128)(2,1)} async-done(((bf16[256,2048]{1,0:T(8,128)(2,1)}), bf16[64,2048]{1,0:T(8,128)(2,1)}) %reduce-scatter.5.cloned.1.call-update) | async-done | bytes 262160 | tf_op jit(solution)/shard_map/reduce_scatter | solution.py:168
  108.5 1.1 fusion.48
  109.7 1.4 convolution_convert_fusion
  111.1 30.0 %all_to_all.10 = bf16[4,2,32,2048]{3,2,1,0:T(8,128)(2,1)S(1)} all-to-all(bf16[4,2,32,2048]{3,2,1,0:T(8,128)(2,1)S(1)} %bitcast.163), channel_id=1, replica_groups=mesh['grp'=2,'sp'=4,'tp'=4] {'sp'}, dimensions={0} | all-to-all | bytes 2097152 | tf_op jit(solution)/shard_map/all_to_all | solution.py:205
  141.1 1.0 copy.91
  142.1 0.0 all-gather.2.cloned.1.call-update
  142.1 0.2 all-reduce.3.cloned.1.call-start
  142.4 32.5 %all-gather.2.cloned.1.call-done = bf16[16,2,32,2048]{3,2,0,1:T(8,128)(2,1)} async-done(((bf16[4,2,32,2048]{3,2,0,1:T(8,128)(2,1)}), bf16[16,2,32,2048]{3,2,0,1:T(8,128)(2,1)}) %all-gather.2.cloned.1.call-update) | async-done | bytes 4194320 | tf_op jit(solution)/shard_map/all_gather | solution.py:204
  174.9 4.1 %fusion.14 = f32[16,2,32,256]{3,2,0,1:T(8,128)S(1)} fusion(bf16[16,2,32,2048]{3,2,0,1:T(8,128)(2,1)} %all-gather.2.cloned.1.call-done, bf16[2,2048,256]{2,1,0:T(8,128)(2,1)} %param.35), kind=kOutput, calls=%fused_computation.21 | convolution fusion | flops 1073741824 | bytes 7340032 | tf_op jit(solution)/shard_map/secd,edf->secf/dot_general | solution.py:210
  179.0 7.3 %convert_bitcast_fusion = bf16[16,2,32,2048]{3,2,0,1:T(8,128)(2,1)} fusion(bf16[2,256,2048]{2,1,0:T(8,128)(2,1)S(1)} %copy-done, bf16[16,2,32,2048]{3,2,0,1:T(8,128)(2,1)} %all-gather.2.cloned.1.call-done, bf16[2,2048,256]{2,1,0:T(8,128)(2,1)} %param.36, f32[16,2,32,256]{3,2,0,1:T(8,128)S(1)} %fusion.14), kind=kOutput, calls=%fused_computation.3 | convolution fusion | flops 2151153664 | bytes 13631488 | tf_op jit(solution)/shard_map/secf,efd->secd/dot_general | solution.py:216
  186.3 0.0 all-reduce.3.cloned.1.call-update
  186.3 0.6 copy-done.17
  187.0 0.6 dynamic-slice
  188.2 83.8 %all-reduce.3.cloned.1.call-done = bf16[16,2,32,2048]{3,2,0,1:T(8,128)(2,1)} async-done(((bf16[16,2,32,2048]{3,2,0,1:T(8,128)(2,1)}), bf16[16,2,32,2048]{3,2,0,1:T(8,128)(2,1)}) %all-reduce.3.cloned.1.call-update) | async-done | bytes 4194320
  272.0 1.3 constant_dynamic-slice_fusion
  273.3 1.1 copy.92
  274.4 4.6 %all-to-all-start.1 = ((bf16[4,2,32,2048]{3,2,1,0:T(8,128)(2,1)}), bf16[4,2,32,2048]{3,2,1,0:T(8,128)(2,1)S(1)}, u32[]{:S(2)}, u32[]{:S(2)}) async-start(bf16[4,2,32,2048]{3,2,1,0:T(8,128)(2,1)} %copy.92), calls=%async_computation.2 | async-start | bytes 2097152 | tf_op jit(solution)/shard_map/all_to_all | solution.py:223
  279.0 25.4 %all-to-all-done.1 = bf16[4,2,32,2048]{3,2,1,0:T(8,128)(2,1)S(1)} async-done(((bf16[4,2,32,2048]{3,2,1,0:T(8,128)(2,1)}), bf16[4,2,32,2048]{3,2,1,0:T(8,128)(2,1)S(1)}, u32[]{:S(2)}, u32[]{:S(2)}) %all-to-all-start.1) | async-done | bytes 1048608 | tf_op jit(solution)/shard_map/all_to_all | solution.py:223
  304.4 0.3 fusion.26
  304.7 1.7 fusion.51
  (52 shorter events, 0.4 us)
Async XLA Ops:
  6.5 172.5 %copy-start = (bf16[2,256,2048]{2,1,0:T(8,128)(2,1)S(1)}, bf16[2,256,2048]{2,1,0:T(8,128)(2,1)}, u32[]{:S(2)}) copy-start(bf16[2,256,2048]{2,1,0:T(8,128)(2,1)} %param.37) | copy-start | bytes 6291460
  6.5 20.1 %copy-start.14 = (f32[128]{0:T(128)S(1)}, f32[128]{0:T(128)}, u32[]{:S(2)}) copy-start(f32[128]{0:T(128)} %param.27) | copy-start | bytes 1540
  6.5 102.0 %reduce-scatter.5.cloned.1.call-start = ((), (), s32[]{:S(2)}) async-start(), calls=%async_computation.3 | async-start | bytes 1310720 | tf_op jit(solution)/shard_map/reduce_scatter | solution.py:168
  27.1 2.4 copy-start.9
  27.1 17.1 %copy-start.10 = (bf16[256,128]{1,0:T(8,128)(2,1)S(1)}, bf16[256,128]{1,0:T(8,128)(2,1)}, u32[]{:S(2)}) copy-start(bf16[256,128]{1,0:T(8,128)(2,1)} %param.20) | copy-start | bytes 196612
  27.7 1.3 copy-start.2
  27.7 16.6 %copy-start.15 = (f32[64]{0:T(128)S(1)}, f32[64]{0:T(128)}, u32[]{:S(2)}) copy-start(f32[64]{0:T(128)} %param.26) | copy-start | bytes 772
  27.7 30.6 %copy-start.7 = (bf16[256,256]{1,0:T(8,128)(2,1)S(1)}, bf16[256,256]{1,0:T(8,128)(2,1)}, u32[]{:S(2)}) copy-start(bf16[256,256]{1,0:T(8,128)(2,1)} %param.19) | copy-start | bytes 393220
  27.7 30.7 %copy-start.16 = (f32[64]{0:T(128)S(1)}, f32[64]{0:T(128)}, u32[]{:S(2)}) copy-start(f32[64]{0:T(128)} %param.25) | copy-start | bytes 772
  59.4 1.9 copy-start.1
  59.4 1.9 copy-start.8
  75.3 3.1 copy-start.5
  78.4 1.6 copy-start.3
  78.9 1.6 copy-start.6
  80.5 1.6 copy-start.12
  80.5 28.0 %copy-start.4 = (bf16[64,2048]{1,0:T(8,128)(2,1)S(1)}, bf16[64,2048]{1,0:T(8,128)(2,1)}, u32[]{:S(2)}) copy-start(bf16[64,2048]{1,0:T(8,128)(2,1)} %param.29) | copy-start | bytes 786436
  80.5 29.1 %copy-start.11 = (f32[2048]{0:T(1024)S(1)}, f32[2048]{0:T(1024)}, u32[]{:S(2)}) copy-start(f32[2048]{0:T(1024)} %param.32) | copy-start | bytes 24580
  82.0 92.9 %all-gather.2.cloned.1.call-start = ((), (), s32[]{:S(2)}) async-start(), calls=%async_computation.4 | async-start | bytes 5242880 | tf_op jit(solution)/shard_map/all_gather | solution.py:204
  142.1 129.9 %all-reduce.3.cloned.1.call-start = ((), (), s32[]{:S(2)}) async-start(), calls=%async_computation.5 | async-start | bytes 8388608
  186.3 0.7 copy-start.17
  273.3 5.7 %copy-start.13 = (f32[64,2]{0,1:T(2,128)S(1)}, f32[64,2]{0,1:T(2,128)}, u32[]{:S(2)}) copy-start(f32[64,2]{0,1:T(2,128)} %param.34) | copy-start | bytes 1540
  274.4 30.0 %all-to-all-start.1 = ((bf16[4,2,32,2048]{3,2,1,0:T(8,128)(2,1)}), bf16[4,2,32,2048]{3,2,1,0:T(8,128)(2,1)S(1)}, u32[]{:S(2)}, u32[]{:S(2)}) async-start(bf16[4,2,32,2048]{3,2,1,0:T(8,128)(2,1)} %copy.92), calls=%async_computation.2 | async-start | bytes 2097152 | tf_op jit(solution)/shard_map/all_to_all | solution.py:223
Sparse Core Ops, SparseCore 0:
  82.1 26.3 reduce-scatter.4
  142.3 32.5 all-gather.1
  186.5 85.4 all-reduce.2
where the time goes:
time: 313 us
  waiting for transfers between devices  167 us (53%)
  blocking collectives  87.7 us (28%)
  matrix products  20.1 us (6%)
  between operations  14.3 us (5%)
  local copies, waits for them, and re-layouts  11.3 us (4%)
  other arithmetic  7.66 us (2%)
  starting transfers between devices  4.86 us (2%)
    unnamed x4, waiting for transfers between devices  83.8 us
    all_gather x1, waiting for transfers between devices, on_device(): lax.all_gather(lax.all_to_all(outgoing, 'sp', split_axis=0, concat_axis=0...  32.5 us
    all_to_all x1, blocking collectives, on_device(): lax.all_to_all(outgoing, 'sp', split_axis=0, concat_axis=0, tiled=True)  30 us
    reduce_scatter x1, waiting for transfers between devices, on_device(): lax.psum_scatter((jnp.dot(heard_small, out_weight_small, preferred_elemen...  25.4 us
    all_to_all x1, waiting for transfers between devices, on_device(): lax.all_to_all(summed, 'sp', split_axis=0, concat_axis=0, tiled=True)  25.4 us
    all_gather x1, blocking collectives, on_device(): key_large = lax.all_gather(turned_large, 'sp', axis=0, tiled=True)  15.7 us
    all_gather x1, blocking collectives, on_device(): value_large = lax.all_gather(values_large, 'sp', axis=0, tiled=True)  14.4 us
    all_gather x1, blocking collectives, on_device(): key_small = lax.all_gather(turned_small, 'sp', axis=0, tiled=True)  13.8 us
  transfers between devices with their start and end apart: 4, of which 4 were waited for; matrix products, arithmetic and copies ran while one was open for 1% of the time, Pallas kernels for 0%

commit v1 on v0

--- a/solution.py
+++ b/solution.py
@@ -118,7 +118,7 @@
     return merged.reshape(merged.shape[0], -1).astype(jnp.bfloat16)
 
 
-def on_device(
+def dispatch_plan(
     queries_small,
     keys_small,
     values_small,
@@ -230,6 +230,204 @@
     return (attended.astype(jnp.float32) + mixed).astype(jnp.bfloat16)
 
 
+def swap(values, axis, flip):
+    size = lax.axis_size(axis)
+    return lax.ppermute(values, axis, [(place, place ^ flip) for place in range(size)])
+
+
+def shift(values, axis, step):
+    size = lax.axis_size(axis)
+    return lax.ppermute(values, axis, [(place, (place + step) % size) for place in range(size)])
+
+
+def flips(axis):
+    size = lax.axis_size(axis)
+    return [1 << bit for bit in range(size.bit_length() - 1)]
+
+
+def gather_near(rows, axis, along=0):
+    for flip in reversed(flips(axis)):
+        rows = jnp.concatenate([rows, swap(rows, axis, flip)], axis=along)
+    return rows
+
+
+def add_near(rows, axis):
+    for flip in flips(axis):
+        kept = rows.shape[0] // 2
+        arrived = swap(rows[kept:], axis, flip)
+        rows = (rows[:kept].astype(jnp.float32) + arrived.astype(jnp.float32)).astype(jnp.bfloat16)
+    return rows
+
+
+def near_order(axis):
+    order = [0]
+    for flip in reversed(flips(axis)):
+        order = order + [place ^ flip for place in order]
+    return order
+
+
+def attend_pieces(queries, key_pieces, value_pieces):
+    head_size = queries.shape[-1]
+    kv_local = queries.shape[1]
+    scores = [
+        jnp.einsum(
+            "qgrd,kgd->grqk",
+            queries,
+            piece.reshape(piece.shape[0], kv_local, head_size),
+            preferred_element_type=jnp.float32,
+        )
+        * head_size ** (-0.5)
+        for piece in key_pieces
+    ]
+    scores = jnp.concatenate(scores, axis=-1)
+    values = jnp.concatenate(value_pieces, axis=0)
+    peak = jnp.max(scores, axis=-1, keepdims=True)
+    weights = jnp.exp(scores - peak)
+    total = jnp.sum(weights, axis=-1)
+    heard = jnp.einsum(
+        "grqk,kgd->qgrd",
+        weights.astype(jnp.bfloat16),
+        values.reshape(values.shape[0], kv_local, head_size),
+        preferred_element_type=jnp.float32,
+    )
+    heard = heard / jnp.transpose(total, (2, 0, 1))[..., None]
+    return heard.reshape(heard.shape[0], -1).astype(jnp.bfloat16)
+
+
+def gather_plan(
+    queries_small,
+    keys_small,
+    values_small,
+    queries_large,
+    keys_large,
+    values_large,
+    query_gain_small,
+    key_gain_small,
+    query_gain_large,
+    key_gain_large,
+    residual_in,
+    out_weight_small,
+    out_weight_large,
+    norm_gain,
+    routes,
+    route_scores,
+    expert_gate,
+    expert_up,
+    expert_down,
+):
+    token_rows = queries_small.shape[0]
+    local_rows = routes.shape[0]
+    sp_count = lax.axis_size("sp")
+    sp_index = lax.axis_index("sp")
+    tp_index = lax.axis_index("tp")
+    local_experts = expert_gate.shape[0]
+    steps = list(range(sp_count))
+    offset = sp_index * token_rows
+    tables_small = grid_tables(offset, token_rows, HS_SMALL)
+    tables_large = grid_tables(offset, token_rows, HS_LARGE)
+    kv_small = keys_small.shape[1] // HS_SMALL
+    kv_large = keys_large.shape[1] // HS_LARGE
+    turned_small = normed_turn(
+        keys_small.reshape(token_rows, kv_small, HS_SMALL), key_gain_small, tables_small
+    ).reshape(token_rows, -1)
+    turned_large = normed_turn(
+        keys_large.reshape(token_rows, kv_large, HS_LARGE), key_gain_large, tables_large
+    ).reshape(token_rows, -1)
+    memory = jnp.concatenate([turned_small, values_small, turned_large, values_large], axis=1)
+    memories = [memory] + [shift(memory, "sp", step) for step in steps[1:]]
+    cuts = [keys_small.shape[1], values_small.shape[1], keys_large.shape[1]]
+    ends = [sum(cuts[: place + 1]) for place in range(3)]
+    pieces = [jnp.split(rows, ends, axis=1) for rows in memories]
+
+    shares = route_scores / jnp.sum(route_scores, axis=1, keepdims=True)
+    experts = jnp.arange(local_experts * sp_count, dtype=jnp.int32)
+    named = (routes[:, :, None] == experts).astype(jnp.float32)
+    mixing = jnp.sum(named * shares[:, :, None], axis=1).T
+    mixing = gather_near(mixing, "tp", along=1)
+    mixings = [mixing] + [shift(mixing, "sp", step) for step in steps[1:]]
+    mixings = [
+        lax.dynamic_slice_in_dim(block, sp_index * local_experts, local_experts, 0)
+        for block in mixings
+    ]
+
+    order = near_order("tp")
+
+    def reorder(rows):
+        return jnp.concatenate(
+            [
+                lax.dynamic_slice_in_dim(rows, (tp_index ^ place) * local_rows, local_rows, 0)
+                for place in order
+            ],
+            axis=0,
+        )
+
+    asked_small = reorder(
+        normed_turn(
+            queries_small.reshape(token_rows, -1, HS_SMALL), query_gain_small, tables_small
+        ).reshape(token_rows, -1)
+    ).reshape(token_rows, kv_small, -1, HS_SMALL)
+    asked_large = reorder(
+        normed_turn(
+            queries_large.reshape(token_rows, -1, HS_LARGE), query_gain_large, tables_large
+        ).reshape(token_rows, -1)
+    ).reshape(token_rows, kv_large, -1, HS_LARGE)
+    heard_small = attend_pieces(asked_small, [p[0] for p in pieces], [p[1] for p in pieces])
+    heard_large = attend_pieces(asked_large, [p[2] for p in pieces], [p[3] for p in pieces])
+    terms = (
+        jnp.dot(heard_small, out_weight_small, preferred_element_type=jnp.float32)
+        + jnp.dot(heard_large, out_weight_large, preferred_element_type=jnp.float32)
+    ).astype(jnp.bfloat16)
+    for flip in flips("tp"):
+        kept = terms.shape[0] // 2
+        arrived = swap(terms[kept:], "tp", flip)
+        terms = terms[:kept].astype(jnp.float32) + arrived.astype(jnp.float32)
+        if kept > local_rows:
+            terms = terms.astype(jnp.bfloat16)
+    attended = (residual_in.astype(jnp.float32) + terms).astype(jnp.bfloat16)
+    widened = attended.astype(jnp.float32)
+    normed = (
+        widened
+        * lax.rsqrt(jnp.mean(widened * widened, axis=-1, keepdims=True) + norm_eps)
+        * norm_gain
+    ).astype(jnp.bfloat16)
+
+    arrivals = [normed] + [shift(normed, "sp", step) for step in steps[1:]]
+    total = attended.astype(jnp.float32)
+    for step in steps:
+        rows = gather_near(arrivals[step], "tp")
+        actives = []
+        for place in range(local_experts):
+            gate_out = jnp.dot(rows, expert_gate[place], preferred_element_type=jnp.float32)
+            up_out = jnp.dot(rows, expert_up[place], preferred_element_type=jnp.float32)
+            actives.append(
+                (jax.nn.silu(gate_out) * up_out * mixings[step][place][:, None]).astype(
+                    jnp.bfloat16
+                )
+            )
+        down = expert_down.reshape(-1, expert_down.shape[2])
+        partial = jnp.dot(
+            jnp.concatenate(actives, axis=1), down, preferred_element_type=jnp.float32
+        ).astype(jnp.bfloat16)
+        summed = add_near(partial, "tp")
+        if step:
+            summed = shift(summed, "sp", -step)
+        total = total + summed.astype(jnp.float32)
+    return total.astype(jnp.bfloat16)
+
+
+def on_device(*arrays):
+    routes, expert_gate = arrays[14], arrays[16]
+    devices = lax.axis_size("sp") * lax.axis_size("tp")
+    tokens = routes.shape[0] * devices
+    expert_count = expert_gate.shape[0] * lax.axis_size("sp")
+    capacity = max(2, (2 * routes.size + expert_count - 1) // expert_count)
+    slots = devices * expert_gate.shape[0] * capacity
+    tp_size = lax.axis_size("tp")
+    if tokens <= slots and tp_size & (tp_size - 1) == 0:
+        return gather_plan(*arrays)
+    return dispatch_plan(*arrays)
+
+
 def solution(mesh):
     in_specs = (
         P(("grp", "sp"), "tp"),

time: 313 us -> 159 us (0.51)
  waiting for transfers between devices: 167 us -> 62.2 us
  blocking collectives: 87.7 us -> 0 us
  starting transfers between devices: 4.86 us -> 43.1 us
  between operations: 14.3 us -> 1.13 us
  other arithmetic: 7.66 us -> 14 us
  local copies, waits for them, and re-layouts: 11.3 us -> 15 us
    unnamed x4 -> x0, waiting for transfers between devices: 83.8 us -> none
    ppermute x0 -> x32, waiting for transfers between devices: none -> 62.2 us  [the longest x12 34.1 us: shift(): lax.ppermute(values, axis, [(place, (place + step) % size) for place in r...]
    all_gather x4 -> x0, blocking collectives: 57.7 us -> none  [the longest x1 15.7 us: on_device(): key_large = lax.all_gather(turned_large, 'sp', axis=0, tiled=True)]
    ppermute x0 -> x32, starting transfers between devices: none -> 43.1 us  [the longest x12 30.9 us: shift(): lax.ppermute(values, axis, [(place, (place + step) % size) for place in r...]
    all_gather x1 -> x0, waiting for transfers between devices: 32.5 us -> none  [on_device(): lax.all_gather(lax.all_to_all(outgoing, 'sp', split_axis=0, concat_axis=0...]
    all_to_all x1 -> x0, blocking collectives: 30 us -> none  [on_device(): lax.all_to_all(outgoing, 'sp', split_axis=0, concat_axis=0, tiled=True)]
    reduce_scatter x1 -> x0, waiting for transfers between devices: 25.4 us -> none  [on_device(): lax.psum_scatter((jnp.dot(heard_small, out_weight_small, preferred_elemen...]
    all_to_all x1 -> x0, waiting for transfers between devices: 25.4 us -> none  [on_device(): lax.all_to_all(summed, 'sp', split_axis=0, concat_axis=0, tiled=True)]
  transfers between devices with their start and end apart: 4 -> 32, of which waited for: 4 -> 12; matrix products, arithmetic and copies ran while one was open for 1% -> 18% of each run, Pallas kernels for 0% -> 0%
where the time goes in v1:
time: 159 us; the launch traced here: 158 us
  waiting for transfers between devices  62.2 us (39%)
  starting transfers between devices  43.1 us (27%)
  matrix products  22.9 us (14%)
  local copies, waits for them, and re-layouts  15 us (9%)
  other arithmetic  14 us (9%)
    ppermute x12, waiting for transfers between devices, shift(): lax.ppermute(values, axis, [(place, (place + step) % size) for place in r...  34.1 us
    ppermute x12, starting transfers between devices, shift(): lax.ppermute(values, axis, [(place, (place + step) % size) for place in r...  30.9 us
    ppermute x20, waiting for transfers between devices, swap(): lax.ppermute(values, axis, [(place, place ^ flip) for place in range(size)])  28 us
    ppermute x20, starting transfers between devices, swap(): lax.ppermute(values, axis, [(place, place ^ flip) for place in range(size)])  12.3 us
    dot_general x8, matrix products, attend_pieces(): jnp.einsum('qgrd,kgd->grqk', queries, piece.reshape(piece.shape[0], kv_lo...  9.21 us
    split x6, local copies, waits for them, and re-layouts, gather_plan(): pieces = [jnp.split(rows, ends, axis=1) for rows in memories]  5.04 us
    unnamed x60, local copies, waits for them, and re-layouts  4.9 us
    dot_general x8, matrix products, gather_plan(): up_out = jnp.dot(rows, expert_up[place], preferred_element_type=jnp.float32)  4.27 us
  transfers between devices with their start and end apart: 32, of which 12 were waited for; matrix products, arithmetic and copies ran while one was open for 18% of the time, Pallas kernels for 0%

profile of v1, /device:TPU:0, one launch (start us, length us, event | category | flops | bytes accessed | tf_op | source)
XLA Modules:
  0.0 158.3 jit_solution(17903453639597552262)
XLA Ops:
  0.1 1.1 copy.109
  1.2 0.9 copy.108
  2.2 0.7 multiply_multiply_fusion.1
  3.3 0.7 fusion.103
  4.9 0.9 concatenate.121
  5.8 3.1 %collective-permute-start = (bf16[256,512]{1,0:T(8,128)(2,1)}, bf16[256,512]{1,0:T(8,128)(2,1)}, u32[]{:S(2)}, u32[]{:S(2)}) collective-permute-start(bf16[256,512]{1,0:T(8,128)(2,1)} %concatenate.121), channel_id=1, source_target_pairs={{0,4},{4,8},{8,12},{12,0},{1,5},{5,9},{9,13},{13,1},{2,6},{6,10},{... | collective-permute-start | bytes 786440 | tf_op jit(solution)/shard_map/ppermute | solution.py:240
  8.8 2.6 %collective-permute-start.1 = (bf16[256,512]{1,0:T(8,128)(2,1)}, bf16[256,512]{1,0:T(8,128)(2,1)}, u32[]{:S(2)}, u32[]{:S(2)}) collective-permute-start(bf16[256,512]{1,0:T(8,128)(2,1)} %concatenate.121), channel_id=1, source_target_pairs={{0,8},{4,12},{8,0},{12,4},{1,9},{5,13},{9,1},{13,5},{2,10},{6,14},... | collective-permute-start | bytes 786440 | tf_op jit(solution)/shard_map/ppermute | solution.py:240
  11.4 1.3 collective-permute-start.2
  12.8 1.0 multiply_cosine_fusion.1
  14.7 0.9 subtract_convert_fusion.1
  15.6 0.8 pad_maximum_fusion.8
  16.8 1.6 %bitcast_reduce_fusion.3 = (f32[2,256]{1,0:T(2,128)}, f32[256,256,2]{1,0,2:T(8,128)}) fusion(bf16[256,2,128]{0,2,1:T(8,128)(2,1)S(1)} %bitcast.228, bf16[256,32]{0,1:T(8,128)(2,1)S(1)} %get-tuple-element.32, bf16[256,32]{0,1:T(8,128)(2,1)S(1)} %get-tuple-element.33, bf16[256,32]{0,1:T(8,128)(2,1)S(1)} %get-tuple-element.37, ...), kind=kOutput, calls=%fused_computation.267 | convolution fusion | flops 34078208 | bytes 722944 | tf_op jit(solution)/shard_map/qgrd,kgd->grqk/dot_general | solution.py:273
  19.5 1.6 fusion.146
  21.1 1.3 fusion.152
  22.5 6.4 %collective-permute-done.1 = bf16[256,512]{1,0:T(8,128)(2,1)} collective-permute-done((bf16[256,512]{1,0:T(8,128)(2,1)}, bf16[256,512]{1,0:T(8,128)(2,1)}, u32[]{:S(2)}, u32[]{:S(2)}) %collective-permute-start.1) | collective-permute-done | bytes 262176 | tf_op jit(solution)/shard_map/ppermute | solution.py:240
  28.8 1.6 fusion.147
  30.5 1.3 fusion.150
  31.9 1.6 fusion.148
  33.6 1.3 fusion.149
  34.9 1.0 pad_maximum_fusion.5
  35.8 0.9 copy.115
  36.7 2.3 %fusion.8 = f32[2,2,256]{2,1,0:T(2,128)S(1)} fusion(f32[2,2,256]{2,1,0:T(2,128)S(1)} %maximum_maximum_fusion, f32[2,2,256,256]{2,3,1,0:T(8,128)} %get-tuple-element.69, f32[2,2,256,256]{2,3,1,0:T(8,128)} %get-tuple-element.71, f32[2,2,256,256]{2,3,1,0:T(8,128)} %get-tuple-element.75, f32[2,2,256,256]{2,3,1,0:T(8,128)S(1)} %get-tuple-element.73), kind=kLoop, calls=%fused_computation.16 | loop fusion | flops 5241856 | bytes 4202496 | tf_op jit(solution)/shard_map/reduce_sum | solution.py:286
  39.5 0.8 fusion.22
  41.3 1.1 bitcast_reduce_fusion.2
  42.4 1.1 bitcast_reduce_fusion.1
  43.4 1.1 bitcast_reduce_fusion
  45.4 0.7 copy-done.7
  46.6 0.8 slice.245
  47.5 1.6 collective-permute-start.7
  49.1 0.6 collective-permute-done.3
  49.7 1.2 add_convert_fusion.4
  50.9 0.8 copy-done.4
  51.7 1.6 collective-permute-start.4
  53.4 1.1 collective-permute-done.8
  54.6 4.3 %collective-permute-start.14 = (f32[8,256]{1,0:T(8,128)S(1)}, f32[8,256]{1,0:T(8,128)S(1)}, u32[]{:S(2)}, u32[]{:S(2)}) collective-permute-start(f32[8,256]{1,0:T(8,128)S(1)} %pad_maximum_fusion.10), channel_id=1, source_target_pairs={{0,4},{4,8},{8,12},{12,0},{1,5},{5,9},{9,13},{13,1},{2,6},{6,10},{... | collective-permute-start | bytes 24584 | tf_op jit(solution)/shard_map/ppermute | solution.py:240
  58.9 3.4 %collective-permute-start.21 = (f32[8,256]{1,0:T(8,128)S(1)}, f32[8,256]{1,0:T(8,128)S(1)}, u32[]{:S(2)}, u32[]{:S(2)}) collective-permute-start(f32[8,256]{1,0:T(8,128)S(1)} %pad_maximum_fusion.10), channel_id=1, source_target_pairs={{0,8},{4,12},{8,0},{12,4},{1,9},{5,13},{9,1},{13,5},{2,10},{6,14},... | collective-permute-start | bytes 24584 | tf_op jit(solution)/shard_map/ppermute | solution.py:240
  62.3 1.2 fusion.74
  63.6 0.6 collective-permute-start.5
  64.3 3.1 %collective-permute-start.11 = (bf16[64,2048]{1,0:T(8,128)(2,1)S(1)}, bf16[64,2048]{1,0:T(8,128)(2,1)S(1)}, u32[]{:S(2)}, u32[]{:S(2)}) collective-permute-start(bf16[64,2048]{1,0:T(8,128)(2,1)S(1)} %fusion.76), channel_id=1, source_target_pairs={{0,4},{4,8},{8,12},{12,0},{1,5},{5,9},{9,13},{13,1},{2,6},{6,10},{... | collective-permute-start | bytes 786440 | tf_op jit(solution)/shard_map/ppermute | solution.py:240
  67.4 3.4 %collective-permute-start.18 = (bf16[64,2048]{1,0:T(8,128)(2,1)S(1)}, bf16[64,2048]{1,0:T(8,128)(2,1)S(1)}, u32[]{:S(2)}, u32[]{:S(2)}) collective-permute-start(bf16[64,2048]{1,0:T(8,128)(2,1)S(1)} %fusion.76), channel_id=1, source_target_pairs={{0,8},{4,12},{8,0},{12,4},{1,9},{5,13},{9,1},{13,5},{2,10},{6,14},... | collective-permute-start | bytes 786440 | tf_op jit(solution)/shard_map/ppermute | solution.py:240
  70.9 0.6 collective-permute-done.5
  71.7 5.9 %collective-permute-done.11 = bf16[64,2048]{1,0:T(8,128)(2,1)S(1)} collective-permute-done((bf16[64,2048]{1,0:T(8,128)(2,1)S(1)}, bf16[64,2048]{1,0:T(8,128)(2,1)S(1)}, u32[]{:S(2)}, u32[]{:S(2)}) %collective-permute-start.11) | collective-permute-done | bytes 262176 | tf_op jit(solution)/shard_map/ppermute | solution.py:240
  78.1 9.0 %collective-permute-done.18 = bf16[64,2048]{1,0:T(8,128)(2,1)S(1)} collective-permute-done((bf16[64,2048]{1,0:T(8,128)(2,1)S(1)}, bf16[64,2048]{1,0:T(8,128)(2,1)S(1)}, u32[]{:S(2)}, u32[]{:S(2)}) %collective-permute-start.18) | collective-permute-done | bytes 262176 | tf_op jit(solution)/shard_map/ppermute | solution.py:240
  87.7 1.5 collective-permute-start.26
  89.4 6.9 %collective-permute-done.19 = bf16[64,2048]{1,0:T(8,128)(2,1)S(1)} collective-permute-done((bf16[64,2048]{1,0:T(8,128)(2,1)S(1)}, bf16[64,2048]{1,0:T(8,128)(2,1)S(1)}, u32[]{:S(2)}, u32[]{:S(2)}) %collective-permute-start.19) | collective-permute-done | bytes 262176 | tf_op jit(solution)/shard_map/ppermute | solution.py:235
  96.4 4.5 %collective-permute-done.26 = bf16[64,2048]{1,0:T(8,128)(2,1)S(1)} collective-permute-done((bf16[64,2048]{1,0:T(8,128)(2,1)S(1)}, bf16[64,2048]{1,0:T(8,128)(2,1)S(1)}, u32[]{:S(2)}, u32[]{:S(2)}) %collective-permute-start.26) | collective-permute-done | bytes 262176 | tf_op jit(solution)/shard_map/ppermute | solution.py:235
  102.1 1.0 copy-done.25
  104.3 0.7 convolution_convert_fusion.3
  105.1 0.6 collective-permute-start.9
  110.1 0.7 convolution_convert_fusion.2
  112.1 0.7 convolution_convert_fusion.1
  114.5 0.7 convolution_convert_fusion
  115.5 0.6 collective-permute-start.10
  116.3 1.5 collective-permute-start.16
  118.0 0.6 collective-permute-start.23
  118.8 1.5 collective-permute-start.30
  120.4 10.1 %collective-permute-done.16 = bf16[64,2048]{1,0:T(8,128)(2,1)S(1)} collective-permute-done((bf16[64,2048]{1,0:T(8,128)(2,1)S(1)}, bf16[64,2048]{1,0:T(8,128)(2,1)S(1)}, u32[]{:S(2)}, u32[]{:S(2)}) %collective-permute-start.16) | collective-permute-done | bytes 262176 | tf_op jit(solution)/shard_map/ppermute | solution.py:235
  130.5 4.0 %collective-permute-start.17 = (bf16[64,2048]{1,0:T(8,128)(2,1)S(1)}, bf16[64,2048]{1,0:T(8,128)(2,1)S(1)}, u32[]{:S(2)}, u32[]{:S(2)}) collective-permute-start(bf16[64,2048]{1,0:T(8,128)(2,1)S(1)} %add_convert_fusion.7), channel_id=1, source_target_pairs={{0,12},{4,0},{8,4},{12,8},{1,13},{5,1},{9,5},{13,9},{2,14},{6,2},{... | collective-permute-start | bytes 786440 | tf_op jit(solution)/shard_map/ppermute | solution.py:240
  134.5 1.5 collective-permute-done.23
  136.1 2.4 %collective-permute-start.24 = (bf16[64,2048]{1,0:T(8,128)(2,1)S(1)}, bf16[64,2048]{1,0:T(8,128)(2,1)S(1)}, u32[]{:S(2)}, u32[]{:S(2)}) collective-permute-start(bf16[64,2048]{1,0:T(8,128)(2,1)S(1)} %add_convert_fusion.6), channel_id=1, source_target_pairs={{0,8},{4,12},{8,0},{12,4},{1,9},{5,13},{9,1},{13,5},{2,10},{6,14},... | collective-permute-start | bytes 786440 | tf_op jit(solution)/shard_map/ppermute | solution.py:240
  138.5 2.7 %collective-permute-done.30 = bf16[64,2048]{1,0:T(8,128)(2,1)S(1)} collective-permute-done((bf16[64,2048]{1,0:T(8,128)(2,1)S(1)}, bf16[64,2048]{1,0:T(8,128)(2,1)S(1)}, u32[]{:S(2)}, u32[]{:S(2)}) %collective-permute-start.30) | collective-permute-done | bytes 262176 | tf_op jit(solution)/shard_map/ppermute | solution.py:235
  141.2 3.2 %collective-permute-start.31 = (bf16[64,2048]{1,0:T(8,128)(2,1)S(1)}, bf16[64,2048]{1,0:T(8,128)(2,1)S(1)}, u32[]{:S(2)}, u32[]{:S(2)}) collective-permute-start(bf16[64,2048]{1,0:T(8,128)(2,1)S(1)} %add_convert_fusion.5), channel_id=1, source_target_pairs={{0,4},{4,8},{8,12},{12,0},{1,5},{5,9},{9,13},{13,1},{2,6},{6,10},{... | collective-permute-start | bytes 786440 | tf_op jit(solution)/shard_map/ppermute | solution.py:240
  144.4 12.9 %collective-permute-done.24 = bf16[64,2048]{1,0:T(8,128)(2,1)S(1)} collective-permute-done((bf16[64,2048]{1,0:T(8,128)(2,1)S(1)}, bf16[64,2048]{1,0:T(8,128)(2,1)S(1)}, u32[]{:S(2)}, u32[]{:S(2)}) %collective-permute-start.24) | collective-permute-done | bytes 262176 | tf_op jit(solution)/shard_map/ppermute | solution.py:240
  157.3 0.9 fusion.80
  (179 shorter events, 18.9 us)
Async XLA Ops:
  0.0 104.3 %copy-start = (bf16[2,256,2048]{2,1,0:T(8,128)(2,1)S(1)}, bf16[2,256,2048]{2,1,0:T(8,128)(2,1)}, u32[]{:S(2)}) copy-start(bf16[2,256,2048]{2,1,0:T(8,128)(2,1)} %param.37) | copy-start | bytes 6291460
  0.0 4.9 %copy-start.10 = (bf16[256,128]{1,0:T(8,128)(2,1)S(1)}, bf16[256,128]{1,0:T(8,128)(2,1)}, u32[]{:S(2)}) copy-start(bf16[256,128]{1,0:T(8,128)(2,1)} %param.21) | copy-start | bytes 196612
  0.0 4.9 %copy-start.16 = (bf16[256,128]{1,0:T(8,128)(2,1)S(1)}, bf16[256,128]{1,0:T(8,128)(2,1)}, u32[]{:S(2)}) copy-start(bf16[256,128]{1,0:T(8,128)(2,1)} %param.24) | copy-start | bytes 196612
  0.0 13.8 %copy-start.11 = (bf16[256,256]{1,0:T(8,128)(2,1)S(1)}, bf16[256,256]{1,0:T(8,128)(2,1)}, u32[]{:S(2)}) copy-start(bf16[256,256]{1,0:T(8,128)(2,1)} %param.22) | copy-start | bytes 393220
  1.2 13.1 %copy-start.23 = (f32[128]{0:T(128)S(1)}, f32[128]{0:T(128)}, u32[]{:S(2)}) copy-start(f32[128]{0:T(128)} %param.27) | copy-start | bytes 1540
  5.8 13.7 %collective-permute-start = (bf16[256,512]{1,0:T(8,128)(2,1)}, bf16[256,512]{1,0:T(8,128)(2,1)}, u32[]{:S(2)}, u32[]{:S(2)}) collective-permute-start(bf16[256,512]{1,0:T(8,128)(2,1)} %concatenate.121), channel_id=1, source_target_pairs={{0,4},{4,8},{8,12},{12,0},{1,5},{5,9},{9,13},{13,1},{2,6},{6,10},{... | collective-permute-start | bytes 786440 | tf_op jit(solution)/shard_map/ppermute | solution.py:240
  8.8 20.0 %collective-permute-start.1 = (bf16[256,512]{1,0:T(8,128)(2,1)}, bf16[256,512]{1,0:T(8,128)(2,1)}, u32[]{:S(2)}, u32[]{:S(2)}) collective-permute-start(bf16[256,512]{1,0:T(8,128)(2,1)} %concatenate.121), channel_id=1, source_target_pairs={{0,8},{4,12},{8,0},{12,4},{1,9},{5,13},{9,1},{13,5},{2,10},{6,14},... | collective-permute-start | bytes 786440 | tf_op jit(solution)/shard_map/ppermute | solution.py:240
  11.4 20.4 %collective-permute-start.2 = (bf16[256,512]{1,0:T(8,128)(2,1)}, bf16[256,512]{1,0:T(8,128)(2,1)}, u32[]{:S(2)}, u32[]{:S(2)}) collective-permute-start(bf16[256,512]{1,0:T(8,128)(2,1)} %concatenate.121), channel_id=1, source_target_pairs={{0,12},{4,0},{8,4},{12,8},{1,13},{5,1},{9,5},{13,9},{2,14},{6,2},{... | collective-permute-start | bytes 786440 | tf_op jit(solution)/shard_map/ppermute | solution.py:240
  14.7 3.8 %copy-start.12 = (bf16[256,256]{1,0:T(8,128)(2,1)S(1)}, bf16[256,256]{1,0:T(8,128)(2,1)}, u32[]{:S(2)}) copy-start(bf16[256,256]{1,0:T(8,128)(2,1)} %param.19) | copy-start | bytes 393220
  14.7 4.0 %copy-start.22 = (f32[64]{0:T(128)S(1)}, f32[64]{0:T(128)}, u32[]{:S(2)}) copy-start(f32[64]{0:T(128)} %param.25) | copy-start | bytes 772
  36.7 2.3 %copy-start.1 = (f32[2,2,256,256]{2,3,1,0:T(8,128)S(1)}, f32[2,2,256,256]{2,3,1,0:T(8,128)}, u32[]{:S(2)}) copy-start(f32[2,2,256,256]{2,3,1,0:T(8,128)} %get-tuple-element.75) | copy-start | bytes 3145732
  36.7 2.5 %copy-start.2 = (f32[2,2,256,256]{2,3,1,0:T(8,128)S(1)}, f32[2,2,256,256]{2,3,1,0:T(8,128)}, u32[]{:S(2)}) copy-start(f32[2,2,256,256]{2,3,1,0:T(8,128)} %get-tuple-element.71) | copy-start | bytes 3145732
  36.7 2.8 %copy-start.3 = (f32[2,2,256,256]{2,3,1,0:T(8,128)S(1)}, f32[2,2,256,256]{2,3,1,0:T(8,128)}, u32[]{:S(2)}) copy-start(f32[2,2,256,256]{2,3,1,0:T(8,128)} %get-tuple-element.69) | copy-start | bytes 3145732
  36.7 2.8 %copy-start.8 = (bf16[1024,128]{0,1:T(8,128)(2,1)S(1)}, bf16[1024,128]{0,1:T(8,128)(2,1)}, u32[]{:S(2)}) copy-start(bf16[1024,128]{0,1:T(8,128)(2,1)} %copy.115) | copy-start | bytes 786436
  39.5 1.2 copy-start.6
  40.8 3.7 %copy-start.19 = (f32[2,256]{1,0:T(2,128)S(1)}, f32[2,256]{1,0:T(2,128)}, u32[]{:S(2)}) copy-start(f32[2,256]{1,0:T(2,128)} %get-tuple-element.80) | copy-start | bytes 6148
  40.8 3.8 %copy-start.5 = (f32[256,256,2]{1,0,2:T(8,128)S(1)}, f32[256,256,2]{1,0,2:T(8,128)}, u32[]{:S(2)}) copy-start(f32[256,256,2]{1,0,2:T(8,128)} %get-tuple-element.81) | copy-start | bytes 1572868
  41.2 3.6 %copy-start.13 = (bf16[256,128]{1,0:T(8,128)(2,1)S(1)}, bf16[256,128]{1,0:T(8,128)(2,1)}, u32[]{:S(2)}) copy-start(bf16[256,128]{1,0:T(8,128)(2,1)} %get-tuple-element.15) | copy-start | bytes 196612
  41.2 3.6 %copy-start.14 = (bf16[256,128]{1,0:T(8,128)(2,1)S(1)}, bf16[256,128]{1,0:T(8,128)(2,1)}, u32[]{:S(2)}) copy-start(bf16[256,128]{1,0:T(8,128)(2,1)} %get-tuple-element.18) | copy-start | bytes 196612
  41.2 3.6 %copy-start.15 = (bf16[256,128]{1,0:T(8,128)(2,1)S(1)}, bf16[256,128]{1,0:T(8,128)(2,1)}, u32[]{:S(2)}) copy-start(bf16[256,128]{1,0:T(8,128)(2,1)} %get-tuple-element.21) | copy-start | bytes 196612
  41.3 3.6 %copy-start.17 = (bf16[256,128]{1,0:T(8,128)(2,1)S(1)}, bf16[256,128]{1,0:T(8,128)(2,1)}, u32[]{:S(2)}) copy-start(bf16[256,128]{1,0:T(8,128)(2,1)} %param.24) | copy-start | bytes 196612
  44.9 1.2 copy-start.7
  46.1 1.4 copy-start.20
  46.1 1.4 copy-start.21
  46.6 15.7 %copy-start.9 = (bf16[64,2048]{1,0:T(8,128)(2,1)S(1)}, bf16[64,2048]{1,0:T(8,128)(2,1)}, u32[]{:S(2)}) copy-start(bf16[64,2048]{1,0:T(8,128)(2,1)} %param.29) | copy-start | bytes 786436
  46.6 16.9 %copy-start.18 = (f32[2048]{0:T(1024)S(1)}, f32[2048]{0:T(1024)}, u32[]{:S(2)}) copy-start(f32[2048]{0:T(1024)} %param.32) | copy-start | bytes 24580
  47.5 2.3 %collective-permute-start.3 = (bf16[128,2048]{1,0:T(8,128)(2,1)}, bf16[128,2048]{1,0:T(8,128)(2,1)}, u32[]{:S(2)}, u32[]{:S(2)}) collective-permute-start(bf16[128,2048]{1,0:T(8,128)(2,1)} %slice.245), channel_id=1, source_target_pairs={{0,1},{1,0},{2,3},{3,2},{4,5},{5,4},{6,7},{7,6},{8,9},{9,8},{10,11... | collective-permute-start | bytes 1572872 | tf_op jit(solution)/shard_map/ppermute | solution.py:235
  47.5 5.8 %collective-permute-start.7 = (f32[8,64]{1,0:T(8,128)S(1)}, f32[8,64]{1,0:T(8,128)S(1)}, u32[]{:S(2)}, u32[]{:S(2)}) collective-permute-start(f32[8,64]{1,0:T(8,128)S(1)} %bitcast.249), channel_id=1, source_target_pairs={{0,2},{1,3},{2,0},{3,1},{4,6},{5,7},{6,4},{7,5},{8,10},{9,11},{10,... | collective-permute-start | bytes 6152 | tf_op jit(solution)/shard_map/ppermute | solution.py:235
  50.9 0.8 copy-start.4
  51.7 10.6 %collective-permute-start.4 = (bf16[64,2048]{1,0:T(8,128)(2,1)S(1)}, bf16[64,2048]{1,0:T(8,128)(2,1)S(1)}, u32[]{:S(2)}, u32[]{:S(2)}) collective-permute-start(bf16[64,2048]{1,0:T(8,128)(2,1)S(1)} %slice.247), channel_id=1, source_target_pairs={{0,2},{1,3},{2,0},{3,1},{4,6},{5,7},{6,4},{7,5},{8,10},{9,11},{10,... | collective-permute-start | bytes 786440 | tf_op jit(solution)/shard_map/ppermute | solution.py:235
  53.4 1.2 collective-permute-start.8
  54.6 9.7 %collective-permute-start.14 = (f32[8,256]{1,0:T(8,128)S(1)}, f32[8,256]{1,0:T(8,128)S(1)}, u32[]{:S(2)}, u32[]{:S(2)}) collective-permute-start(f32[8,256]{1,0:T(8,128)S(1)} %pad_maximum_fusion.10), channel_id=1, source_target_pairs={{0,4},{4,8},{8,12},{12,0},{1,5},{5,9},{9,13},{13,1},{2,6},{6,10},{... | collective-permute-start | bytes 24584 | tf_op jit(solution)/shard_map/ppermute | solution.py:240
  58.9 5.4 %collective-permute-start.21 = (f32[8,256]{1,0:T(8,128)S(1)}, f32[8,256]{1,0:T(8,128)S(1)}, u32[]{:S(2)}, u32[]{:S(2)}) collective-permute-start(f32[8,256]{1,0:T(8,128)S(1)} %pad_maximum_fusion.10), channel_id=1, source_target_pairs={{0,8},{4,12},{8,0},{12,4},{1,9},{5,13},{9,1},{13,5},{2,10},{6,14},... | collective-permute-start | bytes 24584 | tf_op jit(solution)/shard_map/ppermute | solution.py:240
  62.3 5.2 %collective-permute-start.28 = (f32[8,256]{1,0:T(8,128)S(1)}, f32[8,256]{1,0:T(8,128)S(1)}, u32[]{:S(2)}, u32[]{:S(2)}) collective-permute-start(f32[8,256]{1,0:T(8,128)S(1)} %pad_maximum_fusion.10), channel_id=1, source_target_pairs={{0,12},{4,0},{8,4},{12,8},{1,13},{5,1},{9,5},{13,9},{2,14},{6,2},{... | collective-permute-start | bytes 24584 | tf_op jit(solution)/shard_map/ppermute | solution.py:240
  63.6 7.9 %collective-permute-start.5 = (bf16[64,2048]{1,0:T(8,128)(2,1)S(1)}, bf16[64,2048]{1,0:T(8,128)(2,1)S(1)}, u32[]{:S(2)}, u32[]{:S(2)}) collective-permute-start(bf16[64,2048]{1,0:T(8,128)(2,1)S(1)} %fusion.76), channel_id=1, source_target_pairs={{0,2},{1,3},{2,0},{3,1},{4,6},{5,7},{6,4},{7,5},{8,10},{9,11},{10,... | collective-permute-start | bytes 786440 | tf_op jit(solution)/shard_map/ppermute | solution.py:235
  64.3 13.2 %collective-permute-start.11 = (bf16[64,2048]{1,0:T(8,128)(2,1)S(1)}, bf16[64,2048]{1,0:T(8,128)(2,1)S(1)}, u32[]{:S(2)}, u32[]{:S(2)}) collective-permute-start(bf16[64,2048]{1,0:T(8,128)(2,1)S(1)} %fusion.76), channel_id=1, source_target_pairs={{0,4},{4,8},{8,12},{12,0},{1,5},{5,9},{9,13},{13,1},{2,6},{6,10},{... | collective-permute-start | bytes 786440 | tf_op jit(solution)/shard_map/ppermute | solution.py:240
  67.4 19.6 %collective-permute-start.18 = (bf16[64,2048]{1,0:T(8,128)(2,1)S(1)}, bf16[64,2048]{1,0:T(8,128)(2,1)S(1)}, u32[]{:S(2)}, u32[]{:S(2)}) collective-permute-start(bf16[64,2048]{1,0:T(8,128)(2,1)S(1)} %fusion.76), channel_id=1, source_target_pairs={{0,8},{4,12},{8,0},{12,4},{1,9},{5,13},{9,1},{13,5},{2,10},{6,14},... | collective-permute-start | bytes 786440 | tf_op jit(solution)/shard_map/ppermute | solution.py:240
  70.9 16.8 %collective-permute-start.25 = (bf16[64,2048]{1,0:T(8,128)(2,1)S(1)}, bf16[64,2048]{1,0:T(8,128)(2,1)S(1)}, u32[]{:S(2)}, u32[]{:S(2)}) collective-permute-start(bf16[64,2048]{1,0:T(8,128)(2,1)S(1)} %fusion.76), channel_id=1, source_target_pairs={{0,12},{4,0},{8,4},{12,8},{1,13},{5,1},{9,5},{13,9},{2,14},{6,2},{... | collective-permute-start | bytes 786440 | tf_op jit(solution)/shard_map/ppermute | solution.py:240
  71.6 29.5 %collective-permute-start.6 = (bf16[128,2048]{1,0:T(8,128)(2,1)S(1)}, bf16[128,2048]{1,0:T(8,128)(2,1)S(1)}, u32[]{:S(2)}, u32[]{:S(2)}) collective-permute-start(bf16[128,2048]{1,0:T(8,128)(2,1)S(1)} %pad_maximum_fusion.1), channel_id=1, source_target_pairs={{0,1},{1,0},{2,3},{3,2},{4,5},{5,4},{6,7},{7,6},{8,9},{9,8},{10,11... | collective-permute-start | bytes 1572872 | tf_op jit(solution)/shard_map/ppermute | solution.py:235
  77.5 11.7 %collective-permute-start.12 = (bf16[64,2048]{1,0:T(8,128)(2,1)S(1)}, bf16[64,2048]{1,0:T(8,128)(2,1)S(1)}, u32[]{:S(2)}, u32[]{:S(2)}) collective-permute-start(bf16[64,2048]{1,0:T(8,128)(2,1)S(1)} %collective-permute-done.11), channel_id=1, source_target_pairs={{0,2},{1,3},{2,0},{3,1},{4,6},{5,7},{6,4},{7,5},{8,10},{9,11},{10,... | collective-permute-start | bytes 786440 | tf_op jit(solution)/shard_map/ppermute | solution.py:235
  87.1 9.2 %collective-permute-start.19 = (bf16[64,2048]{1,0:T(8,128)(2,1)S(1)}, bf16[64,2048]{1,0:T(8,128)(2,1)S(1)}, u32[]{:S(2)}, u32[]{:S(2)}) collective-permute-start(bf16[64,2048]{1,0:T(8,128)(2,1)S(1)} %collective-permute-done.18), channel_id=1, source_target_pairs={{0,2},{1,3},{2,0},{3,1},{4,6},{5,7},{6,4},{7,5},{8,10},{9,11},{10,... | collective-permute-start | bytes 786440 | tf_op jit(solution)/shard_map/ppermute | solution.py:235
  87.7 13.2 %collective-permute-start.26 = (bf16[64,2048]{1,0:T(8,128)(2,1)S(1)}, bf16[64,2048]{1,0:T(8,128)(2,1)S(1)}, u32[]{:S(2)}, u32[]{:S(2)}) collective-permute-start(bf16[64,2048]{1,0:T(8,128)(2,1)S(1)} %collective-permute-done.25), channel_id=1, source_target_pairs={{0,2},{1,3},{2,0},{3,1},{4,6},{5,7},{6,4},{7,5},{8,10},{9,11},{10,... | collective-permute-start | bytes 786440 | tf_op jit(solution)/shard_map/ppermute | solution.py:235
  89.3 11.8 %copy-start.24 = (bf16[2,2048,256]{2,1,0:T(8,128)(2,1)S(1)}, bf16[2,2048,256]{2,1,0:T(8,128)(2,1)}, u32[]{:S(2)}) copy-start(bf16[2,2048,256]{2,1,0:T(8,128)(2,1)} %param.35) | copy-start | bytes 6291460
  89.3 16.3 %collective-permute-start.13 = (bf16[128,2048]{1,0:T(8,128)(2,1)S(1)}, bf16[128,2048]{1,0:T(8,128)(2,1)S(1)}, u32[]{:S(2)}, u32[]{:S(2)}) collective-permute-start(bf16[128,2048]{1,0:T(8,128)(2,1)S(1)} %pad_maximum_fusion.2), channel_id=1, source_target_pairs={{0,1},{1,0},{2,3},{3,2},{4,5},{5,4},{6,7},{7,6},{8,9},{9,8},{10,11... | collective-permute-start | bytes 1572872 | tf_op jit(solution)/shard_map/ppermute | solution.py:235
  96.3 10.5 %collective-permute-start.20 = (bf16[128,2048]{1,0:T(8,128)(2,1)S(1)}, bf16[128,2048]{1,0:T(8,128)(2,1)S(1)}, u32[]{:S(2)}, u32[]{:S(2)}) collective-permute-start(bf16[128,2048]{1,0:T(8,128)(2,1)S(1)} %pad_maximum_fusion.3), channel_id=1, source_target_pairs={{0,1},{1,0},{2,3},{3,2},{4,5},{5,4},{6,7},{7,6},{8,9},{9,8},{10,11... | collective-permute-start | bytes 1572872 | tf_op jit(solution)/shard_map/ppermute | solution.py:235
  100.9 7.0 %collective-permute-start.27 = (bf16[128,2048]{1,0:T(8,128)(2,1)S(1)}, bf16[128,2048]{1,0:T(8,128)(2,1)S(1)}, u32[]{:S(2)}, u32[]{:S(2)}) collective-permute-start(bf16[128,2048]{1,0:T(8,128)(2,1)S(1)} %pad_maximum_fusion.4), channel_id=1, source_target_pairs={{0,1},{1,0},{2,3},{3,2},{4,5},{5,4},{6,7},{7,6},{8,9},{9,8},{10,11... | collective-permute-start | bytes 1572872 | tf_op jit(solution)/shard_map/ppermute | solution.py:235
  101.6 1.6 %copy-start.25 = (bf16[2,2048,256]{2,1,0:T(8,128)(2,1)S(1)}, bf16[2,2048,256]{2,1,0:T(8,128)(2,1)}, u32[]{:S(2)}) copy-start(bf16[2,2048,256]{2,1,0:T(8,128)(2,1)} %param.36) | copy-start | bytes 6291460
  105.1 10.3 %collective-permute-start.9 = (bf16[128,2048]{1,0:T(8,128)(2,1)S(1)}, bf16[128,2048]{1,0:T(8,128)(2,1)S(1)}, u32[]{:S(2)}, u32[]{:S(2)}) collective-permute-start(bf16[128,2048]{1,0:T(8,128)(2,1)S(1)} %slice.249), channel_id=1, source_target_pairs={{0,1},{1,0},{2,3},{3,2},{4,5},{5,4},{6,7},{7,6},{8,9},{9,8},{10,11... | collective-permute-start | bytes 1572872 | tf_op jit(solution)/shard_map/ppermute | solution.py:235
  110.9 5.3 %collective-permute-start.15 = (bf16[128,2048]{1,0:T(8,128)(2,1)S(1)}, bf16[128,2048]{1,0:T(8,128)(2,1)S(1)}, u32[]{:S(2)}, u32[]{:S(2)}) collective-permute-start(bf16[128,2048]{1,0:T(8,128)(2,1)S(1)} %slice.253), channel_id=1, source_target_pairs={{0,1},{1,0},{2,3},{3,2},{4,5},{5,4},{6,7},{7,6},{8,9},{9,8},{10,11... | collective-permute-start | bytes 1572872 | tf_op jit(solution)/shard_map/ppermute | solution.py:235
  112.8 5.0 %collective-permute-start.22 = (bf16[128,2048]{1,0:T(8,128)(2,1)S(1)}, bf16[128,2048]{1,0:T(8,128)(2,1)S(1)}, u32[]{:S(2)}, u32[]{:S(2)}) collective-permute-start(bf16[128,2048]{1,0:T(8,128)(2,1)S(1)} %slice.257), channel_id=1, source_target_pairs={{0,1},{1,0},{2,3},{3,2},{4,5},{5,4},{6,7},{7,6},{8,9},{9,8},{10,11... | collective-permute-start | bytes 1572872 | tf_op jit(solution)/shard_map/ppermute | solution.py:235
  115.3 3.4 %collective-permute-start.29 = (bf16[128,2048]{1,0:T(8,128)(2,1)S(1)}, bf16[128,2048]{1,0:T(8,128)(2,1)S(1)}, u32[]{:S(2)}, u32[]{:S(2)}) collective-permute-start(bf16[128,2048]{1,0:T(8,128)(2,1)S(1)} %slice.261), channel_id=1, source_target_pairs={{0,1},{1,0},{2,3},{3,2},{4,5},{5,4},{6,7},{7,6},{8,9},{9,8},{10,11... | collective-permute-start | bytes 1572872 | tf_op jit(solution)/shard_map/ppermute | solution.py:235
  115.5 28.9 %collective-permute-start.10 = (bf16[64,2048]{1,0:T(8,128)(2,1)S(1)}, bf16[64,2048]{1,0:T(8,128)(2,1)S(1)}, u32[]{:S(2)}, u32[]{:S(2)}) collective-permute-start(bf16[64,2048]{1,0:T(8,128)(2,1)S(1)} %slice.251), channel_id=1, source_target_pairs={{0,2},{1,3},{2,0},{3,1},{4,6},{5,7},{6,4},{7,5},{8,10},{9,11},{10,... | collective-permute-start | bytes 786440 | tf_op jit(solution)/shard_map/ppermute | solution.py:235
  116.3 14.1 %collective-permute-start.16 = (bf16[64,2048]{1,0:T(8,128)(2,1)S(1)}, bf16[64,2048]{1,0:T(8,128)(2,1)S(1)}, u32[]{:S(2)}, u32[]{:S(2)}) collective-permute-start(bf16[64,2048]{1,0:T(8,128)(2,1)S(1)} %slice.255), channel_id=1, source_target_pairs={{0,2},{1,3},{2,0},{3,1},{4,6},{5,7},{6,4},{7,5},{8,10},{9,11},{10,... | collective-permute-start | bytes 786440 | tf_op jit(solution)/shard_map/ppermute | solution.py:235
  118.0 18.0 %collective-permute-start.23 = (bf16[64,2048]{1,0:T(8,128)(2,1)S(1)}, bf16[64,2048]{1,0:T(8,128)(2,1)S(1)}, u32[]{:S(2)}, u32[]{:S(2)}) collective-permute-start(bf16[64,2048]{1,0:T(8,128)(2,1)S(1)} %slice.259), channel_id=1, source_target_pairs={{0,2},{1,3},{2,0},{3,1},{4,6},{5,7},{6,4},{7,5},{8,10},{9,11},{10,... | collective-permute-start | bytes 786440 | tf_op jit(solution)/shard_map/ppermute | solution.py:235
  118.8 22.4 %collective-permute-start.30 = (bf16[64,2048]{1,0:T(8,128)(2,1)S(1)}, bf16[64,2048]{1,0:T(8,128)(2,1)S(1)}, u32[]{:S(2)}, u32[]{:S(2)}) collective-permute-start(bf16[64,2048]{1,0:T(8,128)(2,1)S(1)} %slice.263), channel_id=1, source_target_pairs={{0,2},{1,3},{2,0},{3,1},{4,6},{5,7},{6,4},{7,5},{8,10},{9,11},{10,... | collective-permute-start | bytes 786440 | tf_op jit(solution)/shard_map/ppermute | solution.py:235
  130.5 14.0 %collective-permute-start.17 = (bf16[64,2048]{1,0:T(8,128)(2,1)S(1)}, bf16[64,2048]{1,0:T(8,128)(2,1)S(1)}, u32[]{:S(2)}, u32[]{:S(2)}) collective-permute-start(bf16[64,2048]{1,0:T(8,128)(2,1)S(1)} %add_convert_fusion.7), channel_id=1, source_target_pairs={{0,12},{4,0},{8,4},{12,8},{1,13},{5,1},{9,5},{13,9},{2,14},{6,2},{... | collective-permute-start | bytes 786440 | tf_op jit(solution)/shard_map/ppermute | solution.py:240
  136.1 21.2 %collective-permute-start.24 = (bf16[64,2048]{1,0:T(8,128)(2,1)S(1)}, bf16[64,2048]{1,0:T(8,128)(2,1)S(1)}, u32[]{:S(2)}, u32[]{:S(2)}) collective-permute-start(bf16[64,2048]{1,0:T(8,128)(2,1)S(1)} %add_convert_fusion.6), channel_id=1, source_target_pairs={{0,8},{4,12},{8,0},{12,4},{1,9},{5,13},{9,1},{13,5},{2,10},{6,14},... | collective-permute-start | bytes 786440 | tf_op jit(solution)/shard_map/ppermute | solution.py:240
  141.2 16.1 %collective-permute-start.31 = (bf16[64,2048]{1,0:T(8,128)(2,1)S(1)}, bf16[64,2048]{1,0:T(8,128)(2,1)S(1)}, u32[]{:S(2)}, u32[]{:S(2)}) collective-permute-start(bf16[64,2048]{1,0:T(8,128)(2,1)S(1)} %add_convert_fusion.5), channel_id=1, source_target_pairs={{0,4},{4,8},{8,12},{12,0},{1,5},{5,9},{9,13},{13,1},{2,6},{6,10},{... | collective-permute-start | bytes 786440 | tf_op jit(solution)/shard_map/ppermute | solution.py:240

commit v2 on v1

--- a/solution.py
+++ b/solution.py
@@ -2,6 +2,7 @@
 import jax.numpy as jnp
 from jax import lax
 from jax.sharding import PartitionSpec as P
+
 
 HS_SMALL = 64
 HS_LARGE = 128
@@ -113,7 +114,7 @@
 
 
 def finish(state):
-    largest, weight_sum, accumulated = state
+    _, weight_sum, accumulated = state
     merged = accumulated / weight_sum[..., None]
     return merged.reshape(merged.shape[0], -1).astype(jnp.bfloat16)
 
@@ -237,7 +238,8 @@
 
 def shift(values, axis, step):
     size = lax.axis_size(axis)
-    return lax.ppermute(values, axis, [(place, (place + step) % size) for place in range(size)])
+    pairs = [(place, (place + step) % size) for place in range(size)]
+    return lax.ppermute(values, axis, pairs)
 
 
 def flips(axis):
@@ -247,16 +249,26 @@
 
 def gather_near(rows, axis, along=0):
     for flip in reversed(flips(axis)):
-        rows = jnp.concatenate([rows, swap(rows, axis, flip)], axis=along)
+        arrived = swap(rows, axis, flip)
+        rows = jnp.concatenate([rows, arrived], axis=along)
     return rows
 
 
-def add_near(rows, axis):
+def add_near(make, row_count):
+    axis = "tp"
+    half = row_count // 2
+    kept, given = None, None
     for flip in flips(axis):
-        kept = rows.shape[0] // 2
-        arrived = swap(rows[kept:], axis, flip)
-        rows = (rows[:kept].astype(jnp.float32) + arrived.astype(jnp.float32)).astype(jnp.bfloat16)
-    return rows
+        if kept is None:
+            given = make(half, row_count)
+            arrived = swap(given, axis, flip)
+            kept = make(0, half).astype(jnp.float32) + arrived.astype(jnp.float32)
+        else:
+            half = kept.shape[0] // 2
+            kept = kept.astype(jnp.bfloat16)
+            arrived = swap(kept[half:], axis, flip)
+            kept = kept[:half].astype(jnp.float32) + arrived.astype(jnp.float32)
+    return kept
 
 
 def near_order(axis):
@@ -373,17 +385,19 @@
     ).reshape(token_rows, kv_large, -1, HS_LARGE)
     heard_small = attend_pieces(asked_small, [p[0] for p in pieces], [p[1] for p in pieces])
     heard_large = attend_pieces(asked_large, [p[2] for p in pieces], [p[3] for p in pieces])
-    terms = (
-        jnp.dot(heard_small, out_weight_small, preferred_element_type=jnp.float32)
-        + jnp.dot(heard_large, out_weight_large, preferred_element_type=jnp.float32)
-    ).astype(jnp.bfloat16)
-    for flip in flips("tp"):
-        kept = terms.shape[0] // 2
-        arrived = swap(terms[kept:], "tp", flip)
-        terms = terms[:kept].astype(jnp.float32) + arrived.astype(jnp.float32)
-        if kept > local_rows:
-            terms = terms.astype(jnp.bfloat16)
-    attended = (residual_in.astype(jnp.float32) + terms).astype(jnp.bfloat16)
+
+    def project(first, last):
+        return (
+            jnp.dot(
+                heard_small[first:last], out_weight_small, preferred_element_type=jnp.float32
+            )
+            + jnp.dot(
+                heard_large[first:last], out_weight_large, preferred_element_type=jnp.float32
+            )
+        ).astype(jnp.bfloat16)
+
+    attended = add_near(project, token_rows)
+    attended = (residual_in.astype(jnp.float32) + attended).astype(jnp.bfloat16)
     widened = attended.astype(jnp.float32)
     normed = (
         widened
@@ -392,9 +406,10 @@
     ).astype(jnp.bfloat16)
 
     arrivals = [normed] + [shift(normed, "sp", step) for step in steps[1:]]
+    down = expert_down.reshape(-1, expert_down.shape[2])
     total = attended.astype(jnp.float32)
     for step in steps:
-        rows = gather_near(arrivals[step], "tp")
+        rows = lax.optimization_barrier(gather_near(arrivals[step], "tp"))
         actives = []
         for place in range(local_experts):
             gate_out = jnp.dot(rows, expert_gate[place], preferred_element_type=jnp.float32)
@@ -404,13 +419,16 @@
                     jnp.bfloat16
                 )
             )
-        down = expert_down.reshape(-1, expert_down.shape[2])
-        partial = jnp.dot(
-            jnp.concatenate(actives, axis=1), down, preferred_element_type=jnp.float32
-        ).astype(jnp.bfloat16)
-        summed = add_near(partial, "tp")
+        actives = jnp.concatenate(actives, axis=1)
+
+        def finish_rows(first, last):
+            return jnp.dot(
+                actives[first:last], down, preferred_element_type=jnp.float32
+            ).astype(jnp.bfloat16)
+
+        summed = add_near(finish_rows, token_rows)
         if step:
-            summed = shift(summed, "sp", -step)
+            summed = shift(summed.astype(jnp.bfloat16), "sp", -step)
         total = total + summed.astype(jnp.float32)
     return total.astype(jnp.bfloat16)
 

time: 159 us -> 163 us (1.025)
  matrix products: 22.9 us -> 27.6 us
  waiting for transfers between devices: 62.2 us -> 65.9 us
  other arithmetic: 14 us -> 11.7 us
  local copies, waits for them, and re-layouts: 15 us -> 12.9 us
    ppermute x20, waiting for transfers between devices: 28 us -> 32.4 us  [swap(): lax.ppermute(values, axis, [(place, place ^ flip) for place in range(size)])]
    dot_general x6 -> x12, matrix products: 3.84 us -> 6.91 us  [the longest x8 3.74 us: finish_rows(): jnp.dot(actives[first:last], down, preferred_element_type=jnp.float32)]
    convert_element_type x8 -> x3, other arithmetic: 1.89 us -> 0.2 us  [gather_plan(): summed = shift(summed.astype(jnp.bfloat16), 'sp', -step)]
    unnamed x60 -> x70, local copies, waits for them, and re-layouts: 4.9 us -> 3.32 us
  transfers between devices with their start and end apart: 32 -> 32, of which waited for: 12 -> 12; matrix products, arithmetic and copies ran while one was open for 18% -> 15% of each run, Pallas kernels for 0% -> 0%
where the time goes in v2:
time: 163 us; the launch traced here: 162 us
  waiting for transfers between devices  65.9 us (40%)
  starting transfers between devices  43 us (26%)
  matrix products  27.6 us (17%)
  local copies, waits for them, and re-layouts  12.9 us (8%)
  other arithmetic  11.7 us (7%)
    ppermute x12, waiting for transfers between devices, shift(): return lax.ppermute(values, axis, pairs)  33.6 us
    ppermute x20, waiting for transfers between devices, swap(): lax.ppermute(values, axis, [(place, place ^ flip) for place in range(size)])  32.4 us
    ppermute x12, starting transfers between devices, shift(): return lax.ppermute(values, axis, pairs)  29.7 us
    ppermute x20, starting transfers between devices, swap(): lax.ppermute(values, axis, [(place, place ^ flip) for place in range(size)])  13.3 us
    dot_general x8, matrix products, attend_pieces(): jnp.einsum('qgrd,kgd->grqk', queries, piece.reshape(piece.shape[0], kv_lo...  9.27 us
    split x6, local copies, waits for them, and re-layouts, gather_plan(): pieces = [jnp.split(rows, ends, axis=1) for rows in memories]  5.01 us
    dot_general x8, matrix products, gather_plan(): up_out = jnp.dot(rows, expert_up[place], preferred_element_type=jnp.float32)  4.43 us
    dot_general x8, matrix products, gather_plan(): jnp.dot(rows, expert_gate[place], preferred_element_type=jnp.float32)  4.4 us
  transfers between devices with their start and end apart: 32, of which 12 were waited for; matrix products, arithmetic and copies ran while one was open for 15% of the time, Pallas kernels for 0%

profile of v2, /device:TPU:0, one launch (start us, length us, event | category | flops | bytes accessed | tf_op | source)
XLA Modules:
  0.0 162.2 jit_solution(8029105994133427934)
XLA Ops:
  0.1 1.1 copy.109
  1.2 0.9 copy.108
  2.2 0.7 multiply_multiply_fusion.1
  3.3 0.7 fusion.97
  5.2 0.9 concatenate.121
  6.1 3.1 %collective-permute-start = (bf16[256,512]{1,0:T(8,128)(2,1)}, bf16[256,512]{1,0:T(8,128)(2,1)}, u32[]{:S(2)}, u32[]{:S(2)}) collective-permute-start(bf16[256,512]{1,0:T(8,128)(2,1)} %concatenate.121), channel_id=1, source_target_pairs={{0,4},{4,8},{8,12},{12,0},{1,5},{5,9},{9,13},{13,1},{2,6},{6,10},{... | collective-permute-start | bytes 786440 | tf_op jit(solution)/shard_map/ppermute | solution.py:242
  9.1 2.6 %collective-permute-start.1 = (bf16[256,512]{1,0:T(8,128)(2,1)}, bf16[256,512]{1,0:T(8,128)(2,1)}, u32[]{:S(2)}, u32[]{:S(2)}) collective-permute-start(bf16[256,512]{1,0:T(8,128)(2,1)} %concatenate.121), channel_id=1, source_target_pairs={{0,8},{4,12},{8,0},{12,4},{1,9},{5,13},{9,1},{13,5},{2,10},{6,14},... | collective-permute-start | bytes 786440 | tf_op jit(solution)/shard_map/ppermute | solution.py:242
  11.7 1.3 collective-permute-start.2
  13.1 1.0 multiply_cosine_fusion.1
  15.0 0.9 subtract_convert_fusion.1
  15.9 0.8 pad_maximum_fusion.19
  17.6 1.7 %fusion.167 = (f32[2,2,256]{2,1,0:T(2,128)}, f32[2,2,256,256]{2,3,1,0:T(8,128)S(1)}) fusion(bf16[256,2,2,64]{0,3,2,1:T(8,128)(2,1)S(1)} %bitcast.242, bf16[256,2,16]{0,2,1:T(8,128)(2,1)} %copy-done.16, bf16[256,2,16]{0,2,1:T(8,128)(2,1)} %copy-done.17, bf16[256,2,16]{0,2,1:T(8,128)(2,1)} %copy-done.15, bf16[256,2,16]{0,2,1:T(8,128)(2,1)S(1)} %get-tuple-element.28), kind=kOutput, calls=%fused_computation.293 | convolution fusion | flops 34339840 | bytes 1249280 | tf_op jit(solution)/shard_map/qgrd,kgd->grqk/dot_general | solution.py:285
  19.4 1.2 bitcast_reduce_fusion.3
  20.6 1.1 bitcast_reduce_fusion.2
  21.7 7.4 %collective-permute-done.1 = bf16[256,512]{1,0:T(8,128)(2,1)} collective-permute-done((bf16[256,512]{1,0:T(8,128)(2,1)}, bf16[256,512]{1,0:T(8,128)(2,1)}, u32[]{:S(2)}, u32[]{:S(2)}) %collective-permute-start.1) | collective-permute-done | bytes 262176 | tf_op jit(solution)/shard_map/ppermute | solution.py:242
  29.1 1.1 bitcast_reduce_fusion.1
  30.8 1.6 fusion.160
  32.3 1.6 fusion.161
  33.9 0.7 fusion.162
  35.1 0.6 fusion.163
  35.8 0.9 copy.117
  36.7 1.3 fusion.168
  38.2 1.3 fusion.166
  39.7 1.3 fusion.165
  41.0 0.9 pad_maximum_fusion.8
  41.9 0.9 copy.115
  42.8 2.3 %fusion.14 = f32[2,2,256]{2,1,0:T(2,128)S(1)} fusion(f32[2,2,256]{2,1,0:T(2,128)S(1)} %maximum_maximum_fusion, f32[2,2,256,256]{2,3,1,0:T(8,128)} %get-tuple-element.73, f32[2,2,256,256]{2,3,1,0:T(8,128)} %get-tuple-element.75, f32[2,2,256,256]{2,3,1,0:T(8,128)} %get-tuple-element.79, f32[2,2,256,256]{2,3,1,0:T(8,128)S(1)} %get-tuple-element.77), kind=kLoop, calls=%fused_computation.27 | loop fusion | flops 5241856 | bytes 4202496 | tf_op jit(solution)/shard_map/reduce_sum | solution.py:298
  45.6 2.1 %fusion.28 = bf16[256,2,2,64]{0,3,2,1:T(8,128)(2,1)S(1)} fusion(bf16[1024,2,64,1]{0,2,3,1:T(8,128)(2,1)S(1)} %bitcast.263, f32[2,2,256]{2,1,0:T(2,128)S(1)} %maximum_maximum_fusion, f32[2,2,256,256]{2,3,1,0:T(8,128)S(1)} %copy-done.7, f32[2,2,256,256]{2,3,1,0:T(8,128)S(1)} %copy-done.6, f32[2,2,256,256]{2,3,1,0:T(8,128)S(1)} %copy-done.5, ...), kind=kOutput, calls=%fused_computation.45 | convolution fusion | flops 139591680 | bytes 4595712 | tf_op jit(solution)/shard_map/grqk,kgd->qgrd/dot_general | solution.py:299
  48.1 0.8 copy-done.2
  49.0 1.1 fusion.3
  50.5 1.8 %collective-permute-done.3 = bf16[128,2048]{1,0:T(8,128)(2,1)} collective-permute-done((bf16[128,2048]{1,0:T(8,128)(2,1)}, bf16[128,2048]{1,0:T(8,128)(2,1)}, u32[]{:S(2)}, u32[]{:S(2)}) %collective-permute-start.3) | collective-permute-done | bytes 524320 | tf_op jit(solution)/shard_map/ppermute | solution.py:236
  52.3 1.4 add_convert_fusion.4
  53.8 1.5 collective-permute-start.4
  55.3 0.6 collective-permute-start.7
  55.9 6.3 %collective-permute-done.7 = f32[8,64]{1,0:T(8,128)S(1)} collective-permute-done((f32[8,64]{1,0:T(8,128)S(1)}, f32[8,64]{1,0:T(8,128)S(1)}, u32[]{:S(2)}, u32[]{:S(2)}) %collective-permute-start.7) | collective-permute-done | bytes 2080 | tf_op jit(solution)/shard_map/ppermute | solution.py:236
  62.4 1.2 collective-permute-done.8
  63.6 4.9 %collective-permute-start.14 = (f32[8,256]{1,0:T(8,128)S(1)}, f32[8,256]{1,0:T(8,128)S(1)}, u32[]{:S(2)}, u32[]{:S(2)}) collective-permute-start(f32[8,256]{1,0:T(8,128)S(1)} %pad_maximum_fusion.21), channel_id=1, source_target_pairs={{0,4},{4,8},{8,12},{12,0},{1,5},{5,9},{9,13},{13,1},{2,6},{6,10},{... | collective-permute-start | bytes 24584 | tf_op jit(solution)/shard_map/ppermute | solution.py:242
  68.5 2.8 %collective-permute-start.21 = (f32[8,256]{1,0:T(8,128)S(1)}, f32[8,256]{1,0:T(8,128)S(1)}, u32[]{:S(2)}, u32[]{:S(2)}) collective-permute-start(f32[8,256]{1,0:T(8,128)S(1)} %pad_maximum_fusion.21), channel_id=1, source_target_pairs={{0,8},{4,12},{8,0},{12,4},{1,9},{5,13},{9,1},{13,5},{2,10},{6,14},... | collective-permute-start | bytes 24584 | tf_op jit(solution)/shard_map/ppermute | solution.py:242
  71.6 2.1 %collective-permute-start.11 = (bf16[64,2048]{1,0:T(8,128)(2,1)S(1)}, bf16[64,2048]{1,0:T(8,128)(2,1)S(1)}, u32[]{:S(2)}, u32[]{:S(2)}) collective-permute-start(bf16[64,2048]{1,0:T(8,128)(2,1)S(1)} %fusion.82), channel_id=1, source_target_pairs={{0,4},{4,8},{8,12},{12,0},{1,5},{5,9},{9,13},{13,1},{2,6},{6,10},{... | collective-permute-start | bytes 786440 | tf_op jit(solution)/shard_map/ppermute | solution.py:242
  73.7 1.5 collective-permute-start.5
  75.4 2.6 %collective-permute-start.25 = (bf16[64,2048]{1,0:T(8,128)(2,1)S(1)}, bf16[64,2048]{1,0:T(8,128)(2,1)S(1)}, u32[]{:S(2)}, u32[]{:S(2)}) collective-permute-start(bf16[64,2048]{1,0:T(8,128)(2,1)S(1)} %fusion.82), channel_id=1, source_target_pairs={{0,12},{4,0},{8,4},{12,8},{1,13},{5,1},{9,5},{13,9},{2,14},{6,2},{... | collective-permute-start | bytes 786440 | tf_op jit(solution)/shard_map/ppermute | solution.py:242
  78.0 4.9 %collective-permute-done.11 = bf16[64,2048]{1,0:T(8,128)(2,1)S(1)} collective-permute-done((bf16[64,2048]{1,0:T(8,128)(2,1)S(1)}, bf16[64,2048]{1,0:T(8,128)(2,1)S(1)}, u32[]{:S(2)}, u32[]{:S(2)}) %collective-permute-start.11) | collective-permute-done | bytes 262176 | tf_op jit(solution)/shard_map/ppermute | solution.py:242
  82.8 1.5 collective-permute-start.12
  84.3 8.4 %collective-permute-done.18 = bf16[64,2048]{1,0:T(8,128)(2,1)S(1)} collective-permute-done((bf16[64,2048]{1,0:T(8,128)(2,1)S(1)}, bf16[64,2048]{1,0:T(8,128)(2,1)S(1)}, u32[]{:S(2)}, u32[]{:S(2)}) %collective-permute-start.18) | collective-permute-done | bytes 262176 | tf_op jit(solution)/shard_map/ppermute | solution.py:242
  92.7 1.5 collective-permute-start.19
  94.3 0.6 collective-permute-start.26
  95.2 6.7 %collective-permute-done.19 = bf16[64,2048]{1,0:T(8,128)(2,1)S(1)} collective-permute-done((bf16[64,2048]{1,0:T(8,128)(2,1)S(1)}, bf16[64,2048]{1,0:T(8,128)(2,1)S(1)}, u32[]{:S(2)}, u32[]{:S(2)}) %collective-permute-start.19) | collective-permute-done | bytes 262176 | tf_op jit(solution)/shard_map/ppermute | solution.py:236
  102.0 4.4 %collective-permute-done.26 = bf16[64,2048]{1,0:T(8,128)(2,1)S(1)} collective-permute-done((bf16[64,2048]{1,0:T(8,128)(2,1)S(1)}, bf16[64,2048]{1,0:T(8,128)(2,1)S(1)}, u32[]{:S(2)}, u32[]{:S(2)}) %collective-permute-start.26) | collective-permute-done | bytes 262176 | tf_op jit(solution)/shard_map/ppermute | solution.py:236
  108.9 0.6 multiply_convert_fusion.6
  114.2 0.6 multiply_convert_fusion.5
  114.7 0.6 multiply_convert_fusion.4
  116.4 0.6 multiply_convert_fusion.2
  118.5 0.6 multiply_convert_fusion
  120.2 1.6 collective-permute-start.10
  122.2 0.6 collective-permute-start.16
  123.3 1.6 collective-permute-start.23
  125.4 0.6 collective-permute-start.30
  126.0 9.0 %collective-permute-done.16 = bf16[64,2048]{1,0:T(8,128)(2,1)S(1)} collective-permute-done((bf16[64,2048]{1,0:T(8,128)(2,1)S(1)}, bf16[64,2048]{1,0:T(8,128)(2,1)S(1)}, u32[]{:S(2)}, u32[]{:S(2)}) %collective-permute-start.16) | collective-permute-done | bytes 262176 | tf_op jit(solution)/shard_map/ppermute | solution.py:236
  135.1 5.3 %collective-permute-start.17 = (bf16[64,2048]{1,0:T(8,128)(2,1)S(1)}, bf16[64,2048]{1,0:T(8,128)(2,1)S(1)}, u32[]{:S(2)}, u32[]{:S(2)}) collective-permute-start(bf16[64,2048]{1,0:T(8,128)(2,1)S(1)} %add_convert_fusion.7), channel_id=1, source_target_pairs={{0,12},{4,0},{8,4},{12,8},{1,13},{5,1},{9,5},{13,9},{2,14},{6,2},{... | collective-permute-start | bytes 786440 | tf_op jit(solution)/shard_map/ppermute | solution.py:242
  140.7 2.4 %collective-permute-start.24 = (bf16[64,2048]{1,0:T(8,128)(2,1)S(1)}, bf16[64,2048]{1,0:T(8,128)(2,1)S(1)}, u32[]{:S(2)}, u32[]{:S(2)}) collective-permute-start(bf16[64,2048]{1,0:T(8,128)(2,1)S(1)} %add_convert_fusion.6), channel_id=1, source_target_pairs={{0,8},{4,12},{8,0},{12,4},{1,9},{5,13},{9,1},{13,5},{2,10},{6,14},... | collective-permute-start | bytes 786440 | tf_op jit(solution)/shard_map/ppermute | solution.py:242
  143.1 2.6 %collective-permute-done.30 = bf16[64,2048]{1,0:T(8,128)(2,1)S(1)} collective-permute-done((bf16[64,2048]{1,0:T(8,128)(2,1)S(1)}, bf16[64,2048]{1,0:T(8,128)(2,1)S(1)}, u32[]{:S(2)}, u32[]{:S(2)}) %collective-permute-start.30) | collective-permute-done | bytes 262176 | tf_op jit(solution)/shard_map/ppermute | solution.py:236
  145.9 2.5 %collective-permute-start.31 = (bf16[64,2048]{1,0:T(8,128)(2,1)S(1)}, bf16[64,2048]{1,0:T(8,128)(2,1)S(1)}, u32[]{:S(2)}, u32[]{:S(2)}) collective-permute-start(bf16[64,2048]{1,0:T(8,128)(2,1)S(1)} %add_convert_fusion.5), channel_id=1, source_target_pairs={{0,4},{4,8},{8,12},{12,0},{1,5},{5,9},{9,13},{13,1},{2,6},{6,10},{... | collective-permute-start | bytes 786440 | tf_op jit(solution)/shard_map/ppermute | solution.py:242
  148.4 12.9 %collective-permute-done.24 = bf16[64,2048]{1,0:T(8,128)(2,1)S(1)} collective-permute-done((bf16[64,2048]{1,0:T(8,128)(2,1)S(1)}, bf16[64,2048]{1,0:T(8,128)(2,1)S(1)}, u32[]{:S(2)}, u32[]{:S(2)}) %collective-permute-start.24) | collective-permute-done | bytes 262176 | tf_op jit(solution)/shard_map/ppermute | solution.py:242
  161.3 0.9 fusion.86
  (188 shorter events, 19.6 us)
Async XLA Ops:
  0.0 109.4 %copy-start = (bf16[2,256,2048]{2,1,0:T(8,128)(2,1)S(1)}, bf16[2,256,2048]{2,1,0:T(8,128)(2,1)}, u32[]{:S(2)}) copy-start(bf16[2,256,2048]{2,1,0:T(8,128)(2,1)} %param.37) | copy-start | bytes 6291460
  0.0 5.2 %copy-start.13 = (bf16[256,128]{1,0:T(8,128)(2,1)S(1)}, bf16[256,128]{1,0:T(8,128)(2,1)}, u32[]{:S(2)}) copy-start(bf16[256,128]{1,0:T(8,128)(2,1)} %param.21) | copy-start | bytes 196612
  0.0 5.2 %copy-start.24 = (bf16[256,128]{1,0:T(8,128)(2,1)S(1)}, bf16[256,128]{1,0:T(8,128)(2,1)}, u32[]{:S(2)}) copy-start(bf16[256,128]{1,0:T(8,128)(2,1)} %param.24) | copy-start | bytes 196612
  0.0 14.1 %copy-start.22 = (bf16[256,256]{1,0:T(8,128)(2,1)S(1)}, bf16[256,256]{1,0:T(8,128)(2,1)}, u32[]{:S(2)}) copy-start(bf16[256,256]{1,0:T(8,128)(2,1)} %param.22) | copy-start | bytes 393220
  1.2 13.4 %copy-start.31 = (f32[128]{0:T(128)S(1)}, f32[128]{0:T(128)}, u32[]{:S(2)}) copy-start(f32[128]{0:T(128)} %param.27) | copy-start | bytes 1540
  3.2 1.4 copy-start.15
  3.2 1.4 copy-start.16
  3.2 1.4 copy-start.17
  4.4 0.6 copy-start.20
  4.5 7.3 %copy-start.18 = (bf16[256,32]{0,1:T(8,128)(2,1)}, bf16[256,32]{0,1:T(8,128)(2,1)S(1)}, u32[]{:S(2)}) copy-start(bf16[256,32]{0,1:T(8,128)(2,1)S(1)} %get-tuple-element.32) | copy-start | bytes 49156
  6.1 14.6 %collective-permute-start = (bf16[256,512]{1,0:T(8,128)(2,1)}, bf16[256,512]{1,0:T(8,128)(2,1)}, u32[]{:S(2)}, u32[]{:S(2)}) collective-permute-start(bf16[256,512]{1,0:T(8,128)(2,1)} %concatenate.121), channel_id=1, source_target_pairs={{0,4},{4,8},{8,12},{12,0},{1,5},{5,9},{9,13},{13,1},{2,6},{6,10},{... | collective-permute-start | bytes 786440 | tf_op jit(solution)/shard_map/ppermute | solution.py:242
  9.1 20.0 %collective-permute-start.1 = (bf16[256,512]{1,0:T(8,128)(2,1)}, bf16[256,512]{1,0:T(8,128)(2,1)}, u32[]{:S(2)}, u32[]{:S(2)}) collective-permute-start(bf16[256,512]{1,0:T(8,128)(2,1)} %concatenate.121), channel_id=1, source_target_pairs={{0,8},{4,12},{8,0},{12,4},{1,9},{5,13},{9,1},{13,5},{2,10},{6,14},... | collective-permute-start | bytes 786440 | tf_op jit(solution)/shard_map/ppermute | solution.py:242
  11.7 18.5 %collective-permute-start.2 = (bf16[256,512]{1,0:T(8,128)(2,1)}, bf16[256,512]{1,0:T(8,128)(2,1)S(1)}, u32[]{:S(2)}, u32[]{:S(2)}) collective-permute-start(bf16[256,512]{1,0:T(8,128)(2,1)} %concatenate.121), channel_id=1, source_target_pairs={{0,12},{4,0},{8,4},{12,8},{1,13},{5,1},{9,5},{13,9},{2,14},{6,2},{... | collective-permute-start | bytes 786440 | tf_op jit(solution)/shard_map/ppermute | solution.py:242
  14.2 2.6 %copy-start.23 = (bf16[256,256]{1,0:T(8,128)(2,1)S(1)}, bf16[256,256]{1,0:T(8,128)(2,1)}, u32[]{:S(2)}) copy-start(bf16[256,256]{1,0:T(8,128)(2,1)} %param.19) | copy-start | bytes 393220
  14.6 2.4 %copy-start.30 = (f32[64]{0:T(128)S(1)}, f32[64]{0:T(128)}, u32[]{:S(2)}) copy-start(f32[64]{0:T(128)} %param.25) | copy-start | bytes 772
  19.3 23.5 %copy-start.4 = (f32[2,2,256,256]{2,3,1,0:T(8,128)}, f32[2,2,256,256]{2,3,1,0:T(8,128)S(1)}, u32[]{:S(2)}) copy-start(f32[2,2,256,256]{2,3,1,0:T(8,128)S(1)} %get-tuple-element.77) | copy-start | bytes 3145732
  30.2 4.4 %copy-start.25 = (bf16[256,128]{1,0:T(8,128)(2,1)S(1)}, bf16[256,128]{1,0:T(8,128)(2,1)}, u32[]{:S(2)}) copy-start(bf16[256,128]{1,0:T(8,128)(2,1)} %param.24) | copy-start | bytes 196612
  34.6 3.4 %copy-start.10 = (bf16[256,128]{1,0:T(8,128)(2,1)S(1)}, bf16[256,128]{1,0:T(8,128)(2,1)}, u32[]{:S(2)}) copy-start(bf16[256,128]{1,0:T(8,128)(2,1)} %get-tuple-element.19) | copy-start | bytes 196612
  35.1 4.4 %copy-start.9 = (bf16[256,128]{1,0:T(8,128)(2,1)S(1)}, bf16[256,128]{1,0:T(8,128)(2,1)}, u32[]{:S(2)}) copy-start(bf16[256,128]{1,0:T(8,128)(2,1)} %get-tuple-element.22) | copy-start | bytes 196612
  38.1 4.7 %copy-start.26 = (f32[2,2,256]{2,1,0:T(2,128)S(1)}, f32[2,2,256]{2,1,0:T(2,128)}, u32[]{:S(2)}) copy-start(f32[2,2,256]{2,1,0:T(2,128)} %get-tuple-element.76) | copy-start | bytes 12292
  38.2 2.8 %copy-start.12 = (bf16[256,128]{1,0:T(8,128)(2,1)S(1)}, bf16[256,128]{1,0:T(8,128)(2,1)}, u32[]{:S(2)}) copy-start(bf16[256,128]{1,0:T(8,128)(2,1)} %get-tuple-element.17) | copy-start | bytes 196612
  42.8 2.3 %copy-start.5 = (f32[2,2,256,256]{2,3,1,0:T(8,128)S(1)}, f32[2,2,256,256]{2,3,1,0:T(8,128)}, u32[]{:S(2)}) copy-start(f32[2,2,256,256]{2,3,1,0:T(8,128)} %get-tuple-element.79) | copy-start | bytes 3145732
  42.8 2.5 %copy-start.6 = (f32[2,2,256,256]{2,3,1,0:T(8,128)S(1)}, f32[2,2,256,256]{2,3,1,0:T(8,128)}, u32[]{:S(2)}) copy-start(f32[2,2,256,256]{2,3,1,0:T(8,128)} %get-tuple-element.75) | copy-start | bytes 3145732
  42.8 2.8 %copy-start.7 = (f32[2,2,256,256]{2,3,1,0:T(8,128)S(1)}, f32[2,2,256,256]{2,3,1,0:T(8,128)}, u32[]{:S(2)}) copy-start(f32[2,2,256,256]{2,3,1,0:T(8,128)} %get-tuple-element.73) | copy-start | bytes 3145732
  42.8 2.8 %copy-start.8 = (bf16[1024,128]{0,1:T(8,128)(2,1)S(1)}, bf16[1024,128]{0,1:T(8,128)(2,1)}, u32[]{:S(2)}) copy-start(bf16[1024,128]{0,1:T(8,128)(2,1)} %copy.115) | copy-start | bytes 786436
  45.6 2.1 %copy-start.1 = (bf16[256,2048]{1,0:T(8,128)(2,1)S(1)}, bf16[256,2048]{1,0:T(8,128)(2,1)}, u32[]{:S(2)}) copy-start(bf16[256,2048]{1,0:T(8,128)(2,1)} %param.30) | copy-start | bytes 3145732
  47.7 1.2 copy-start.2
  47.7 1.2 copy-start.14
  47.8 2.3 %copy-start.28 = (f32[64,2]{0,1:T(2,128)S(1)}, f32[64,2]{0,1:T(2,128)}, u32[]{:S(2)}) copy-start(f32[64,2]{0,1:T(2,128)} %param.34) | copy-start | bytes 1540
  50.1 2.3 %collective-permute-start.3 = (bf16[128,2048]{1,0:T(8,128)(2,1)}, bf16[128,2048]{1,0:T(8,128)(2,1)}, u32[]{:S(2)}, u32[]{:S(2)}) collective-permute-start(bf16[128,2048]{1,0:T(8,128)(2,1)} %fusion.3), channel_id=1, source_target_pairs={{0,1},{1,0},{2,3},{3,2},{4,5},{5,4},{6,7},{7,6},{8,9},{9,8},{10,11... | collective-permute-start | bytes 1572872 | tf_op jit(solution)/shard_map/ppermute | solution.py:236
  50.1 2.2 %copy-start.3 = (bf16[256,2048]{1,0:T(8,128)(2,1)S(1)}, bf16[256,2048]{1,0:T(8,128)(2,1)}, u32[]{:S(2)}) copy-start(bf16[256,2048]{1,0:T(8,128)(2,1)} %param.31) | copy-start | bytes 3145732
  50.5 4.9 %copy-start.29 = (s32[64,2]{0,1:T(2,128)S(1)}, s32[64,2]{0,1:T(2,128)}, u32[]{:S(2)}) copy-start(s32[64,2]{0,1:T(2,128)} %param.33) | copy-start | bytes 1540
  50.5 20.8 %copy-start.11 = (bf16[64,2048]{1,0:T(8,128)(2,1)S(1)}, bf16[64,2048]{1,0:T(8,128)(2,1)}, u32[]{:S(2)}) copy-start(bf16[64,2048]{1,0:T(8,128)(2,1)} %param.29) | copy-start | bytes 786436
  52.3 19.2 %copy-start.27 = (f32[2048]{0:T(1024)S(1)}, f32[2048]{0:T(1024)}, u32[]{:S(2)}) copy-start(f32[2048]{0:T(1024)} %param.32) | copy-start | bytes 24580
  53.8 17.5 %collective-permute-start.4 = (bf16[64,2048]{1,0:T(8,128)(2,1)S(1)}, bf16[64,2048]{1,0:T(8,128)(2,1)S(1)}, u32[]{:S(2)}, u32[]{:S(2)}) collective-permute-start(bf16[64,2048]{1,0:T(8,128)(2,1)S(1)} %slice.273), channel_id=1, source_target_pairs={{0,2},{1,3},{2,0},{3,1},{4,6},{5,7},{6,4},{7,5},{8,10},{9,11},{10,... | collective-permute-start | bytes 786440 | tf_op jit(solution)/shard_map/ppermute | solution.py:236
  55.3 6.9 %collective-permute-start.7 = (f32[8,64]{1,0:T(8,128)S(1)}, f32[8,64]{1,0:T(8,128)S(1)}, u32[]{:S(2)}, u32[]{:S(2)}) collective-permute-start(f32[8,64]{1,0:T(8,128)S(1)} %bitcast.269), channel_id=1, source_target_pairs={{0,2},{1,3},{2,0},{3,1},{4,6},{5,7},{6,4},{7,5},{8,10},{9,11},{10,... | collective-permute-start | bytes 6152 | tf_op jit(solution)/shard_map/ppermute | solution.py:236
  62.3 1.2 collective-permute-start.8
  63.6 11.6 %collective-permute-start.14 = (f32[8,256]{1,0:T(8,128)S(1)}, f32[8,256]{1,0:T(8,128)S(1)}, u32[]{:S(2)}, u32[]{:S(2)}) collective-permute-start(f32[8,256]{1,0:T(8,128)S(1)} %pad_maximum_fusion.21), channel_id=1, source_target_pairs={{0,4},{4,8},{8,12},{12,0},{1,5},{5,9},{9,13},{13,1},{2,6},{6,10},{... | collective-permute-start | bytes 24584 | tf_op jit(solution)/shard_map/ppermute | solution.py:242
  68.5 6.9 %collective-permute-start.21 = (f32[8,256]{1,0:T(8,128)S(1)}, f32[8,256]{1,0:T(8,128)S(1)}, u32[]{:S(2)}, u32[]{:S(2)}) collective-permute-start(f32[8,256]{1,0:T(8,128)S(1)} %pad_maximum_fusion.21), channel_id=1, source_target_pairs={{0,8},{4,12},{8,0},{12,4},{1,9},{5,13},{9,1},{13,5},{2,10},{6,14},... | collective-permute-start | bytes 24584 | tf_op jit(solution)/shard_map/ppermute | solution.py:242
  71.3 13.1 %collective-permute-start.28 = (f32[8,256]{1,0:T(8,128)S(1)}, f32[8,256]{1,0:T(8,128)S(1)}, u32[]{:S(2)}, u32[]{:S(2)}) collective-permute-start(f32[8,256]{1,0:T(8,128)S(1)} %pad_maximum_fusion.21), channel_id=1, source_target_pairs={{0,12},{4,0},{8,4},{12,8},{1,13},{5,1},{9,5},{13,9},{2,14},{6,2},{... | collective-permute-start | bytes 24584 | tf_op jit(solution)/shard_map/ppermute | solution.py:242
  71.6 11.2 %collective-permute-start.11 = (bf16[64,2048]{1,0:T(8,128)(2,1)S(1)}, bf16[64,2048]{1,0:T(8,128)(2,1)S(1)}, u32[]{:S(2)}, u32[]{:S(2)}) collective-permute-start(bf16[64,2048]{1,0:T(8,128)(2,1)S(1)} %fusion.82), channel_id=1, source_target_pairs={{0,4},{4,8},{8,12},{12,0},{1,5},{5,9},{9,13},{13,1},{2,6},{6,10},{... | collective-permute-start | bytes 786440 | tf_op jit(solution)/shard_map/ppermute | solution.py:242
  73.7 20.5 %collective-permute-start.5 = (bf16[64,2048]{1,0:T(8,128)(2,1)S(1)}, bf16[64,2048]{1,0:T(8,128)(2,1)S(1)}, u32[]{:S(2)}, u32[]{:S(2)}) collective-permute-start(bf16[64,2048]{1,0:T(8,128)(2,1)S(1)} %fusion.82), channel_id=1, source_target_pairs={{0,2},{1,3},{2,0},{3,1},{4,6},{5,7},{6,4},{7,5},{8,10},{9,11},{10,... | collective-permute-start | bytes 786440 | tf_op jit(solution)/shard_map/ppermute | solution.py:236
  75.2 17.5 %collective-permute-start.18 = (bf16[64,2048]{1,0:T(8,128)(2,1)S(1)}, bf16[64,2048]{1,0:T(8,128)(2,1)S(1)}, u32[]{:S(2)}, u32[]{:S(2)}) collective-permute-start(bf16[64,2048]{1,0:T(8,128)(2,1)S(1)} %fusion.82), channel_id=1, source_target_pairs={{0,8},{4,12},{8,0},{12,4},{1,9},{5,13},{9,1},{13,5},{2,10},{6,14},... | collective-permute-start | bytes 786440 | tf_op jit(solution)/shard_map/ppermute | solution.py:242
  75.4 18.9 %collective-permute-start.25 = (bf16[64,2048]{1,0:T(8,128)(2,1)S(1)}, bf16[64,2048]{1,0:T(8,128)(2,1)S(1)}, u32[]{:S(2)}, u32[]{:S(2)}) collective-permute-start(bf16[64,2048]{1,0:T(8,128)(2,1)S(1)} %fusion.82), channel_id=1, source_target_pairs={{0,12},{4,0},{8,4},{12,8},{1,13},{5,1},{9,5},{13,9},{2,14},{6,2},{... | collective-permute-start | bytes 786440 | tf_op jit(solution)/shard_map/ppermute | solution.py:242
  82.8 12.1 %collective-permute-start.12 = (bf16[64,2048]{1,0:T(8,128)(2,1)S(1)}, bf16[64,2048]{1,0:T(8,128)(2,1)S(1)}, u32[]{:S(2)}, u32[]{:S(2)}) collective-permute-start(bf16[64,2048]{1,0:T(8,128)(2,1)S(1)} %collective-permute-done.11), channel_id=1, source_target_pairs={{0,2},{1,3},{2,0},{3,1},{4,6},{5,7},{6,4},{7,5},{8,10},{9,11},{10,... | collective-permute-start | bytes 786440 | tf_op jit(solution)/shard_map/ppermute | solution.py:236
  92.7 9.2 %collective-permute-start.19 = (bf16[64,2048]{1,0:T(8,128)(2,1)S(1)}, bf16[64,2048]{1,0:T(8,128)(2,1)S(1)}, u32[]{:S(2)}, u32[]{:S(2)}) collective-permute-start(bf16[64,2048]{1,0:T(8,128)(2,1)S(1)} %collective-permute-done.18), channel_id=1, source_target_pairs={{0,2},{1,3},{2,0},{3,1},{4,6},{5,7},{6,4},{7,5},{8,10},{9,11},{10,... | collective-permute-start | bytes 786440 | tf_op jit(solution)/shard_map/ppermute | solution.py:236
  94.2 12.3 %collective-permute-start.6 = (bf16[128,2048]{1,0:T(8,128)(2,1)S(1)}, bf16[128,2048]{1,0:T(8,128)(2,1)S(1)}, u32[]{:S(2)}, u32[]{:S(2)}) collective-permute-start(bf16[128,2048]{1,0:T(8,128)(2,1)S(1)} %pad_maximum_fusion.4), channel_id=1, source_target_pairs={{0,1},{1,0},{2,3},{3,2},{4,5},{5,4},{6,7},{7,6},{8,9},{9,8},{10,11... | collective-permute-start | bytes 1572872 | tf_op jit(solution)/shard_map/ppermute | solution.py:236
  94.3 12.1 %collective-permute-start.26 = (bf16[64,2048]{1,0:T(8,128)(2,1)S(1)}, bf16[64,2048]{1,0:T(8,128)(2,1)S(1)}, u32[]{:S(2)}, u32[]{:S(2)}) collective-permute-start(bf16[64,2048]{1,0:T(8,128)(2,1)S(1)} %collective-permute-done.25), channel_id=1, source_target_pairs={{0,2},{1,3},{2,0},{3,1},{4,6},{5,7},{6,4},{7,5},{8,10},{9,11},{10,... | collective-permute-start | bytes 786440 | tf_op jit(solution)/shard_map/ppermute | solution.py:236
  95.0 11.7 %copy-start.32 = (bf16[2,2048,256]{2,1,0:T(8,128)(2,1)S(1)}, bf16[2,2048,256]{2,1,0:T(8,128)(2,1)}, u32[]{:S(2)}) copy-start(bf16[2,2048,256]{2,1,0:T(8,128)(2,1)} %param.35) | copy-start | bytes 6291460
  95.0 15.5 %collective-permute-start.13 = (bf16[128,2048]{1,0:T(8,128)(2,1)S(1)}, bf16[128,2048]{1,0:T(8,128)(2,1)S(1)}, u32[]{:S(2)}, u32[]{:S(2)}) collective-permute-start(bf16[128,2048]{1,0:T(8,128)(2,1)S(1)} %pad_maximum_fusion.5), channel_id=1, source_target_pairs={{0,1},{1,0},{2,3},{3,2},{4,5},{5,4},{6,7},{7,6},{8,9},{9,8},{10,11... | collective-permute-start | bytes 1572872 | tf_op jit(solution)/shard_map/ppermute | solution.py:236
  101.9 9.8 %collective-permute-start.20 = (bf16[128,2048]{1,0:T(8,128)(2,1)S(1)}, bf16[128,2048]{1,0:T(8,128)(2,1)S(1)}, u32[]{:S(2)}, u32[]{:S(2)}) collective-permute-start(bf16[128,2048]{1,0:T(8,128)(2,1)S(1)} %pad_maximum_fusion.6), channel_id=1, source_target_pairs={{0,1},{1,0},{2,3},{3,2},{4,5},{5,4},{6,7},{7,6},{8,9},{9,8},{10,11... | collective-permute-start | bytes 1572872 | tf_op jit(solution)/shard_map/ppermute | solution.py:236
  106.5 6.4 %collective-permute-start.27 = (bf16[128,2048]{1,0:T(8,128)(2,1)S(1)}, bf16[128,2048]{1,0:T(8,128)(2,1)S(1)}, u32[]{:S(2)}, u32[]{:S(2)}) collective-permute-start(bf16[128,2048]{1,0:T(8,128)(2,1)S(1)} %pad_maximum_fusion.7), channel_id=1, source_target_pairs={{0,1},{1,0},{2,3},{3,2},{4,5},{5,4},{6,7},{7,6},{8,9},{9,8},{10,11... | collective-permute-start | bytes 1572872 | tf_op jit(solution)/shard_map/ppermute | solution.py:236
  106.7 1.6 copy-start.33
  109.9 9.8 %collective-permute-start.9 = (bf16[128,2048]{1,0:T(8,128)(2,1)S(1)}, bf16[128,2048]{1,0:T(8,128)(2,1)S(1)}, u32[]{:S(2)}, u32[]{:S(2)}) collective-permute-start(bf16[128,2048]{1,0:T(8,128)(2,1)S(1)} %convolution_convert_fusion.6), channel_id=1, source_target_pairs={{0,1},{1,0},{2,3},{3,2},{4,5},{5,4},{6,7},{7,6},{8,9},{9,8},{10,11... | collective-permute-start | bytes 1572872 | tf_op jit(solution)/shard_map/ppermute | solution.py:236
  115.7 6.0 %collective-permute-start.15 = (bf16[128,2048]{1,0:T(8,128)(2,1)S(1)}, bf16[128,2048]{1,0:T(8,128)(2,1)S(1)}, u32[]{:S(2)}, u32[]{:S(2)}) collective-permute-start(bf16[128,2048]{1,0:T(8,128)(2,1)S(1)} %convolution_convert_fusion.4), channel_id=1, source_target_pairs={{0,1},{1,0},{2,3},{3,2},{4,5},{5,4},{6,7},{7,6},{8,9},{9,8},{10,11... | collective-permute-start | bytes 1572872 | tf_op jit(solution)/shard_map/ppermute | solution.py:236
  117.4 5.4 %collective-permute-start.22 = (bf16[128,2048]{1,0:T(8,128)(2,1)S(1)}, bf16[128,2048]{1,0:T(8,128)(2,1)S(1)}, u32[]{:S(2)}, u32[]{:S(2)}) collective-permute-start(bf16[128,2048]{1,0:T(8,128)(2,1)S(1)} %convolution_convert_fusion.2), channel_id=1, source_target_pairs={{0,1},{1,0},{2,3},{3,2},{4,5},{5,4},{6,7},{7,6},{8,9},{9,8},{10,11... | collective-permute-start | bytes 1572872 | tf_op jit(solution)/shard_map/ppermute | solution.py:236
  119.6 5.3 %collective-permute-start.29 = (bf16[128,2048]{1,0:T(8,128)(2,1)S(1)}, bf16[128,2048]{1,0:T(8,128)(2,1)S(1)}, u32[]{:S(2)}, u32[]{:S(2)}) collective-permute-start(bf16[128,2048]{1,0:T(8,128)(2,1)S(1)} %convolution_convert_fusion), channel_id=1, source_target_pairs={{0,1},{1,0},{2,3},{3,2},{4,5},{5,4},{6,7},{7,6},{8,9},{9,8},{10,11... | collective-permute-start | bytes 1572872 | tf_op jit(solution)/shard_map/ppermute | solution.py:236
  120.2 28.2 %collective-permute-start.10 = (bf16[64,2048]{1,0:T(8,128)(2,1)S(1)}, bf16[64,2048]{1,0:T(8,128)(2,1)S(1)}, u32[]{:S(2)}, u32[]{:S(2)}) collective-permute-start(bf16[64,2048]{1,0:T(8,128)(2,1)S(1)} %slice.277), channel_id=1, source_target_pairs={{0,2},{1,3},{2,0},{3,1},{4,6},{5,7},{6,4},{7,5},{8,10},{9,11},{10,... | collective-permute-start | bytes 786440 | tf_op jit(solution)/shard_map/ppermute | solution.py:236
  122.2 12.8 %collective-permute-start.16 = (bf16[64,2048]{1,0:T(8,128)(2,1)S(1)}, bf16[64,2048]{1,0:T(8,128)(2,1)S(1)}, u32[]{:S(2)}, u32[]{:S(2)}) collective-permute-start(bf16[64,2048]{1,0:T(8,128)(2,1)S(1)} %slice.281), channel_id=1, source_target_pairs={{0,2},{1,3},{2,0},{3,1},{4,6},{5,7},{6,4},{7,5},{8,10},{9,11},{10,... | collective-permute-start | bytes 786440 | tf_op jit(solution)/shard_map/ppermute | solution.py:236
  123.3 17.3 %collective-permute-start.23 = (bf16[64,2048]{1,0:T(8,128)(2,1)S(1)}, bf16[64,2048]{1,0:T(8,128)(2,1)S(1)}, u32[]{:S(2)}, u32[]{:S(2)}) collective-permute-start(bf16[64,2048]{1,0:T(8,128)(2,1)S(1)} %slice.285), channel_id=1, source_target_pairs={{0,2},{1,3},{2,0},{3,1},{4,6},{5,7},{6,4},{7,5},{8,10},{9,11},{10,... | collective-permute-start | bytes 786440 | tf_op jit(solution)/shard_map/ppermute | solution.py:236
  125.4 20.4 %collective-permute-start.30 = (bf16[64,2048]{1,0:T(8,128)(2,1)S(1)}, bf16[64,2048]{1,0:T(8,128)(2,1)S(1)}, u32[]{:S(2)}, u32[]{:S(2)}) collective-permute-start(bf16[64,2048]{1,0:T(8,128)(2,1)S(1)} %slice.289), channel_id=1, source_target_pairs={{0,2},{1,3},{2,0},{3,1},{4,6},{5,7},{6,4},{7,5},{8,10},{9,11},{10,... | collective-permute-start | bytes 786440 | tf_op jit(solution)/shard_map/ppermute | solution.py:236
  135.1 13.3 %collective-permute-start.17 = (bf16[64,2048]{1,0:T(8,128)(2,1)S(1)}, bf16[64,2048]{1,0:T(8,128)(2,1)S(1)}, u32[]{:S(2)}, u32[]{:S(2)}) collective-permute-start(bf16[64,2048]{1,0:T(8,128)(2,1)S(1)} %add_convert_fusion.7), channel_id=1, source_target_pairs={{0,12},{4,0},{8,4},{12,8},{1,13},{5,1},{9,5},{13,9},{2,14},{6,2},{... | collective-permute-start | bytes 786440 | tf_op jit(solution)/shard_map/ppermute | solution.py:242
  140.7 20.5 %collective-permute-start.24 = (bf16[64,2048]{1,0:T(8,128)(2,1)S(1)}, bf16[64,2048]{1,0:T(8,128)(2,1)S(1)}, u32[]{:S(2)}, u32[]{:S(2)}) collective-permute-start(bf16[64,2048]{1,0:T(8,128)(2,1)S(1)} %add_convert_fusion.6), channel_id=1, source_target_pairs={{0,8},{4,12},{8,0},{12,4},{1,9},{5,13},{9,1},{13,5},{2,10},{6,14},... | collective-permute-start | bytes 786440 | tf_op jit(solution)/shard_map/ppermute | solution.py:242
  145.9 15.4 %collective-permute-start.31 = (bf16[64,2048]{1,0:T(8,128)(2,1)S(1)}, bf16[64,2048]{1,0:T(8,128)(2,1)S(1)}, u32[]{:S(2)}, u32[]{:S(2)}) collective-permute-start(bf16[64,2048]{1,0:T(8,128)(2,1)S(1)} %add_convert_fusion.5), channel_id=1, source_target_pairs={{0,4},{4,8},{8,12},{12,0},{1,5},{5,9},{9,13},{13,1},{2,6},{6,10},{... | collective-permute-start | bytes 786440 | tf_op jit(solution)/shard_map/ppermute | solution.py:242
  (2 other events, 1.2 us)

commit v3 on v2

--- a/solution.py
+++ b/solution.py
@@ -1,6 +1,9 @@
 import jax
 import jax.numpy as jnp
+import numpy as np
 from jax import lax
+from jax.experimental import pallas as pl
+from jax.experimental.pallas import tpu as pltpu
 from jax.sharding import PartitionSpec as P
 
 
@@ -236,10 +239,17 @@
     return lax.ppermute(values, axis, [(place, place ^ flip) for place in range(size)])
 
 
-def shift(values, axis, step):
-    size = lax.axis_size(axis)
-    pairs = [(place, (place + step) % size) for place in range(size)]
-    return lax.ppermute(values, axis, pairs)
+def meet(values, flip):
+    return swap(values, "sp", flip)
+
+
+def inner_meet(values):
+    return lax.ppermute(values, "sp", [(0, 0), (1, 2), (2, 1), (3, 3)])
+
+
+def is_inner():
+    place = lax.axis_index("sp")
+    return jnp.logical_or(place == 1, place == 2)
 
 
 def flips(axis):
@@ -278,32 +288,268 @@
     return order
 
 
-def attend_pieces(queries, key_pieces, value_pieces):
-    head_size = queries.shape[-1]
-    kv_local = queries.shape[1]
-    scores = [
-        jnp.einsum(
-            "qgrd,kgd->grqk",
-            queries,
-            piece.reshape(piece.shape[0], kv_local, head_size),
-            preferred_element_type=jnp.float32,
+LANES = 128
+
+
+def turn_tables(head_size, rows):
+    quarter = head_size // 4
+    lane = np.arange(LANES) % head_size
+    rate = theta_base ** (-2.0 * (lane % quarter) / (head_size // 2))
+    sign = np.where((lane // quarter) % 2 == 0, -1.0, 1.0)
+
+    def pair(count):
+        angles = np.arange(count)[:, None] * rate
+        return [np.cos(angles).astype(np.float32), (np.sin(angles) * sign).astype(np.float32)]
+
+    return pair(rows) + pair(GRID_W)
+
+
+def swap_quarters(rows, head_size):
+    quarter = head_size // 4
+    lane = lax.broadcasted_iota(jnp.int32, rows.shape, 1)
+    ahead = pltpu.roll(rows, LANES - quarter, 1)
+    behind = pltpu.roll(rows, quarter, 1)
+    return jnp.where((lane // quarter) % 2 == 0, ahead, behind)
+
+
+def turn_block(raw, gain, head_size, cosine, sine):
+    rows = raw.astype(jnp.float32)
+    squares = rows * rows
+    lane = lax.broadcasted_iota(jnp.int32, rows.shape, 1)
+    means = None
+    for head in range(LANES // head_size):
+        inside = (lane // head_size) == head
+        mean = jnp.sum(jnp.where(inside, squares, 0.0), axis=1, keepdims=True) / head_size
+        means = mean if means is None else jnp.where(inside, mean, means)
+    scaled = rows * lax.rsqrt(means + norm_eps) * gain
+    return (scaled * cosine + swap_quarters(scaled, head_size) * sine).astype(jnp.bfloat16)
+
+
+def lane_tables(first_row, blocks, head_size, refs):
+    row_cos, row_sin, col_cos, col_sin = refs
+    lane = lax.broadcasted_iota(jnp.int32, (GRID_W, LANES), 1)
+    by_row = (lane % head_size) < head_size // 2
+    cosines, sines = [], []
+    for block in range(blocks):
+        row = pl.ds(first_row + block, 1)
+        cosines.append(jnp.where(by_row, row_cos[row, :], col_cos[...]))
+        sines.append(jnp.where(by_row, row_sin[row, :], col_sin[...]))
+    return jnp.concatenate(cosines, axis=0), jnp.concatenate(sines, axis=0)
+
+
+def key_kernel(*refs):
+    sources, (memory,), held, sems = refs[:7], refs[7:8], refs[8:13], refs[13]
+    keys_s, keys_l, gain_s, gain_l, tables = held
+    targets = [
+        keys_s,
+        memory.at[:, LANES : 2 * LANES],
+        keys_l,
+        memory.at[:, 3 * LANES :],
+        gain_s,
+        gain_l,
+        tables,
+    ]
+    copies = [
+        pltpu.make_async_copy(source, target, sems.at[place])
+        for place, (source, target) in enumerate(zip(sources, targets))
+    ]
+    for copy in copies:
+        copy.start()
+    for copy in copies:
+        copy.wait()
+    blocks = memory.shape[0] // GRID_W
+    first = lax.axis_index("sp") * blocks
+    rows = tables.shape[0] // 4 - GRID_W
+    place = 0
+    parts = []
+    for count in (rows, rows, GRID_W, GRID_W) * 2:
+        parts.append(tables.at[place : place + count])
+        place += count
+    gain = jnp.concatenate([gain_s[...]] * (LANES // HS_SMALL), axis=1)
+    cosine, sine = lane_tables(first, blocks, HS_SMALL, parts[:4])
+    memory[:, :LANES] = turn_block(keys_s[...], gain, HS_SMALL, cosine, sine)
+    cosine, sine = lane_tables(first, blocks, HS_LARGE, parts[4:])
+    memory[:, 2 * LANES : 3 * LANES] = turn_block(
+        keys_l[...], gain_l[...], HS_LARGE, cosine, sine
+    )
+
+
+def make_memory(keys_s, values_s, keys_l, values_l, gain_s, gain_l, rows):
+    rows = (rows + 7) // 8 * 8
+    tables = np.concatenate(turn_tables(HS_SMALL, rows) + turn_tables(HS_LARGE, rows))
+    operands = (keys_s, values_s, keys_l, values_l, gain_s[None, :], gain_l[None, :], tables)
+    held = [operands[place] for place in (0, 2, 4, 5, 6)]
+    return pl.pallas_call(
+        key_kernel,
+        out_shape=jax.ShapeDtypeStruct((keys_s.shape[0], 4 * LANES), jnp.bfloat16),
+        in_specs=[pl.BlockSpec(memory_space=pl.ANY)] * len(operands),
+        out_specs=pl.BlockSpec(memory_space=pltpu.VMEM),
+        scratch_shapes=[pltpu.VMEM(array.shape, array.dtype) for array in held]
+        + [pltpu.SemaphoreType.DMA((len(operands),))],
+        name="keys",
+        cost_estimate=pl.CostEstimate(flops=4000000, bytes_accessed=1000000, transcendentals=0),
+    )(*operands)
+
+
+def attend_kernel(asked_s, asked_l, *rest):
+    heard_s, heard_l, last = rest[5:]
+    inner = is_inner()
+
+    @pl.when(inner)
+    def _():
+        last[...] = rest[3][...]
+
+    @pl.when(jnp.logical_not(inner))
+    def _():
+        last[...] = rest[4][...]
+
+    memories = (rest[0], rest[1], rest[2], last)
+    rows = asked_s.shape[0]
+    low = lax.broadcasted_iota(jnp.int32, (rows, LANES), 1) < HS_SMALL
+
+    def attend(queries, key_at, scale):
+        factor = scale * 1.4426950408889634
+        scores = [
+            lax.dot_general(
+                queries,
+                memory[:, key_at : key_at + LANES],
+                (((1,), (1,)), ((), ())),
+                preferred_element_type=jnp.float32,
+            )
+            for memory in memories
+        ]
+        peak = scores[0]
+        for piece in scores[1:]:
+            peak = jnp.maximum(peak, piece)
+        peak = jnp.max(peak, axis=1, keepdims=True)
+        total, heard = None, None
+        for piece, memory in zip(scores, memories):
+            weights = jnp.exp2((piece - peak) * factor)
+            total = weights if total is None else total + weights
+            part = jnp.dot(
+                weights.astype(jnp.bfloat16),
+                memory[:, key_at + LANES : key_at + 2 * LANES],
+                preferred_element_type=jnp.float32,
+            )
+            heard = part if heard is None else heard + part
+        return heard / jnp.sum(total, axis=1, keepdims=True)
+
+    zero = jnp.zeros((rows, LANES), jnp.float32)
+    for side in range(2):
+        both = asked_s[:, side * LANES : (side + 1) * LANES].astype(jnp.float32)
+        turned = pltpu.roll(both, HS_SMALL, 1)
+        here = low if side == 0 else jnp.logical_not(low)
+        first, second = (both, turned) if side == 0 else (turned, both)
+        first = jnp.where(here, first, zero).astype(jnp.bfloat16)
+        second = jnp.where(here, second, zero).astype(jnp.bfloat16)
+        one = attend(first, 0, HS_SMALL**-0.5)
+        two = attend(second, 0, HS_SMALL**-0.5)
+        if side == 0:
+            two = pltpu.roll(two, HS_SMALL, 1)
+        else:
+            one = pltpu.roll(one, HS_SMALL, 1)
+        heard_s[:, side * LANES : (side + 1) * LANES] = jnp.where(low, one, two).astype(
+            jnp.bfloat16
         )
-        * head_size ** (-0.5)
-        for piece in key_pieces
-    ]
-    scores = jnp.concatenate(scores, axis=-1)
-    values = jnp.concatenate(value_pieces, axis=0)
-    peak = jnp.max(scores, axis=-1, keepdims=True)
-    weights = jnp.exp(scores - peak)
-    total = jnp.sum(weights, axis=-1)
-    heard = jnp.einsum(
-        "grqk,kgd->qgrd",
-        weights.astype(jnp.bfloat16),
-        values.reshape(values.shape[0], kv_local, head_size),
-        preferred_element_type=jnp.float32,
-    )
-    heard = heard / jnp.transpose(total, (2, 0, 1))[..., None]
-    return heard.reshape(heard.shape[0], -1).astype(jnp.bfloat16)
+    for head in range(asked_l.shape[1] // LANES):
+        lanes = slice(head * LANES, (head + 1) * LANES)
+        heard_l[:, lanes] = attend(asked_l[:, lanes], 2 * LANES, HS_LARGE**-0.5).astype(
+            jnp.bfloat16
+        )
+
+
+def attend_all(asked_s, asked_l, memories):
+    rows = asked_s.shape[0]
+    vmem = pl.BlockSpec(memory_space=pltpu.VMEM)
+    shapes = [jax.ShapeDtypeStruct(a.shape, jnp.bfloat16) for a in (asked_s, asked_l)]
+    return pl.pallas_call(
+        attend_kernel,
+        out_shape=shapes,
+        in_specs=[vmem] * (2 + len(memories)),
+        out_specs=[vmem, vmem],
+        scratch_shapes=[pltpu.VMEM(memories[0].shape, jnp.bfloat16)],
+        name="attend",
+        cost_estimate=pl.CostEstimate(
+            flops=2 * 6 * 2 * rows * rows * 4 * LANES,
+            bytes_accessed=2 << 20,
+            transcendentals=6 * rows * rows * 4,
+        ),
+        compiler_params=pltpu.CompilerParams(vmem_limit_bytes=16 << 20),
+    )(asked_s, asked_l, *memories)
+
+
+def pick_kernel(inner, outer, picked):
+    at_inner = is_inner()
+
+    @pl.when(at_inner)
+    def _():
+        picked[...] = inner[...]
+
+    @pl.when(jnp.logical_not(at_inner))
+    def _():
+        picked[...] = outer[...]
+
+
+def pick(inner, outer):
+    vmem = pl.BlockSpec(memory_space=pltpu.VMEM)
+    return pl.pallas_call(
+        pick_kernel,
+        out_shape=jax.ShapeDtypeStruct(inner.shape, inner.dtype),
+        in_specs=[vmem, vmem],
+        out_specs=vmem,
+        name="pick",
+        cost_estimate=pl.CostEstimate(flops=1000000, bytes_accessed=1 << 19, transcendentals=0),
+        compiler_params=pltpu.CompilerParams(vmem_limit_bytes=2 << 20),
+    )(inner, outer)
+
+
+def expert_kernel(*refs):
+    pieces, (blend, gate, up, down) = refs[:4], refs[4:8]
+    kept, other, given, rows, active = refs[8:]
+    local = pieces[0].shape[0]
+    for place, piece in enumerate(pieces):
+        rows[place * local : (place + 1) * local, :] = piece[...]
+    width = gate.shape[2]
+    columns = blend[...].T
+    expert = lax.broadcasted_iota(jnp.int32, columns.shape, 1)
+    first_expert = lax.axis_index("sp") * gate.shape[0]
+    for place in range(gate.shape[0]):
+        chosen = jnp.where(expert == first_expert + place, columns, 0.0)
+        mixing = jnp.sum(chosen, axis=1, keepdims=True)
+        gate_out = jnp.dot(rows[...], gate[place], preferred_element_type=jnp.float32)
+        up_out = jnp.dot(rows[...], up[place], preferred_element_type=jnp.float32)
+        result = gate_out / (1.0 + jnp.exp(-gate_out)) * up_out * mixing
+        active[:, place * width : (place + 1) * width] = result.astype(jnp.bfloat16)
+    step = 512
+    for first in range(0, down.shape[1], step):
+        columns = slice(first, first + step)
+        out = jnp.dot(active[...], down[:, columns], preferred_element_type=jnp.float32)
+        out = out.astype(jnp.bfloat16)
+        kept[:, columns] = out[:local]
+        other[:, columns] = out[local : 2 * local]
+        given[:, columns] = out[2 * local :]
+
+
+def run_experts(pieces, mixing, gate, up, down):
+    local, wide = pieces[0].shape
+    vmem = pl.BlockSpec(memory_space=pltpu.VMEM)
+    hidden = gate.shape[0] * gate.shape[2]
+    shapes = [jax.ShapeDtypeStruct((n, wide), jnp.bfloat16) for n in (local, local, 2 * local)]
+    return pl.pallas_call(
+        expert_kernel,
+        out_shape=shapes,
+        in_specs=[vmem] * 8,
+        out_specs=[vmem] * 3,
+        scratch_shapes=[
+            pltpu.VMEM((4 * local, wide), jnp.bfloat16),
+            pltpu.VMEM((4 * local, hidden), jnp.bfloat16),
+        ],
+        name="expert",
+        cost_estimate=pl.CostEstimate(
+            flops=6 * 4 * local * wide * hidden, bytes_accessed=4 << 20, transcendentals=0
+        ),
+        compiler_params=pltpu.CompilerParams(vmem_limit_bytes=16 << 20),
+    )(*pieces, mixing, gate, up, down)
 
 
 def gather_plan(
@@ -337,31 +583,25 @@
     offset = sp_index * token_rows
     tables_small = grid_tables(offset, token_rows, HS_SMALL)
     tables_large = grid_tables(offset, token_rows, HS_LARGE)
-    kv_small = keys_small.shape[1] // HS_SMALL
-    kv_large = keys_large.shape[1] // HS_LARGE
-    turned_small = normed_turn(
-        keys_small.reshape(token_rows, kv_small, HS_SMALL), key_gain_small, tables_small
-    ).reshape(token_rows, -1)
-    turned_large = normed_turn(
-        keys_large.reshape(token_rows, kv_large, HS_LARGE), key_gain_large, tables_large
-    ).reshape(token_rows, -1)
-    memory = jnp.concatenate([turned_small, values_small, turned_large, values_large], axis=1)
-    memories = [memory] + [shift(memory, "sp", step) for step in steps[1:]]
-    cuts = [keys_small.shape[1], values_small.shape[1], keys_large.shape[1]]
-    ends = [sum(cuts[: place + 1]) for place in range(3)]
-    pieces = [jnp.split(rows, ends, axis=1) for rows in memories]
+    memory = make_memory(
+        keys_small,
+        values_small,
+        keys_large,
+        values_large,
+        key_gain_small,
+        key_gain_large,
+        sp_count * token_rows // GRID_W,
+    )
+    second = meet(memory, 2)
+    inner = inner_meet(memory)
+    memories = [memory, meet(memory, 1), second, inner, meet(second, 1)]
 
     shares = route_scores / jnp.sum(route_scores, axis=1, keepdims=True)
     experts = jnp.arange(local_experts * sp_count, dtype=jnp.int32)
     named = (routes[:, :, None] == experts).astype(jnp.float32)
     mixing = jnp.sum(named * shares[:, :, None], axis=1).T
     mixing = gather_near(mixing, "tp", along=1)
-    mixings = [mixing] + [shift(mixing, "sp", step) for step in steps[1:]]
-    mixings = [
-        lax.dynamic_slice_in_dim(block, sp_index * local_experts, local_experts, 0)
-        for block in mixings
-    ]
-
+    mixings = [mixing] + [meet(mixing, step) for step in steps[1:]]
     order = near_order("tp")
 
     def reorder(rows):
@@ -377,14 +617,13 @@
         normed_turn(
             queries_small.reshape(token_rows, -1, HS_SMALL), query_gain_small, tables_small
         ).reshape(token_rows, -1)
-    ).reshape(token_rows, kv_small, -1, HS_SMALL)
+    )
     asked_large = reorder(
         normed_turn(
             queries_large.reshape(token_rows, -1, HS_LARGE), query_gain_large, tables_large
         ).reshape(token_rows, -1)
-    ).reshape(token_rows, kv_large, -1, HS_LARGE)
-    heard_small = attend_pieces(asked_small, [p[0] for p in pieces], [p[1] for p in pieces])
-    heard_large = attend_pieces(asked_large, [p[2] for p in pieces], [p[3] for p in pieces])
+    )
+    heard_small, heard_large = attend_all(asked_small, asked_large, memories)
 
     def project(first, last):
         return (
@@ -405,30 +644,27 @@
         * norm_gain
     ).astype(jnp.bfloat16)
 
-    arrivals = [normed] + [shift(normed, "sp", step) for step in steps[1:]]
+    arrivals = [normed, meet(normed, 1), meet(normed, 2)]
+    inner = inner_meet(normed)
+    outer = meet(arrivals[2], 1)
+    arrivals.append(pick(inner, outer))
     down = expert_down.reshape(-1, expert_down.shape[2])
     total = attended.astype(jnp.float32)
+    near, far = flips("tp")
     for step in steps:
-        rows = lax.optimization_barrier(gather_near(arrivals[step], "tp"))
-        actives = []
-        for place in range(local_experts):
-            gate_out = jnp.dot(rows, expert_gate[place], preferred_element_type=jnp.float32)
-            up_out = jnp.dot(rows, expert_up[place], preferred_element_type=jnp.float32)
-            actives.append(
-                (jax.nn.silu(gate_out) * up_out * mixings[step][place][:, None]).astype(
-                    jnp.bfloat16
-                )
-            )
-        actives = jnp.concatenate(actives, axis=1)
-
-        def finish_rows(first, last):
-            return jnp.dot(
-                actives[first:last], down, preferred_element_type=jnp.float32
-            ).astype(jnp.bfloat16)
-
-        summed = add_near(finish_rows, token_rows)
+        own = arrivals[step]
+        beside = swap(own, "tp", far)
+        pieces = [own, beside]
+        pieces += [swap(own, "tp", near), swap(beside, "tp", near)]
+        kept, other, given = run_experts(pieces, mixings[step], expert_gate, expert_up, down)
+        arrived = swap(given, "tp", near).astype(jnp.float32)
+        other = (other.astype(jnp.float32) + arrived[local_rows:]).astype(jnp.bfloat16)
+        crossed = swap(other, "tp", far).astype(jnp.float32)
+        summed = kept.astype(jnp.float32) + arrived[:local_rows] + crossed
         if step:
-            summed = shift(summed.astype(jnp.bfloat16), "sp", -step)
+            summed = summed.astype(jnp.bfloat16)
+        if step:
+            summed = meet(summed, step)
         total = total + summed.astype(jnp.float32)
     return total.astype(jnp.bfloat16)
 
@@ -441,7 +677,9 @@
     capacity = max(2, (2 * routes.size + expert_count - 1) // expert_count)
     slots = devices * expert_gate.shape[0] * capacity
     tp_size = lax.axis_size("tp")
-    if tokens <= slots and tp_size & (tp_size - 1) == 0:
+    widths = [array.shape[1] for array in arrays[:6]]
+    fits = widths == [256, 128, 128, 256, 128, 128] and arrays[0].shape[0] % GRID_W == 0
+    if tokens <= slots and tp_size == 4 and lax.axis_size("sp") == 4 and fits:
         return gather_plan(*arrays)
     return dispatch_plan(*arrays)
 

time: 163 us -> 140 us (0.86)
  matrix products: 27.6 us -> 1.24 us
  Pallas kernels: 0 us -> 13 us
  waiting for transfers between devices: 65.9 us -> 73.8 us
  local copies, waits for them, and re-layouts: 12.9 us -> 6.62 us
  starting transfers between devices: 43 us -> 37.1 us
  other arithmetic: 11.7 us -> 7.34 us
    ppermute x20 -> x36, waiting for transfers between devices: 32.4 us -> 73.8 us  [swap(): lax.ppermute(values, axis, [(place, place ^ flip) for place in range(size)])]
    ppermute x12 -> x2, waiting for transfers between devices: 33.6 us -> 0.01 us  [inner_meet(): return lax.ppermute(values, 'sp', [(0, 0), (1, 2), (2, 1), (3, 3)])]
    ppermute x12 -> x2, starting transfers between devices: 29.7 us -> 2.26 us  [inner_meet(): return lax.ppermute(values, 'sp', [(0, 0), (1, 2), (2, 1), (3, 3)])]
    dot_general x34 -> x0, matrix products: 24.4 us -> none  [the longest x8 9.27 us: attend_pieces(): jnp.einsum('qgrd,kgd->grqk', queries, piece.reshape(piece.shape[0], kv_lo...]
    ppermute x20 -> x36, starting transfers between devices: 13.3 us -> 34.8 us  [swap(): lax.ppermute(values, axis, [(place, place ^ flip) for place in range(size)])]
    pallas_call x0 -> x7, Pallas kernels: none -> 13 us  [the longest x4 7.44 us: run_experts(): pl.pallas_call(expert_kernel, out_shape=shapes, in_specs=[vmem] * 8, out_...]
    split x6 -> x0, local copies, waits for them, and re-layouts: 5.01 us -> none  [gather_plan(): pieces = [jnp.split(rows, ends, axis=1) for rows in memories]]
    reduce_sum x2 -> x0, other arithmetic: 2.58 us -> none  [attend_pieces(): total = jnp.sum(weights, axis=-1)]
  transfers between devices with their start and end apart: 32 -> 38, of which waited for: 12 -> 16; matrix products, arithmetic and copies ran while one was open for 15% -> 6% of each run, Pallas kernels for 0% -> 5%
where the time goes in v3:
time: 140 us
  waiting for transfers between devices  73.8 us (53%)
  starting transfers between devices  37.1 us (26%)
  Pallas kernels  13 us (9%)
  other arithmetic  7.34 us (5%)
  local copies, waits for them, and re-layouts  6.62 us (5%)
    ppermute x36, waiting for transfers between devices, swap(): lax.ppermute(values, axis, [(place, place ^ flip) for place in range(size)])  73.8 us
    ppermute x36, starting transfers between devices, swap(): lax.ppermute(values, axis, [(place, place ^ flip) for place in range(size)])  34.8 us
    pallas_call x4, Pallas kernels, run_experts(): pl.pallas_call(expert_kernel, out_shape=shapes, in_specs=[vmem] * 8, out_...  7.44 us
    unnamed x30, local copies, waits for them, and re-layouts  5.41 us
    pallas_call x1, Pallas kernels, attend_all(): pl.pallas_call(attend_kernel, out_shape=shapes, in_specs=[vmem] * (2 + le...  2.99 us
  transfers between devices with their start and end apart: 38, of which 16 were waited for; matrix products, arithmetic and copies ran while one was open for 6% of the time, Pallas kernels for 5%

profile of v3, /device:TPU:0, one launch (start us, length us, event | category | flops | bytes accessed | tf_op | source)
XLA Modules:
  0.0 139.6 jit_solution(573186525892408365)
XLA Ops:
  0.0 2.3 %keys.1.rest_0_ = bf16[256,512]{1,0:T(8,128)(2,1)} custom-call(bf16[256,128]{1,0:T(8,128)(2,1)} %refs_0_.1, bf16[256,128]{1,0:T(8,128)(2,1)} %refs_1_.1, bf16[256,128]{1,0:T(8,128)(2,1)} %refs_2_.1, bf16[256,128]{1,0:T(8,128)(2,1)} %refs_3_.1, f32[1,64]{1,0:T(1,128)} %bitcast.27, f32[1,128]{1,0:T(1,128)} %bitcast.28, f32[320,128]{1,0:T(8,128)} %constant.79.clone.refs_6_), custom_call_target="tpu_custom_call" | custom-call | flops 4000000 | bytes 1000000 | tf_op jit(solution)/shard_map/keys/pallas_call | solution.py:382
  2.4 3.1 %collective-permute-start = (bf16[256,512]{1,0:T(8,128)(2,1)}, bf16[256,512]{1,0:T(8,128)(2,1)S(1)}, u32[]{:S(2)}, u32[]{:S(2)}) collective-permute-start(bf16[256,512]{1,0:T(8,128)(2,1)} %keys.1.rest_0_), channel_id=1, source_target_pairs={{0,4},{4,0},{8,12},{12,8},{1,5},{5,1},{9,13},{13,9},{2,6},{6,2},{1... | collective-permute-start | bytes 786440 | tf_op jit(solution)/shard_map/ppermute | solution.py:239
  5.5 2.6 %collective-permute-start.1 = (bf16[256,512]{1,0:T(8,128)(2,1)}, bf16[256,512]{1,0:T(8,128)(2,1)S(1)}, u32[]{:S(2)}, u32[]{:S(2)}) collective-permute-start(bf16[256,512]{1,0:T(8,128)(2,1)} %keys.1.rest_0_), channel_id=1, source_target_pairs={{0,8},{4,12},{8,0},{12,4},{1,9},{5,13},{9,1},{13,5},{2,10},{6,14},... | collective-permute-start | bytes 786440 | tf_op jit(solution)/shard_map/ppermute | solution.py:239
  8.1 1.6 %collective-permute-start.2 = (bf16[256,512]{1,0:T(8,128)(2,1)}, bf16[256,512]{1,0:T(8,128)(2,1)S(1)}, u32[]{:S(2)}, u32[]{:S(2)}) collective-permute-start(bf16[256,512]{1,0:T(8,128)(2,1)} %keys.1.rest_0_), channel_id=1, source_target_pairs={{0,0},{4,8},{8,4},{12,12},{1,1},{5,9},{9,5},{13,13},{2,2},{6,10},{... | collective-permute-start | bytes 786440 | tf_op jit(solution)/shard_map/ppermute | solution.py:247
  9.7 1.0 copy.41
  10.8 1.0 reshape.319
  11.8 0.3 multiply_reduce_fusion
  12.4 1.0 multiply_cosine_fusion.1
  13.5 0.3 multiply_multiply_fusion
  13.9 0.9 subtract_convert_fusion.1
  14.8 0.8 pad_maximum_fusion.2
  15.9 5.5 %collective-permute-done.1.rest_2_ = bf16[256,512]{1,0:T(8,128)(2,1)S(1)} collective-permute-done((bf16[256,512]{1,0:T(8,128)(2,1)}, bf16[256,512]{1,0:T(8,128)(2,1)S(1)}, u32[]{:S(2)}, u32[]{:S(2)}) %collective-permute-start.1) | collective-permute-done | bytes 262176 | tf_op jit(solution)/shard_map/ppermute | solution.py:239
  21.9 5.9 %collective-permute-done.3.rest_4_ = bf16[256,512]{1,0:T(8,128)(2,1)S(1)} collective-permute-done((bf16[256,512]{1,0:T(8,128)(2,1)S(1)}, bf16[256,512]{1,0:T(8,128)(2,1)S(1)}, u32[]{:S(2)}, u32[]{:S(2)}) %collective-permute-start.3) | collective-permute-done | bytes 262176 | tf_op jit(solution)/shard_map/ppermute | solution.py:239
  27.8 3.0 %attend.1 = (bf16[256,256]{1,0:T(8,128)(2,1)S(1)}, bf16[256,256]{1,0:T(8,128)(2,1)S(1)}) custom-call(bf16[256,256]{1,0:T(8,128)(2,1)S(1)} %pad_maximum_fusion.1.asked_s, bf16[256,256]{1,0:T(8,128)(2,1)S(1)} %pad_maximum_fusion.3.asked_l, bf16[256,512]{1,0:T(8,128)(2,1)S(1)} %copy-done.4, bf16[256,512]{1,0:T(8,128)(2,1)S(1)} %collective-permute-done.rest_1_, ...), custom_call_target="tpu_custom_call" | custom-call | flops 805306368 | bytes 2097152 | tf_op jit(solution)/shard_map/attend/pallas_call | solution.py:465
  30.8 0.3 fusion.25
  31.1 0.3 fusion.4
  31.5 0.3 fusion.28
  31.8 1.5 %collective-permute-done.4 = bf16[128,2048]{1,0:T(8,128)(2,1)S(1)} collective-permute-done((bf16[128,2048]{1,0:T(8,128)(2,1)S(1)}, bf16[128,2048]{1,0:T(8,128)(2,1)S(1)}, u32[]{:S(2)}, u32[]{:S(2)}) %collective-permute-start.4) | collective-permute-done | bytes 524320 | tf_op jit(solution)/shard_map/ppermute | solution.py:239
  33.4 0.3 fusion.3
  33.7 0.8 copy-done.6
  34.5 1.6 %collective-permute-start.5 = (bf16[64,2048]{1,0:T(8,128)(2,1)S(1)}, bf16[64,2048]{1,0:T(8,128)(2,1)}, u32[]{:S(2)}, u32[]{:S(2)}) collective-permute-start(bf16[64,2048]{1,0:T(8,128)(2,1)S(1)} %slice.109), channel_id=1, source_target_pairs={{0,2},{1,3},{2,0},{3,1},{4,6},{5,7},{6,4},{7,5},{8,10},{9,11},{10,... | collective-permute-start | bytes 786440 | tf_op jit(solution)/shard_map/ppermute | solution.py:239
  36.1 6.9 %collective-permute-done.5 = bf16[64,2048]{1,0:T(8,128)(2,1)} collective-permute-done((bf16[64,2048]{1,0:T(8,128)(2,1)S(1)}, bf16[64,2048]{1,0:T(8,128)(2,1)}, u32[]{:S(2)}, u32[]{:S(2)}) %collective-permute-start.5) | collective-permute-done | bytes 262176 | tf_op jit(solution)/shard_map/ppermute | solution.py:239
  43.1 1.3 fusion.5
  44.6 1.1 collective-permute-start.21
  45.6 1.5 %collective-permute-start.6 = (bf16[64,2048]{1,0:T(8,128)(2,1)S(1)}, bf16[64,2048]{1,0:T(8,128)(2,1)S(1)}, u32[]{:S(2)}, u32[]{:S(2)}) collective-permute-start(bf16[64,2048]{1,0:T(8,128)(2,1)S(1)} %fusion.7.refs_0_), channel_id=1, source_target_pairs={{0,2},{1,3},{2,0},{3,1},{4,6},{5,7},{6,4},{7,5},{8,10},{9,11},{10,... | collective-permute-start | bytes 786440 | tf_op jit(solution)/shard_map/ppermute | solution.py:239
  47.2 0.6 collective-permute-start.9
  47.7 0.7 collective-permute-start.29
  48.4 3.8 %collective-permute-start.13 = (bf16[64,2048]{1,0:T(8,128)(2,1)S(1)}, bf16[64,2048]{1,0:T(8,128)(2,1)S(1)}, u32[]{:S(2)}, u32[]{:S(2)}) collective-permute-start(bf16[64,2048]{1,0:T(8,128)(2,1)S(1)} %fusion.7.refs_0_), channel_id=1, source_target_pairs={{0,4},{4,0},{8,12},{12,8},{1,5},{5,1},{9,13},{13,9},{2,6},{6,2},{1... | collective-permute-start | bytes 786440 | tf_op jit(solution)/shard_map/ppermute | solution.py:239
  52.2 0.8 collective-permute-done.9
  53.0 5.6 %collective-permute-done.21.refs_0_ = bf16[64,2048]{1,0:T(8,128)(2,1)S(1)} collective-permute-done((bf16[64,2048]{1,0:T(8,128)(2,1)S(1)}, bf16[64,2048]{1,0:T(8,128)(2,1)S(1)}, u32[]{:S(2)}, u32[]{:S(2)}) %collective-permute-start.21) | collective-permute-done | bytes 262176 | tf_op jit(solution)/shard_map/ppermute | solution.py:239
  58.7 2.7 %collective-permute-start.25 = (f32[8,256]{1,0:T(8,128)S(1)}, f32[8,256]{1,0:T(8,128)S(1)}, u32[]{:S(2)}, u32[]{:S(2)}) collective-permute-start(f32[8,256]{1,0:T(8,128)S(1)} %pad_maximum_fusion.4.refs_4_), channel_id=1, source_target_pairs={{0,8},{4,12},{8,0},{12,4},{1,9},{5,13},{9,1},{13,5},{2,10},{6,14},... | collective-permute-start | bytes 24584 | tf_op jit(solution)/shard_map/ppermute | solution.py:239
  61.3 3.4 %collective-permute-done.25.refs_4_ = f32[8,256]{1,0:T(8,128)S(1)} collective-permute-done((f32[8,256]{1,0:T(8,128)S(1)}, f32[8,256]{1,0:T(8,128)S(1)}, u32[]{:S(2)}, u32[]{:S(2)}) %collective-permute-start.25) | collective-permute-done | bytes 8224 | tf_op jit(solution)/shard_map/ppermute | solution.py:239
  64.7 3.1 %collective-permute-start.17 = (f32[8,256]{1,0:T(8,128)S(1)}, f32[8,256]{1,0:T(8,128)S(1)}, u32[]{:S(2)}, u32[]{:S(2)}) collective-permute-start(f32[8,256]{1,0:T(8,128)S(1)} %pad_maximum_fusion.4.refs_4_), channel_id=1, source_target_pairs={{0,4},{4,0},{8,12},{12,8},{1,5},{5,1},{9,13},{13,9},{2,6},{6,2},{1... | collective-permute-start | bytes 24584 | tf_op jit(solution)/shard_map/ppermute | solution.py:239
  67.8 1.6 %collective-permute-done.17.refs_4_ = f32[8,256]{1,0:T(8,128)S(1)} collective-permute-done((f32[8,256]{1,0:T(8,128)S(1)}, f32[8,256]{1,0:T(8,128)S(1)}, u32[]{:S(2)}, u32[]{:S(2)}) %collective-permute-start.17) | collective-permute-done | bytes 8224 | tf_op jit(solution)/shard_map/ppermute | solution.py:239
  69.5 1.5 %collective-permute-start.22 = (bf16[64,2048]{1,0:T(8,128)(2,1)S(1)}, bf16[64,2048]{1,0:T(8,128)(2,1)S(1)}, u32[]{:S(2)}, u32[]{:S(2)}) collective-permute-start(bf16[64,2048]{1,0:T(8,128)(2,1)S(1)} %collective-permute-done.21.refs_0_), channel_id=1, source_target_pairs={{0,2},{1,3},{2,0},{3,1},{4,6},{5,7},{6,4},{7,5},{8,10},{9,11},{10,... | collective-permute-start | bytes 786440 | tf_op jit(solution)/shard_map/ppermute | solution.py:239
  71.2 0.5 collective-permute-start.14
  71.9 1.6 %collective-permute-start.31 = (bf16[64,2048]{1,0:T(8,128)(2,1)S(1)}, bf16[64,2048]{1,0:T(8,128)(2,1)S(1)}, u32[]{:S(2)}, u32[]{:S(2)}) collective-permute-start(bf16[64,2048]{1,0:T(8,128)(2,1)S(1)} %pick.1.refs_0_), channel_id=1, source_target_pairs={{0,2},{1,3},{2,0},{3,1},{4,6},{5,7},{6,4},{7,5},{8,10},{9,11},{10,... | collective-permute-start | bytes 786440 | tf_op jit(solution)/shard_map/ppermute | solution.py:239
  73.5 5.1 %collective-permute-done.22.refs_1_ = bf16[64,2048]{1,0:T(8,128)(2,1)S(1)} collective-permute-done((bf16[64,2048]{1,0:T(8,128)(2,1)S(1)}, bf16[64,2048]{1,0:T(8,128)(2,1)S(1)}, u32[]{:S(2)}, u32[]{:S(2)}) %collective-permute-start.22) | collective-permute-done | bytes 262176 | tf_op jit(solution)/shard_map/ppermute | solution.py:239
  78.6 0.5 collective-permute-start.15
  79.2 5.1 %collective-permute-done.14.refs_1_ = bf16[64,2048]{1,0:T(8,128)(2,1)S(1)} collective-permute-done((bf16[64,2048]{1,0:T(8,128)(2,1)S(1)}, bf16[64,2048]{1,0:T(8,128)(2,1)S(1)}, u32[]{:S(2)}, u32[]{:S(2)}) %collective-permute-start.14) | collective-permute-done | bytes 262176 | tf_op jit(solution)/shard_map/ppermute | solution.py:239
  84.3 1.6 %copy-done.2 = bf16[2,2048,256]{2,1,0:T(8,128)(2,1)S(1)} copy-done((bf16[2,2048,256]{2,1,0:T(8,128)(2,1)S(1)}, bf16[2,2048,256]{2,1,0:T(8,128)(2,1)}, u32[]{:S(2)}) %copy-start.2) | copy-done | bytes 2097176
  85.9 1.6 %copy-done.3 = bf16[2,256,2048]{2,1,0:T(8,128)(2,1)S(1)} copy-done((bf16[2,256,2048]{2,1,0:T(8,128)(2,1)S(1)}, bf16[2,256,2048]{2,1,0:T(8,128)(2,1)}, u32[]{:S(2)}) %copy-start.3) | copy-done | bytes 2097176
  87.4 1.9 %expert.4 = (bf16[64,2048]{1,0:T(8,128)(2,1)S(1)}, bf16[64,2048]{1,0:T(8,128)(2,1)S(1)}, bf16[128,2048]{1,0:T(8,128)(2,1)S(1)}) custom-call(bf16[64,2048]{1,0:T(8,128)(2,1)S(1)} %fusion.7.refs_0_, bf16[64,2048]{1,0:T(8,128)(2,1)S(1)} %collective-permute-done.6.refs_1_, bf16[64,2048]{1,0:T(8,128)(2,1)S(1)} %collective-permute-done.7.refs_2_, ...), custom_call_target="tpu_custom_call" | custom-call | flops 1610612736 | bytes 4194304 | tf_op jit(solution)/shard_map/expert/pallas_call | solution.py:538
  89.3 0.6 collective-permute-start.11
  90.0 0.4 collective-permute-start.33
  90.4 1.9 %expert.6 = (bf16[64,2048]{1,0:T(8,128)(2,1)S(1)}, bf16[64,2048]{1,0:T(8,128)(2,1)S(1)}, bf16[128,2048]{1,0:T(8,128)(2,1)S(1)}) custom-call(bf16[64,2048]{1,0:T(8,128)(2,1)S(1)} %collective-permute-done.21.refs_0_, bf16[64,2048]{1,0:T(8,128)(2,1)S(1)} %collective-permute-done.22.refs_1_, bf16[64,2048]{1,0:T(8,128)(2,1)S(1)} %collective-permute-done.23.refs_2_, ...), custom_call_target="tpu_custom_call" | custom-call | flops 1610612736 | bytes 4194304 | tf_op jit(solution)/shard_map/expert/pallas_call | solution.py:538
  92.3 1.8 %collective-permute-start.34 = (f32[8,256]{1,0:T(8,128)S(1)}, f32[8,256]{1,0:T(8,128)S(1)}, u32[]{:S(2)}, u32[]{:S(2)}) collective-permute-start(f32[8,256]{1,0:T(8,128)S(1)} %pad_maximum_fusion.4.refs_4_), channel_id=1, source_target_pairs={{0,12},{4,8},{8,4},{12,0},{1,13},{5,9},{9,5},{13,1},{2,14},{6,10},... | collective-permute-start | bytes 24584 | tf_op jit(solution)/shard_map/ppermute | solution.py:239
  94.1 1.9 %expert.5 = (bf16[64,2048]{1,0:T(8,128)(2,1)S(1)}, bf16[64,2048]{1,0:T(8,128)(2,1)S(1)}, bf16[128,2048]{1,0:T(8,128)(2,1)S(1)}) custom-call(bf16[64,2048]{1,0:T(8,128)(2,1)S(1)} %collective-permute-done.13.refs_0_, bf16[64,2048]{1,0:T(8,128)(2,1)S(1)} %collective-permute-done.14.refs_1_, bf16[64,2048]{1,0:T(8,128)(2,1)S(1)} %collective-permute-done.15.refs_2_, ...), custom_call_target="tpu_custom_call" | custom-call | flops 1610612736 | bytes 4194304 | tf_op jit(solution)/shard_map/expert/pallas_call | solution.py:538
  96.0 1.8 %collective-permute-done.34.refs_4_ = f32[8,256]{1,0:T(8,128)S(1)} collective-permute-done((f32[8,256]{1,0:T(8,128)S(1)}, f32[8,256]{1,0:T(8,128)S(1)}, u32[]{:S(2)}, u32[]{:S(2)}) %collective-permute-start.34) | collective-permute-done | bytes 8224 | tf_op jit(solution)/shard_map/ppermute | solution.py:239
  97.8 1.9 %expert.7 = (bf16[64,2048]{1,0:T(8,128)(2,1)S(1)}, bf16[64,2048]{1,0:T(8,128)(2,1)S(1)}, bf16[128,2048]{1,0:T(8,128)(2,1)S(1)}) custom-call(bf16[64,2048]{1,0:T(8,128)(2,1)S(1)} %pick.1.refs_0_, bf16[64,2048]{1,0:T(8,128)(2,1)S(1)} %collective-permute-done.31.refs_1_, bf16[64,2048]{1,0:T(8,128)(2,1)S(1)} %collective-permute-done.32.refs_2_, ...), custom_call_target="tpu_custom_call" | custom-call | flops 1610612736 | bytes 4194304 | tf_op jit(solution)/shard_map/expert/pallas_call | solution.py:538
  99.7 0.6 collective-permute-start.35
  100.4 1.6 %collective-permute-start.12 = (bf16[64,2048]{1,0:T(8,128)(2,1)S(1)}, bf16[64,2048]{1,0:T(8,128)(2,1)S(1)}, u32[]{:S(2)}, u32[]{:S(2)}) collective-permute-start(bf16[64,2048]{1,0:T(8,128)(2,1)S(1)} %fusion.21), channel_id=1, source_target_pairs={{0,2},{1,3},{2,0},{3,1},{4,6},{5,7},{6,4},{7,5},{8,10},{9,11},{10,... | collective-permute-start | bytes 786440 | tf_op jit(solution)/shard_map/ppermute | solution.py:239
  102.2 0.6 collective-permute-start.27
  102.9 1.6 %collective-permute-start.19 = (bf16[64,2048]{1,0:T(8,128)(2,1)S(1)}, bf16[64,2048]{1,0:T(8,128)(2,1)S(1)}, u32[]{:S(2)}, u32[]{:S(2)}) collective-permute-start(bf16[64,2048]{1,0:T(8,128)(2,1)S(1)} %fusion.18), channel_id=1, source_target_pairs={{0,2},{1,3},{2,0},{3,1},{4,6},{5,7},{6,4},{7,5},{8,10},{9,11},{10,... | collective-permute-start | bytes 786440 | tf_op jit(solution)/shard_map/ppermute | solution.py:239
  104.7 0.6 collective-permute-start.36
  105.3 10.0 %collective-permute-done.27 = bf16[64,2048]{1,0:T(8,128)(2,1)S(1)} collective-permute-done((bf16[64,2048]{1,0:T(8,128)(2,1)S(1)}, bf16[64,2048]{1,0:T(8,128)(2,1)S(1)}, u32[]{:S(2)}, u32[]{:S(2)}) %collective-permute-start.27) | collective-permute-done | bytes 262176 | tf_op jit(solution)/shard_map/ppermute | solution.py:239
  115.4 0.6 collective-permute-start.28
  116.0 5.0 %collective-permute-done.19 = bf16[64,2048]{1,0:T(8,128)(2,1)S(1)} collective-permute-done((bf16[64,2048]{1,0:T(8,128)(2,1)S(1)}, bf16[64,2048]{1,0:T(8,128)(2,1)S(1)}, u32[]{:S(2)}, u32[]{:S(2)}) %collective-permute-start.19) | collective-permute-done | bytes 262176 | tf_op jit(solution)/shard_map/ppermute | solution.py:239
  121.0 0.3 collective-permute-start.20
  121.3 4.3 %collective-permute-done.36 = bf16[64,2048]{1,0:T(8,128)(2,1)S(1)} collective-permute-done((bf16[64,2048]{1,0:T(8,128)(2,1)S(1)}, bf16[64,2048]{1,0:T(8,128)(2,1)S(1)}, u32[]{:S(2)}, u32[]{:S(2)}) %collective-permute-start.36) | collective-permute-done | bytes 262176 | tf_op jit(solution)/shard_map/ppermute | solution.py:239
  125.7 1.8 %collective-permute-start.37 = (bf16[64,2048]{1,0:T(8,128)(2,1)S(1)}, bf16[64,2048]{1,0:T(8,128)(2,1)S(1)}, u32[]{:S(2)}, u32[]{:S(2)}) collective-permute-start(bf16[64,2048]{1,0:T(8,128)(2,1)S(1)} %fusion.14), channel_id=1, source_target_pairs={{0,12},{4,8},{8,4},{12,0},{1,13},{5,9},{9,5},{13,1},{2,14},{6,10},... | collective-permute-start | bytes 786440 | tf_op jit(solution)/shard_map/ppermute | solution.py:239
  127.5 0.7 collective-permute-done.28
  128.2 10.4 %collective-permute-done.20 = bf16[64,2048]{1,0:T(8,128)(2,1)S(1)} collective-permute-done((bf16[64,2048]{1,0:T(8,128)(2,1)S(1)}, bf16[64,2048]{1,0:T(8,128)(2,1)S(1)}, u32[]{:S(2)}, u32[]{:S(2)}) %collective-permute-start.20) | collective-permute-done | bytes 262176 | tf_op jit(solution)/shard_map/ppermute | solution.py:239
  138.6 1.0 fusion.11
  (94 shorter events, 3.0 us)
Async XLA Ops:
  0.0 30.8 %copy-start = (bf16[256,2048]{1,0:T(8,128)(2,1)S(1)}, bf16[256,2048]{1,0:T(8,128)(2,1)}, u32[]{:S(2)}) copy-start(bf16[256,2048]{1,0:T(8,128)(2,1)} %param.32) | copy-start | bytes 3145732
  0.0 13.4 %copy-start.10 = (f32[64]{0:T(128)S(1)}, f32[64]{0:T(128)}, u32[]{:S(2)}) copy-start(f32[64]{0:T(128)} %param.26) | copy-start | bytes 772
  0.0 13.5 %copy-start.11 = (f32[128]{0:T(128)S(1)}, f32[128]{0:T(128)}, u32[]{:S(2)}) copy-start(f32[128]{0:T(128)} %param.28) | copy-start | bytes 1540
  2.4 19.5 %collective-permute-start = (bf16[256,512]{1,0:T(8,128)(2,1)}, bf16[256,512]{1,0:T(8,128)(2,1)S(1)}, u32[]{:S(2)}, u32[]{:S(2)}) collective-permute-start(bf16[256,512]{1,0:T(8,128)(2,1)} %keys.1.rest_0_), channel_id=1, source_target_pairs={{0,4},{4,0},{8,12},{12,8},{1,5},{5,1},{9,13},{13,9},{2,6},{6,2},{1... | collective-permute-start | bytes 786440 | tf_op jit(solution)/shard_map/ppermute | solution.py:239
  5.5 15.9 %collective-permute-start.1 = (bf16[256,512]{1,0:T(8,128)(2,1)}, bf16[256,512]{1,0:T(8,128)(2,1)S(1)}, u32[]{:S(2)}, u32[]{:S(2)}) collective-permute-start(bf16[256,512]{1,0:T(8,128)(2,1)} %keys.1.rest_0_), channel_id=1, source_target_pairs={{0,8},{4,12},{8,0},{12,4},{1,9},{5,13},{9,1},{13,5},{2,10},{6,14},... | collective-permute-start | bytes 786440 | tf_op jit(solution)/shard_map/ppermute | solution.py:239
  8.1 13.8 %collective-permute-start.2 = (bf16[256,512]{1,0:T(8,128)(2,1)}, bf16[256,512]{1,0:T(8,128)(2,1)S(1)}, u32[]{:S(2)}, u32[]{:S(2)}) collective-permute-start(bf16[256,512]{1,0:T(8,128)(2,1)} %keys.1.rest_0_), channel_id=1, source_target_pairs={{0,0},{4,8},{8,4},{12,12},{1,1},{5,9},{9,5},{13,13},{2,2},{6,10},{... | collective-permute-start | bytes 786440 | tf_op jit(solution)/shard_map/ppermute | solution.py:247
  13.9 13.9 %copy-start.4 = (bf16[256,512]{1,0:T(8,128)(2,1)S(1)}, bf16[256,512]{1,0:T(8,128)(2,1)}, u32[]{:S(2)}) copy-start(bf16[256,512]{1,0:T(8,128)(2,1)} %keys.1.rest_0_) | copy-start | bytes 786436
  21.4 6.4 %collective-permute-start.3 = (bf16[256,512]{1,0:T(8,128)(2,1)S(1)}, bf16[256,512]{1,0:T(8,128)(2,1)S(1)}, u32[]{:S(2)}, u32[]{:S(2)}) collective-permute-start(bf16[256,512]{1,0:T(8,128)(2,1)S(1)} %collective-permute-done.1.rest_2_), channel_id=1, source_target_pairs={{0,4},{4,0},{8,12},{12,8},{1,5},{5,1},{9,13},{13,9},{2,6},{6,2},{1... | collective-permute-start | bytes 786440 | tf_op jit(solution)/shard_map/ppermute | solution.py:239
  21.8 9.3 %copy-start.5 = (bf16[256,2048]{1,0:T(8,128)(2,1)S(1)}, bf16[256,2048]{1,0:T(8,128)(2,1)}, u32[]{:S(2)}) copy-start(bf16[256,2048]{1,0:T(8,128)(2,1)} %param.31) | copy-start | bytes 3145732
  31.4 2.0 %collective-permute-start.4 = (bf16[128,2048]{1,0:T(8,128)(2,1)S(1)}, bf16[128,2048]{1,0:T(8,128)(2,1)S(1)}, u32[]{:S(2)}, u32[]{:S(2)}) collective-permute-start(bf16[128,2048]{1,0:T(8,128)(2,1)S(1)} %fusion.4), channel_id=1, source_target_pairs={{0,1},{1,0},{2,3},{3,2},{4,5},{5,4},{6,7},{7,6},{8,9},{9,8},{10,11... | collective-permute-start | bytes 1572872 | tf_op jit(solution)/shard_map/ppermute | solution.py:239
  31.8 4.3 %copy-start.8 = (f32[64,2]{0,1:T(2,128)S(1)}, f32[64,2]{0,1:T(2,128)}, u32[]{:S(2)}) copy-start(f32[64,2]{0,1:T(2,128)} %param.35) | copy-start | bytes 1540
  31.8 12.6 %copy-start.7 = (f32[2048]{0:T(1024)S(1)}, f32[2048]{0:T(1024)}, u32[]{:S(2)}) copy-start(f32[2048]{0:T(1024)} %param.33) | copy-start | bytes 24580
  31.8 15.3 %copy-start.9 = (s32[64,2]{0,1:T(2,128)S(1)}, s32[64,2]{0,1:T(2,128)}, u32[]{:S(2)}) copy-start(s32[64,2]{0,1:T(2,128)} %param.34) | copy-start | bytes 1540
  33.7 0.8 copy-start.6
  34.5 49.7 %copy-start.1 = (bf16[2,2048,256]{2,1,0:T(8,128)(2,1)S(1)}, bf16[2,2048,256]{2,1,0:T(8,128)(2,1)}, u32[]{:S(2)}) copy-start(bf16[2,2048,256]{2,1,0:T(8,128)(2,1)} %refs_5_.7) | copy-start | bytes 6291460
  34.5 8.5 %collective-permute-start.5 = (bf16[64,2048]{1,0:T(8,128)(2,1)S(1)}, bf16[64,2048]{1,0:T(8,128)(2,1)}, u32[]{:S(2)}, u32[]{:S(2)}) collective-permute-start(bf16[64,2048]{1,0:T(8,128)(2,1)S(1)} %slice.109), channel_id=1, source_target_pairs={{0,2},{1,3},{2,0},{3,1},{4,6},{5,7},{6,4},{7,5},{8,10},{9,11},{10,... | collective-permute-start | bytes 786440 | tf_op jit(solution)/shard_map/ppermute | solution.py:239
  44.6 14.0 %collective-permute-start.21 = (bf16[64,2048]{1,0:T(8,128)(2,1)S(1)}, bf16[64,2048]{1,0:T(8,128)(2,1)S(1)}, u32[]{:S(2)}, u32[]{:S(2)}) collective-permute-start(bf16[64,2048]{1,0:T(8,128)(2,1)S(1)} %fusion.7.refs_0_), channel_id=1, source_target_pairs={{0,8},{4,12},{8,0},{12,4},{1,9},{5,13},{9,1},{13,5},{2,10},{6,14},... | collective-permute-start | bytes 786440 | tf_op jit(solution)/shard_map/ppermute | solution.py:239
  45.6 23.8 %collective-permute-start.6 = (bf16[64,2048]{1,0:T(8,128)(2,1)S(1)}, bf16[64,2048]{1,0:T(8,128)(2,1)S(1)}, u32[]{:S(2)}, u32[]{:S(2)}) collective-permute-start(bf16[64,2048]{1,0:T(8,128)(2,1)S(1)} %fusion.7.refs_0_), channel_id=1, source_target_pairs={{0,2},{1,3},{2,0},{3,1},{4,6},{5,7},{6,4},{7,5},{8,10},{9,11},{10,... | collective-permute-start | bytes 786440 | tf_op jit(solution)/shard_map/ppermute | solution.py:239
  47.2 5.8 %collective-permute-start.9 = (f32[8,64]{1,0:T(8,128)S(1)}, f32[8,64]{1,0:T(8,128)S(1)}, u32[]{:S(2)}, u32[]{:S(2)}) collective-permute-start(f32[8,64]{1,0:T(8,128)S(1)} %bitcast.24), channel_id=1, source_target_pairs={{0,2},{1,3},{2,0},{3,1},{4,6},{5,7},{6,4},{7,5},{8,10},{9,11},{10,... | collective-permute-start | bytes 6152 | tf_op jit(solution)/shard_map/ppermute | solution.py:239
  47.7 23.2 %collective-permute-start.29 = (bf16[64,2048]{1,0:T(8,128)(2,1)S(1)}, bf16[64,2048]{1,0:T(8,128)(2,1)S(1)}, u32[]{:S(2)}, u32[]{:S(2)}) collective-permute-start(bf16[64,2048]{1,0:T(8,128)(2,1)S(1)} %fusion.7.refs_0_), channel_id=1, source_target_pairs={{0,0},{4,8},{8,4},{12,12},{1,1},{5,9},{9,5},{13,13},{2,2},{6,10},{... | collective-permute-start | bytes 786440 | tf_op jit(solution)/shard_map/ppermute | solution.py:247
  48.4 22.8 %collective-permute-start.13 = (bf16[64,2048]{1,0:T(8,128)(2,1)S(1)}, bf16[64,2048]{1,0:T(8,128)(2,1)S(1)}, u32[]{:S(2)}, u32[]{:S(2)}) collective-permute-start(bf16[64,2048]{1,0:T(8,128)(2,1)S(1)} %fusion.7.refs_0_), channel_id=1, source_target_pairs={{0,4},{4,0},{8,12},{12,8},{1,5},{5,1},{9,13},{13,9},{2,6},{6,2},{1... | collective-permute-start | bytes 786440 | tf_op jit(solution)/shard_map/ppermute | solution.py:239
  53.0 5.6 %collective-permute-start.10 = (f32[8,128]{1,0:T(8,128)S(1)}, f32[8,128]{1,0:T(8,128)S(1)}, u32[]{:S(2)}, u32[]{:S(2)}) collective-permute-start(f32[8,128]{1,0:T(8,128)S(1)} %pad_maximum_fusion.5), channel_id=1, source_target_pairs={{0,1},{1,0},{2,3},{3,2},{4,5},{5,4},{6,7},{7,6},{8,9},{9,8},{10,11... | collective-permute-start | bytes 12296 | tf_op jit(solution)/shard_map/ppermute | solution.py:239
  58.6 13.1 %collective-permute-start.30 = (bf16[64,2048]{1,0:T(8,128)(2,1)S(1)}, bf16[64,2048]{1,0:T(8,128)(2,1)S(1)}, u32[]{:S(2)}, u32[]{:S(2)}) collective-permute-start(bf16[64,2048]{1,0:T(8,128)(2,1)S(1)} %collective-permute-done.21.refs_0_), channel_id=1, source_target_pairs={{0,4},{4,0},{8,12},{12,8},{1,5},{5,1},{9,13},{13,9},{2,6},{6,2},{1... | collective-permute-start | bytes 786440 | tf_op jit(solution)/shard_map/ppermute | solution.py:239
  58.7 6.0 %collective-permute-start.25 = (f32[8,256]{1,0:T(8,128)S(1)}, f32[8,256]{1,0:T(8,128)S(1)}, u32[]{:S(2)}, u32[]{:S(2)}) collective-permute-start(f32[8,256]{1,0:T(8,128)S(1)} %pad_maximum_fusion.4.refs_4_), channel_id=1, source_target_pairs={{0,8},{4,12},{8,0},{12,4},{1,9},{5,13},{9,1},{13,5},{2,10},{6,14},... | collective-permute-start | bytes 24584 | tf_op jit(solution)/shard_map/ppermute | solution.py:239
  64.7 4.7 %collective-permute-start.17 = (f32[8,256]{1,0:T(8,128)S(1)}, f32[8,256]{1,0:T(8,128)S(1)}, u32[]{:S(2)}, u32[]{:S(2)}) collective-permute-start(f32[8,256]{1,0:T(8,128)S(1)} %pad_maximum_fusion.4.refs_4_), channel_id=1, source_target_pairs={{0,4},{4,0},{8,12},{12,8},{1,5},{5,1},{9,13},{13,9},{2,6},{6,2},{1... | collective-permute-start | bytes 24584 | tf_op jit(solution)/shard_map/ppermute | solution.py:239
  69.5 2.5 %collective-permute-start.7 = (bf16[64,2048]{1,0:T(8,128)(2,1)S(1)}, bf16[64,2048]{1,0:T(8,128)(2,1)S(1)}, u32[]{:S(2)}, u32[]{:S(2)}) collective-permute-start(bf16[64,2048]{1,0:T(8,128)(2,1)S(1)} %fusion.7.refs_0_), channel_id=1, source_target_pairs={{0,1},{1,0},{2,3},{3,2},{4,5},{5,4},{6,7},{7,6},{8,9},{9,8},{10,11... | collective-permute-start | bytes 786440 | tf_op jit(solution)/shard_map/ppermute | solution.py:239
  69.5 9.2 %collective-permute-start.22 = (bf16[64,2048]{1,0:T(8,128)(2,1)S(1)}, bf16[64,2048]{1,0:T(8,128)(2,1)S(1)}, u32[]{:S(2)}, u32[]{:S(2)}) collective-permute-start(bf16[64,2048]{1,0:T(8,128)(2,1)S(1)} %collective-permute-done.21.refs_0_), channel_id=1, source_target_pairs={{0,2},{1,3},{2,0},{3,1},{4,6},{5,7},{6,4},{7,5},{8,10},{9,11},{10,... | collective-permute-start | bytes 786440 | tf_op jit(solution)/shard_map/ppermute | solution.py:239
  71.0 7.7 %collective-permute-start.8 = (bf16[64,2048]{1,0:T(8,128)(2,1)S(1)}, bf16[64,2048]{1,0:T(8,128)(2,1)S(1)}, u32[]{:S(2)}, u32[]{:S(2)}) collective-permute-start(bf16[64,2048]{1,0:T(8,128)(2,1)S(1)} %collective-permute-done.6.refs_1_), channel_id=1, source_target_pairs={{0,1},{1,0},{2,3},{3,2},{4,5},{5,4},{6,7},{7,6},{8,9},{9,8},{10,11... | collective-permute-start | bytes 786440 | tf_op jit(solution)/shard_map/ppermute | solution.py:239
  71.2 13.1 %collective-permute-start.14 = (bf16[64,2048]{1,0:T(8,128)(2,1)S(1)}, bf16[64,2048]{1,0:T(8,128)(2,1)S(1)}, u32[]{:S(2)}, u32[]{:S(2)}) collective-permute-start(bf16[64,2048]{1,0:T(8,128)(2,1)S(1)} %collective-permute-done.13.refs_0_), channel_id=1, source_target_pairs={{0,2},{1,3},{2,0},{3,1},{4,6},{5,7},{6,4},{7,5},{8,10},{9,11},{10,... | collective-permute-start | bytes 786440 | tf_op jit(solution)/shard_map/ppermute | solution.py:239
  71.7 17.6 %collective-permute-start.23 = (bf16[64,2048]{1,0:T(8,128)(2,1)S(1)}, bf16[64,2048]{1,0:T(8,128)(2,1)S(1)}, u32[]{:S(2)}, u32[]{:S(2)}) collective-permute-start(bf16[64,2048]{1,0:T(8,128)(2,1)S(1)} %collective-permute-done.21.refs_0_), channel_id=1, source_target_pairs={{0,1},{1,0},{2,3},{3,2},{4,5},{5,4},{6,7},{7,6},{8,9},{9,8},{10,11... | collective-permute-start | bytes 786440 | tf_op jit(solution)/shard_map/ppermute | solution.py:239
  71.9 18.0 %collective-permute-start.31 = (bf16[64,2048]{1,0:T(8,128)(2,1)S(1)}, bf16[64,2048]{1,0:T(8,128)(2,1)S(1)}, u32[]{:S(2)}, u32[]{:S(2)}) collective-permute-start(bf16[64,2048]{1,0:T(8,128)(2,1)S(1)} %pick.1.refs_0_), channel_id=1, source_target_pairs={{0,2},{1,3},{2,0},{3,1},{4,6},{5,7},{6,4},{7,5},{8,10},{9,11},{10,... | collective-permute-start | bytes 786440 | tf_op jit(solution)/shard_map/ppermute | solution.py:239
  78.6 11.3 %collective-permute-start.24 = (bf16[64,2048]{1,0:T(8,128)(2,1)S(1)}, bf16[64,2048]{1,0:T(8,128)(2,1)S(1)}, u32[]{:S(2)}, u32[]{:S(2)}) collective-permute-start(bf16[64,2048]{1,0:T(8,128)(2,1)S(1)} %collective-permute-done.22.refs_1_), channel_id=1, source_target_pairs={{0,1},{1,0},{2,3},{3,2},{4,5},{5,4},{6,7},{7,6},{8,9},{9,8},{10,11... | collective-permute-start | bytes 786440 | tf_op jit(solution)/shard_map/ppermute | solution.py:239
  78.6 13.6 %collective-permute-start.15 = (bf16[64,2048]{1,0:T(8,128)(2,1)S(1)}, bf16[64,2048]{1,0:T(8,128)(2,1)S(1)}, u32[]{:S(2)}, u32[]{:S(2)}) collective-permute-start(bf16[64,2048]{1,0:T(8,128)(2,1)S(1)} %collective-permute-done.13.refs_0_), channel_id=1, source_target_pairs={{0,1},{1,0},{2,3},{3,2},{4,5},{5,4},{6,7},{7,6},{8,9},{9,8},{10,11... | collective-permute-start | bytes 786440 | tf_op jit(solution)/shard_map/ppermute | solution.py:239
  84.3 9.8 %collective-permute-start.16 = (bf16[64,2048]{1,0:T(8,128)(2,1)S(1)}, bf16[64,2048]{1,0:T(8,128)(2,1)S(1)}, u32[]{:S(2)}, u32[]{:S(2)}) collective-permute-start(bf16[64,2048]{1,0:T(8,128)(2,1)S(1)} %collective-permute-done.14.refs_1_), channel_id=1, source_target_pairs={{0,1},{1,0},{2,3},{3,2},{4,5},{5,4},{6,7},{7,6},{8,9},{9,8},{10,11... | collective-permute-start | bytes 786440 | tf_op jit(solution)/shard_map/ppermute | solution.py:239
  84.3 1.6 %copy-start.2 = (bf16[2,2048,256]{2,1,0:T(8,128)(2,1)S(1)}, bf16[2,2048,256]{2,1,0:T(8,128)(2,1)}, u32[]{:S(2)}) copy-start(bf16[2,2048,256]{2,1,0:T(8,128)(2,1)} %refs_6_.8) | copy-start | bytes 6291460
  85.9 1.6 %copy-start.3 = (bf16[2,256,2048]{2,1,0:T(8,128)(2,1)S(1)}, bf16[2,256,2048]{2,1,0:T(8,128)(2,1)}, u32[]{:S(2)}) copy-start(bf16[2,256,2048]{2,1,0:T(8,128)(2,1)} %param.38) | copy-start | bytes 6291460
  89.3 10.9 %collective-permute-start.11 = (bf16[128,2048]{1,0:T(8,128)(2,1)S(1)}, bf16[128,2048]{1,0:T(8,128)(2,1)S(1)}, u32[]{:S(2)}, u32[]{:S(2)}) collective-permute-start(bf16[128,2048]{1,0:T(8,128)(2,1)S(1)} %get-tuple-element.22), channel_id=1, source_target_pairs={{0,1},{1,0},{2,3},{3,2},{4,5},{5,4},{6,7},{7,6},{8,9},{9,8},{10,11... | collective-permute-start | bytes 1572872 | tf_op jit(solution)/shard_map/ppermute | solution.py:239
  89.9 7.9 %collective-permute-start.32 = (bf16[64,2048]{1,0:T(8,128)(2,1)S(1)}, bf16[64,2048]{1,0:T(8,128)(2,1)S(1)}, u32[]{:S(2)}, u32[]{:S(2)}) collective-permute-start(bf16[64,2048]{1,0:T(8,128)(2,1)S(1)} %pick.1.refs_0_), channel_id=1, source_target_pairs={{0,1},{1,0},{2,3},{3,2},{4,5},{5,4},{6,7},{7,6},{8,9},{9,8},{10,11... | collective-permute-start | bytes 786440 | tf_op jit(solution)/shard_map/ppermute | solution.py:239
  90.0 7.8 %collective-permute-start.33 = (bf16[64,2048]{1,0:T(8,128)(2,1)S(1)}, bf16[64,2048]{1,0:T(8,128)(2,1)S(1)}, u32[]{:S(2)}, u32[]{:S(2)}) collective-permute-start(bf16[64,2048]{1,0:T(8,128)(2,1)S(1)} %collective-permute-done.31.refs_1_), channel_id=1, source_target_pairs={{0,1},{1,0},{2,3},{3,2},{4,5},{5,4},{6,7},{7,6},{8,9},{9,8},{10,11... | collective-permute-start | bytes 786440 | tf_op jit(solution)/shard_map/ppermute | solution.py:239
  92.3 5.5 %collective-permute-start.34 = (f32[8,256]{1,0:T(8,128)S(1)}, f32[8,256]{1,0:T(8,128)S(1)}, u32[]{:S(2)}, u32[]{:S(2)}) collective-permute-start(f32[8,256]{1,0:T(8,128)S(1)} %pad_maximum_fusion.4.refs_4_), channel_id=1, source_target_pairs={{0,12},{4,8},{8,4},{12,0},{1,13},{5,9},{9,5},{13,1},{2,14},{6,10},... | collective-permute-start | bytes 24584 | tf_op jit(solution)/shard_map/ppermute | solution.py:239
  94.1 7.9 %collective-permute-start.26 = (bf16[128,2048]{1,0:T(8,128)(2,1)S(1)}, bf16[128,2048]{1,0:T(8,128)(2,1)S(1)}, u32[]{:S(2)}, u32[]{:S(2)}) collective-permute-start(bf16[128,2048]{1,0:T(8,128)(2,1)S(1)} %get-tuple-element.28), channel_id=1, source_target_pairs={{0,1},{1,0},{2,3},{3,2},{4,5},{5,4},{6,7},{7,6},{8,9},{9,8},{10,11... | collective-permute-start | bytes 1572872 | tf_op jit(solution)/shard_map/ppermute | solution.py:239
  97.8 5.0 %collective-permute-start.18 = (bf16[128,2048]{1,0:T(8,128)(2,1)S(1)}, bf16[128,2048]{1,0:T(8,128)(2,1)S(1)}, u32[]{:S(2)}, u32[]{:S(2)}) collective-permute-start(bf16[128,2048]{1,0:T(8,128)(2,1)S(1)} %get-tuple-element.25), channel_id=1, source_target_pairs={{0,1},{1,0},{2,3},{3,2},{4,5},{5,4},{6,7},{7,6},{8,9},{9,8},{10,11... | collective-permute-start | bytes 1572872 | tf_op jit(solution)/shard_map/ppermute | solution.py:239
  99.7 4.8 %collective-permute-start.35 = (bf16[128,2048]{1,0:T(8,128)(2,1)S(1)}, bf16[128,2048]{1,0:T(8,128)(2,1)S(1)}, u32[]{:S(2)}, u32[]{:S(2)}) collective-permute-start(bf16[128,2048]{1,0:T(8,128)(2,1)S(1)} %get-tuple-element.31), channel_id=1, source_target_pairs={{0,1},{1,0},{2,3},{3,2},{4,5},{5,4},{6,7},{7,6},{8,9},{9,8},{10,11... | collective-permute-start | bytes 1572872 | tf_op jit(solution)/shard_map/ppermute | solution.py:239
  100.4 27.1 %collective-permute-start.12 = (bf16[64,2048]{1,0:T(8,128)(2,1)S(1)}, bf16[64,2048]{1,0:T(8,128)(2,1)S(1)}, u32[]{:S(2)}, u32[]{:S(2)}) collective-permute-start(bf16[64,2048]{1,0:T(8,128)(2,1)S(1)} %fusion.21), channel_id=1, source_target_pairs={{0,2},{1,3},{2,0},{3,1},{4,6},{5,7},{6,4},{7,5},{8,10},{9,11},{10,... | collective-permute-start | bytes 786440 | tf_op jit(solution)/shard_map/ppermute | solution.py:239
  102.2 13.1 %collective-permute-start.27 = (bf16[64,2048]{1,0:T(8,128)(2,1)S(1)}, bf16[64,2048]{1,0:T(8,128)(2,1)S(1)}, u32[]{:S(2)}, u32[]{:S(2)}) collective-permute-start(bf16[64,2048]{1,0:T(8,128)(2,1)S(1)} %fusion.15), channel_id=1, source_target_pairs={{0,2},{1,3},{2,0},{3,1},{4,6},{5,7},{6,4},{7,5},{8,10},{9,11},{10,... | collective-permute-start | bytes 786440 | tf_op jit(solution)/shard_map/ppermute | solution.py:239
  102.9 18.0 %collective-permute-start.19 = (bf16[64,2048]{1,0:T(8,128)(2,1)S(1)}, bf16[64,2048]{1,0:T(8,128)(2,1)S(1)}, u32[]{:S(2)}, u32[]{:S(2)}) collective-permute-start(bf16[64,2048]{1,0:T(8,128)(2,1)S(1)} %fusion.18), channel_id=1, source_target_pairs={{0,2},{1,3},{2,0},{3,1},{4,6},{5,7},{6,4},{7,5},{8,10},{9,11},{10,... | collective-permute-start | bytes 786440 | tf_op jit(solution)/shard_map/ppermute | solution.py:239
  104.7 20.9 %collective-permute-start.36 = (bf16[64,2048]{1,0:T(8,128)(2,1)S(1)}, bf16[64,2048]{1,0:T(8,128)(2,1)S(1)}, u32[]{:S(2)}, u32[]{:S(2)}) collective-permute-start(bf16[64,2048]{1,0:T(8,128)(2,1)S(1)} %fusion.12), channel_id=1, source_target_pairs={{0,2},{1,3},{2,0},{3,1},{4,6},{5,7},{6,4},{7,5},{8,10},{9,11},{10,... | collective-permute-start | bytes 786440 | tf_op jit(solution)/shard_map/ppermute | solution.py:239
  115.4 12.8 %collective-permute-start.28 = (bf16[64,2048]{1,0:T(8,128)(2,1)S(1)}, bf16[64,2048]{1,0:T(8,128)(2,1)S(1)}, u32[]{:S(2)}, u32[]{:S(2)}) collective-permute-start(bf16[64,2048]{1,0:T(8,128)(2,1)S(1)} %fusion.17), channel_id=1, source_target_pairs={{0,8},{4,12},{8,0},{12,4},{1,9},{5,13},{9,1},{13,5},{2,10},{6,14},... | collective-permute-start | bytes 786440 | tf_op jit(solution)/shard_map/ppermute | solution.py:239
  121.0 17.6 %collective-permute-start.20 = (bf16[64,2048]{1,0:T(8,128)(2,1)S(1)}, bf16[64,2048]{1,0:T(8,128)(2,1)S(1)}, u32[]{:S(2)}, u32[]{:S(2)}) collective-permute-start(bf16[64,2048]{1,0:T(8,128)(2,1)S(1)} %fusion.20), channel_id=1, source_target_pairs={{0,4},{4,0},{8,12},{12,8},{1,5},{5,1},{9,13},{13,9},{2,6},{6,2},{1... | collective-permute-start | bytes 786440 | tf_op jit(solution)/shard_map/ppermute | solution.py:239
  125.7 13.0 %collective-permute-start.37 = (bf16[64,2048]{1,0:T(8,128)(2,1)S(1)}, bf16[64,2048]{1,0:T(8,128)(2,1)S(1)}, u32[]{:S(2)}, u32[]{:S(2)}) collective-permute-start(bf16[64,2048]{1,0:T(8,128)(2,1)S(1)} %fusion.14), channel_id=1, source_target_pairs={{0,12},{4,8},{8,4},{12,0},{1,13},{5,9},{9,5},{13,1},{2,14},{6,10},... | collective-permute-start | bytes 786440 | tf_op jit(solution)/shard_map/ppermute | solution.py:239
